TPU v7x, 32 devices: a whole 2x2x4 slice. The times are simulated.
32 devices in a mesh: sp: 16 (over z, y, core), tp: 2 (over x).
Axes of the slice: x: 2, y: 2, z: 4, core: 2. Of those that a mesh axis runs over, the one named last changes fastest.
Arguments:
- inputs: bfloat16 [4096, 4096], P('sp', 'tp'), may hold values from -20 to 20
- norm_gain: float32 [3, 4096], replicated, may hold values from 0.1 to 1.9
- in_weight: bfloat16 [3, 4096, 1024], P(None, 'tp', 'sp'), may hold values from -0.09375 to 0.09375
- pool_scale: float32 [3, 1024], replicated, may hold values from 0.1 to 1.9
- out_weight: bfloat16 [3, 1024, 4096], P(None, 'sp', 'tp'), may hold values from -0.1875 to 0.1875
Outputs:
- final_state: bfloat16 [4096, 4096], P('sp', 'tp')
All inputs are finite; a program needn't handle non-finite values.
Results may differ from a plain program's by a relative error of at most 0.017.
Values may be sent and summed in bfloat16 or wider, within the bound.
No kernel may reach another device: no remote copies, remote signals or barrier semaphores. Data moves between devices by JAX's collectives and lax.ppermute only.
A program may use at most 64 MiB of HBM per device.

v0:
```python
import functools
import math

import jax
import jax.numpy as jnp
import numpy as np
from jax import lax
from jax.experimental import pallas as pl
from jax.experimental.pallas import tpu as pltpu
from jax.sharding import PartitionSpec as P


epsilon = 1e-06
early_pieces = ()
window = 16
group_count = 4
lanes = 128
row_tile = 16


VMEM = pl.BlockSpec(memory_space=pltpu.VMEM)
SMEM = pl.BlockSpec(memory_space=pltpu.SMEM)
ANY = pl.BlockSpec(memory_space=pl.ANY)


def move(value, axis, target):
    pairs = [(s, target(s)) for s in range(lax.axis_size(axis))]
    return lax.ppermute(value, axis, [(s, t) for s, t in pairs if t is not None])


def levels(nz):
    return [1 << b for b in range(nz.bit_length() - 1)]


def next_hop(z, m, step):
    at = z % (2 * m)
    if step == 0:
        return z + 1 if at == m - 1 else z - 1 if at == m else None
    return z - 1 if at == m - step else z + 1 if at == m - 1 + step else None


def order_table(nz):
    table = [[z] for z in range(nz)]
    for m in levels(nz):
        edge = lambda z: z - z % (2 * m) + (m if z % (2 * m) < m else m - 1)
        table = [table[z] + table[edge(z)] for z in range(nz)]
    return table


def hop(value, m, step):
    def target(s):
        z = next_hop(s // 4, m, step)
        return None if z is None else 4 * z + s % 4

    return move(value, "sp", target)


def gather(own, nz, split, early):
    across = lambda v: move(v, "sp", lambda s: s ^ 2)
    beyond = lambda at: [p + nz for p in at]
    join = lambda parts: [(jnp.concatenate([v for v, _ in parts], 0), sum([at for _, at in parts], []))]
    z = lax.axis_index("sp") // 4
    pieces = [(own, [0])]
    for m in levels(nz):
        last = 2 * m == nz
        if early and last:
            pieces = join(pieces + [(across(v), beyond(at)) for v, at in pieces])
        arrived = []
        for v, at in pieces:
            steps = z % (2 * m)
            steps = jnp.where(steps < m, m - 1 - steps, steps - m)
            far = got = hop(v, m, 0)
            for t in range(1, m):
                got = hop(got, m, t)
                far = jnp.where(steps == t, got, far)
            arrived.append((far, [q + m for q in at]))
        pieces = pieces + arrived
        if not split and not last:
            pieces = join(pieces)
    if not early:
        pieces = pieces + [(across(v), beyond(at)) for v, at in pieces]
    return pieces


def load_weight(pieces, refs, shard, w, sems):
    copies = []
    for (_, places), ref in zip(pieces, refs):
        for k, place in enumerate(places):
            copies.append(
                pltpu.make_async_copy(
                    ref.at[pl.ds(k * shard, shard)],
                    w.at[pl.ds(place * shard, shard)],
                    sems.at[len(copies)],
                )
            )
    for copy in copies:
        copy.start()
    return copies


def in_kernel(first, pieces, shard, *refs):
    refs = list(refs)
    state = refs.pop(0)
    deltas = [] if first else [refs.pop(0), refs.pop(0)]
    arrays = [refs.pop(0) for _ in pieces]
    fresh = state if first else refs.pop(0)
    out, squares, w, sq, sems = refs
    copies = load_weight(pieces, arrays, shard, w, sems)
    rows = state.shape[0]
    tile = 5 * row_tile if rows % (5 * row_tile) == 0 else row_tile

    @pl.loop(0, rows // tile)
    def _(i):
        at = pl.ds(pl.multiple_of(i * tile, row_tile), tile)
        value = state[at, :].astype(jnp.float32)
        if not first:
            value = value + (deltas[0][at, :].astype(jnp.float32) + deltas[1][at, :].astype(jnp.float32))
            rounded = value.astype(jnp.bfloat16)
            fresh[at, :] = rounded
            value = rounded.astype(jnp.float32)
        total = jnp.sum(value * value, axis=1, keepdims=True)
        sq[at, :] = jnp.broadcast_to(total, (tile, lanes))

    if rows < sq.shape[0]:
        sq[rows:, :] = jnp.zeros((sq.shape[0] - rows, lanes), jnp.float32)
    squares[...] = sq[...].T[: squares.shape[0], :]
    for copy in copies:
        copy.wait()
    step = min(256, w.shape[0])
    for n in range(0, w.shape[0], step):
        out[:, n : n + step] = lax.dot_general(
            fresh[...], w[n : n + step, :], (((1,), (1,)), ((), ())), preferred_element_type=jnp.float32
        ).astype(jnp.bfloat16)


def out_kernel(last, pieces, shard, features, halo, *refs):
    refs = list(refs)
    place, own, other, sq_own, sq_other, group, scale = [refs.pop(0) for _ in range(7)]
    arrays = [refs.pop(0) for _ in pieces]
    outs = [refs.pop(0) for _ in range(2 if last else 1)]
    w, mixed, sems = refs
    copies = load_weight(pieces, arrays, shard, w, sems)
    rows, width = own.shape
    inv = lax.rsqrt((sq_own[...] + sq_other[...]) / features + epsilon)
    inv = jnp.broadcast_to(inv[:1, :], (lanes, inv.shape[1])).T[:rows, :]
    position = place[0] - halo + lax.broadcasted_iota(jnp.int32, (rows, lanes), 0)
    inv = jnp.where(position >= 0, inv, 0.0)
    for n in range(0, width, lanes):
        at = slice(n, n + lanes)
        value = (own[:, at].astype(jnp.float32) + other[:, at].astype(jnp.float32)) * inv
        value = value.astype(jnp.bfloat16).astype(jnp.float32)
        kind = jnp.broadcast_to(group[:1, at], (rows, lanes))
        sums, running, shift = [], value, 1
        while shift < window:
            running = running + pltpu.roll(running, shift, 0)
            sums.append(running)
            shift *= 2
        total = sums[-1]
        for g in range(group_count - 1):
            total = jnp.where(kind == g, sums[g], total)
        length = jnp.left_shift(jnp.int32(2), kind)
        divisor = jnp.maximum(jnp.minimum(position + 1, length), 1).astype(jnp.float32)
        means = total / divisor - value
        mixed[:, at] = (means * scale[:1, at]).astype(jnp.bfloat16)
    for copy in copies:
        copy.wait()
    if last:
        count = outs[0].shape[0]
        spans = [halo + place[1] * count, halo + (1 - place[1]) * count]
        takes = [pl.ds(pl.multiple_of(s, row_tile), count) for s in spans]
    else:
        takes = [pl.ds(0, rows)]
    step = min(256, w.shape[1])

    @pl.loop(0, w.shape[1] // step)
    def _(i):
        at = pl.ds(pl.multiple_of(i * step, step), step)
        for out, take in zip(outs, takes):
            out[:, at] = jnp.dot(mixed[take, :], w[:, at], preferred_element_type=jnp.float32).astype(jnp.bfloat16)


def body(inputs, norm_gain, in_weight, pool_scale, out_weight):
    rows, feats = inputs.shape
    layers, _, shard = in_weight.shape
    count = lax.axis_size("sp")
    nz = count // 4
    channels = shard * count
    half = channels // 2
    features = norm_gain.shape[1]
    bf16 = jnp.bfloat16
    here = lax.axis_index("sp")
    core = here % 2

    gain = lax.dynamic_slice_in_dim(norm_gain, lax.axis_index("tp") * feats, feats, 1)
    in_t = (jnp.swapaxes(in_weight, 1, 2).astype(jnp.float32) * gain[:, None, :]).astype(bf16)
    mats = []
    for l in range(layers):
        mats += [in_t[l], out_weight[l]]
    found = {}
    for m, own in enumerate(mats):
        found[m] = gather(own, nz, m == 0, m in early_pieces)

    order = order_table(nz)
    table = [[(order[s // 4][b % nz] * 2 + ((s // 2) % 2 ^ (b // nz))) * 2 + s % 2 for b in range(2 * nz)] for s in range(count)]
    shards = jnp.asarray(np.array(table, np.int32))[here]
    channel = (shards[:, None] * shard + jnp.arange(shard, dtype=jnp.int32)[None, :]).reshape(1, half)
    group = jnp.broadcast_to(channel // (channels // group_count), (8, half))
    scale = pool_scale.reshape(layers, count, shard)[:, shards].reshape(layers, 1, half)
    scale = jnp.broadcast_to(scale, (layers, 8, half))
    place = jnp.stack([(here // 2) * 2 * rows, core]).astype(jnp.int32)

    halo = math.ceil(layers * (window - 1) / row_tile) * row_tile
    tail = inputs[rows - halo :]
    reach = lambda d: move(tail, "sp", lambda s: s + d if s % 2 == 1 and s + d < count else None)
    before = [reach(d) for d in (1, 2)]
    sibling = move(inputs, "sp", lambda s: s ^ 1)
    low = core == 0
    state = jnp.concatenate(
        [jnp.where(low, *before), jnp.where(low, inputs, sibling), jnp.where(low, sibling, inputs)], 0
    )
    total = state.shape[0]
    padded = math.ceil(total / lanes) * lanes
    shape = jax.ShapeDtypeStruct
    params = pltpu.CompilerParams(vmem_limit_bytes=24 * 2**20)
    flops = 2 * total * feats * half
    cost = pl.CostEstimate(flops=flops, bytes_accessed=2 * (half * feats + 3 * total * feats), transcendentals=0)

    deltas = []
    for l in range(layers):
        first, last = l == 0, l == layers - 1
        pieces = found[2 * l]
        outs = [shape((total, half), bf16), shape((8, padded), jnp.float32)]
        if not first:
            outs = [shape((total, feats), bf16)] + outs
        results = pl.pallas_call(
            functools.partial(in_kernel, first, pieces, shard),
            out_shape=outs,
            in_specs=[VMEM] * (1 if first else 3) + [ANY] * len(pieces),
            out_specs=[VMEM] * len(outs),
            scratch_shapes=[
                pltpu.VMEM((half, feats), bf16),
                pltpu.VMEM((padded, lanes), jnp.float32),
                pltpu.SemaphoreType.DMA((2 * nz,)),
            ],
            compiler_params=params,
            cost_estimate=cost,
        )(state, *deltas, *[a for a, _ in pieces])
        if not first:
            state = results[0]
        partial, squares = results[-2:]
        bits = levels(lax.axis_size("tp"))
        for b, bit in enumerate(bits):
            swap = lambda v: move(v, "tp", lambda s: s ^ bit)
            others = [swap(partial), swap(squares)]
            if b < len(bits) - 1:
                partial, squares = partial + others[0], squares + others[1]
        pieces = found[2 * l + 1]
        outs = [shape((rows if last else total, feats), bf16)] * (2 if last else 1)
        results = pl.pallas_call(
            functools.partial(out_kernel, last, pieces, shard, features, halo),
            out_shape=outs,
            in_specs=[SMEM] + [VMEM] * 6 + [ANY] * len(pieces),
            out_specs=[VMEM] * len(outs),
            scratch_shapes=[
                pltpu.VMEM((half, feats), bf16),
                pltpu.VMEM((total, half), bf16),
                pltpu.SemaphoreType.DMA((2 * nz,)),
            ],
            compiler_params=params,
            cost_estimate=cost,
        )(place, partial, others[0], squares, others[1], group, scale[l], *[a for a, _ in pieces])
        deltas = [results[0], move(results[-1], "sp", lambda s: s ^ 1)]

    own = lax.dynamic_slice_in_dim(state, halo + core * rows, rows, 0)
    return (own.astype(jnp.float32) + (deltas[0].astype(jnp.float32) + deltas[1].astype(jnp.float32))).astype(bf16)


def solution(mesh):
    placed = (P("sp", "tp"), P(), P(None, "tp", "sp"), P(), P(None, "sp", "tp"))

    return jax.shard_map(body, mesh=mesh, in_specs=placed, out_specs=P("sp", "tp"), check_vma=False)
```

profile of v0, /device:TPU:4, one launch (start us, length us, event | category | flops | bytes accessed | tf_op | source)
XLA Modules:
  0.0 249.7 jit_solution(10917504963183782077)
XLA Ops:
  0.0 0.8 copy-done
  0.9 1.3 fusion
  2.2 0.9 slice_bitcast_fusion
  3.0 1.6 collective-permute-start.3
  5.4 1.3 collective-permute-start
  7.4 2.0 slice_bitcast_fusion.3
  11.0 1.4 collective-permute-done
  12.4 5.8 %collective-permute-start.14 = (bf16[64,2048]{1,0:T(8,128)(2,1)S(1)}, bf16[64,2048]{1,0:T(8,128)(2,1)S(1)}, u32[]{:S(2)}, u32[]{:S(2)}) collective-permute-start(bf16[64,2048]{1,0:T(8,128)(2,1)S(1)} %get-tuple-element.31), channel_id=1, source_target_pairs={{0,8},{2,10},{4,12},{6,14},{8,0},{10,2},{12,4},{14,6},{16,24},{18,... | collective-permute-start | bytes 786440 | tf_op jit(solution)/shard_map/ppermute | solution.py:28
  18.9 1.3 collective-permute-start.5
  20.2 3.0 %collective-permute-done.14 = bf16[64,2048]{1,0:T(8,128)(2,1)S(1)} collective-permute-done((bf16[64,2048]{1,0:T(8,128)(2,1)S(1)}, bf16[64,2048]{1,0:T(8,128)(2,1)S(1)}, u32[]{:S(2)}, u32[]{:S(2)}) %collective-permute-start.14) | collective-permute-done | bytes 262176 | tf_op jit(solution)/shard_map/ppermute | solution.py:28
  23.9 1.0 collective-permute-start.9
  24.9 6.3 %collective-permute-done.5 = bf16[64,2048]{1,0:T(8,128)(2,1)S(1)} collective-permute-done((bf16[64,2048]{1,0:T(8,128)(2,1)S(1)}, bf16[64,2048]{1,0:T(8,128)(2,1)S(1)}, u32[]{:S(2)}, u32[]{:S(2)}) %collective-permute-start.5) | collective-permute-done | bytes 262176 | tf_op jit(solution)/shard_map/ppermute | solution.py:28
  31.2 1.3 collective-permute-start.7
  32.5 9.0 %collective-permute-done.7 = bf16[64,2048]{1,0:T(8,128)(2,1)S(1)} collective-permute-done((bf16[64,2048]{1,0:T(8,128)(2,1)S(1)}, bf16[64,2048]{1,0:T(8,128)(2,1)S(1)}, u32[]{:S(2)}, u32[]{:S(2)}) %collective-permute-start.7) | collective-permute-done | bytes 262176 | tf_op jit(solution)/shard_map/ppermute | solution.py:28
  41.8 1.8 collective-permute-start.11
  43.6 1.3 collective-permute-start.16
  44.9 1.4 broadcast_select_fusion.1
  46.5 2.7 %collective-permute-start.20 = (bf16[64,2048]{1,0:T(8,128)(2,1)}, bf16[64,2048]{1,0:T(8,128)(2,1)}, u32[]{:S(2)}, u32[]{:S(2)}) collective-permute-start(bf16[64,2048]{1,0:T(8,128)(2,1)} %get-tuple-element.34), channel_id=1, source_target_pairs={{0,8},{2,10},{4,12},{6,14},{8,0},{10,2},{12,4},{14,6},{16,24},{18,... | collective-permute-start | bytes 786440 | tf_op jit(solution)/shard_map/ppermute | solution.py:28
  49.5 1.2 collective-permute-done.10.refs_7_
  50.7 5.6 %collective-permute-done.11.refs_8_ = bf16[64,2048]{1,0:T(8,128)(2,1)S(1)} collective-permute-done((bf16[64,2048]{1,0:T(8,128)(2,1)S(1)}, bf16[64,2048]{1,0:T(8,128)(2,1)S(1)}, u32[]{:S(2)}, u32[]{:S(2)}) %collective-permute-start.11) | collective-permute-done | bytes 262176 | tf_op jit(solution)/shard_map/ppermute | solution.py:28
  56.3 3.6 %shard_map.64 = (bf16[560,512]{1,0:T(8,128)(2,1)}, f32[8,640]{1,0:T(8,128)S(1)}) custom-call(bf16[560,2048]{1,0:T(8,128)(2,1)S(1)} %pad_maximum_fusion.refs_0_, bf16[64,2048]{1,0:T(8,128)(2,1)S(1)} %get-tuple-element.35.refs_1_, bf16[64,2048]{1,0:T(8,128)(2,1)S(1)} %collective-permute-done.3.refs_2_, bf16[64,2048]{1,0:T(8,128)(2,1)S(1)} %broadcast_select_fusion.8.refs_3_, ...), custom_call_target="tpu_custom_call" | custom-call | flops 1174405120 | bytes 8978432 | tf_op jit(solution)/shard_map/pallas_call | solution.py:235
  59.9 1.6 collective-permute-start.12
  63.2 4.4 %collective-permute-done.17.refs_9_ = bf16[128,2048]{1,0:T(8,128)(2,1)} collective-permute-done((bf16[128,2048]{1,0:T(8,128)(2,1)S(1)}, bf16[128,2048]{1,0:T(8,128)(2,1)}, u32[]{:S(2)}, u32[]{:S(2)}) %collective-permute-start.17) | collective-permute-done | bytes 524320 | tf_op jit(solution)/shard_map/ppermute | solution.py:28
  67.6 4.8 %collective-permute-done.13.refs_4_ = f32[8,640]{1,0:T(8,128)S(1)} collective-permute-done((f32[8,640]{1,0:T(8,128)S(1)}, f32[8,640]{1,0:T(8,128)S(1)}, u32[]{:S(2)}, u32[]{:S(2)}) %collective-permute-start.13) | collective-permute-done | bytes 20512 | tf_op jit(solution)/shard_map/ppermute | solution.py:28
  72.4 4.9 %collective-permute-done.18.refs_10_ = bf16[128,2048]{1,0:T(8,128)(2,1)} collective-permute-done((bf16[128,2048]{1,0:T(8,128)(2,1)S(1)}, bf16[128,2048]{1,0:T(8,128)(2,1)}, u32[]{:S(2)}, u32[]{:S(2)}) %collective-permute-start.18) | collective-permute-done | bytes 524320 | tf_op jit(solution)/shard_map/ppermute | solution.py:28
  77.3 5.2 %shard_map.65.refs_1_ = bf16[560,2048]{1,0:T(8,128)(2,1)S(1)} custom-call(s32[2]{0:T(128)S(1)} %pad_add_fusion.refs_0_, bf16[560,512]{1,0:T(8,128)(2,1)} %get-tuple-element.15.refs_1_, bf16[560,512]{1,0:T(8,128)(2,1)} %collective-permute-done.12.refs_2_, f32[8,640]{1,0:T(8,128)S(1)} %get-tuple-element.16.refs_3_, ...), custom_call_target="tpu_custom_call" | custom-call | flops 1174405120 | bytes 8978432 | tf_op jit(solution)/shard_map/pallas_call | solution.py:259
  82.6 1.1 pad_maximum_fusion.2.refs_3_
  84.4 1.3 collective-permute-start.22
  85.7 15.5 %collective-permute-start.27 = (bf16[64,2048]{1,0:T(8,128)(2,1)S(1)}, bf16[64,2048]{1,0:T(8,128)(2,1)S(1)}, u32[]{:S(2)}, u32[]{:S(2)}) collective-permute-start(bf16[64,2048]{1,0:T(8,128)(2,1)S(1)} %copy-done.12), channel_id=1, source_target_pairs={{0,8},{2,10},{4,12},{6,14},{8,0},{10,2},{12,4},{14,6},{16,24},{18,... | collective-permute-start | bytes 786440 | tf_op jit(solution)/shard_map/ppermute | solution.py:28
  101.2 1.0 collective-permute-start.23
  102.2 16.5 %collective-permute-done.27 = bf16[64,2048]{1,0:T(8,128)(2,1)S(1)} collective-permute-done((bf16[64,2048]{1,0:T(8,128)(2,1)S(1)}, bf16[64,2048]{1,0:T(8,128)(2,1)S(1)}, u32[]{:S(2)}, u32[]{:S(2)}) %collective-permute-start.27) | collective-permute-done | bytes 262176 | tf_op jit(solution)/shard_map/ppermute | solution.py:28
  119.5 1.0 collective-permute-start.24
  120.6 1.3 collective-permute-start.29
  121.9 1.1 collective-permute-start.30
  123.0 11.4 %collective-permute-done.24.refs_6_ = bf16[128,2048]{1,0:T(8,128)(2,1)S(1)} collective-permute-done((bf16[128,2048]{1,0:T(8,128)(2,1)S(1)}, bf16[128,2048]{1,0:T(8,128)(2,1)S(1)}, u32[]{:S(2)}, u32[]{:S(2)}) %collective-permute-start.24) | collective-permute-done | bytes 524320 | tf_op jit(solution)/shard_map/ppermute | solution.py:28
  134.4 3.3 %shard_map.66 = (bf16[560,2048]{1,0:T(8,128)(2,1)S(1)}, bf16[560,512]{1,0:T(8,128)(2,1)S(1)}, f32[8,640]{1,0:T(8,128)S(1)}) custom-call(bf16[560,2048]{1,0:T(8,128)(2,1)S(1)} %pad_maximum_fusion.refs_0_, bf16[560,2048]{1,0:T(8,128)(2,1)S(1)} %shard_map.65.refs_1_, bf16[560,2048]{1,0:T(8,128)(2,1)S(1)} %collective-permute-done.19.refs_2_, ...), custom_call_target="tpu_custom_call" | custom-call | flops 1174405120 | bytes 8978432 | tf_op jit(solution)/shard_map/pallas_call | solution.py:235
  137.8 1.4 copy-done.1
  139.1 1.5 collective-permute-start.25
  140.6 4.6 %collective-permute-done.29 = bf16[128,2048]{1,0:T(8,128)(2,1)S(1)} collective-permute-done((bf16[128,2048]{1,0:T(8,128)(2,1)S(1)}, bf16[128,2048]{1,0:T(8,128)(2,1)S(1)}, u32[]{:S(2)}, u32[]{:S(2)}) %collective-permute-start.29) | collective-permute-done | bytes 524320 | tf_op jit(solution)/shard_map/ppermute | solution.py:28
  145.3 1.0 collective-permute-start.31
  146.3 1.5 collective-permute-start.26
  147.9 9.3 %collective-permute-done.31.refs_10_ = bf16[128,2048]{1,0:T(8,128)(2,1)S(1)} collective-permute-done((bf16[128,2048]{1,0:T(8,128)(2,1)S(1)}, bf16[128,2048]{1,0:T(8,128)(2,1)S(1)}, u32[]{:S(2)}, u32[]{:S(2)}) %collective-permute-start.31) | collective-permute-done | bytes 524320 | tf_op jit(solution)/shard_map/ppermute | solution.py:28
  157.2 4.6 %shard_map.67.refs_1_ = bf16[560,2048]{1,0:T(8,128)(2,1)S(1)} custom-call(s32[2]{0:T(128)S(1)} %pad_add_fusion.refs_0_, bf16[560,512]{1,0:T(8,128)(2,1)S(1)} %get-tuple-element.18.refs_1_, bf16[560,512]{1,0:T(8,128)(2,1)S(1)} %collective-permute-done.25.refs_2_, f32[8,640]{1,0:T(8,128)S(1)} %get-tuple-element.19.refs_3_, ...), custom_call_target="tpu_custom_call" | custom-call | flops 1174405120 | bytes 8978432 | tf_op jit(solution)/shard_map/pallas_call | solution.py:259
  161.8 1.1 pad_maximum_fusion.4.refs_3_
  163.7 1.3 collective-permute-start.35
  165.0 16.6 %collective-permute-start.40 = (bf16[64,2048]{1,0:T(8,128)(2,1)S(1)}, bf16[64,2048]{1,0:T(8,128)(2,1)S(1)}, u32[]{:S(2)}, u32[]{:S(2)}) collective-permute-start(bf16[64,2048]{1,0:T(8,128)(2,1)S(1)} %copy-done.11), channel_id=1, source_target_pairs={{0,8},{2,10},{4,12},{6,14},{8,0},{10,2},{12,4},{14,6},{16,24},{18,... | collective-permute-start | bytes 786440 | tf_op jit(solution)/shard_map/ppermute | solution.py:28
  181.6 1.0 collective-permute-start.36
  182.5 16.1 %collective-permute-done.40 = bf16[64,2048]{1,0:T(8,128)(2,1)S(1)} collective-permute-done((bf16[64,2048]{1,0:T(8,128)(2,1)S(1)}, bf16[64,2048]{1,0:T(8,128)(2,1)S(1)}, u32[]{:S(2)}, u32[]{:S(2)}) %collective-permute-start.40) | collective-permute-done | bytes 262176 | tf_op jit(solution)/shard_map/ppermute | solution.py:28
  199.5 1.0 collective-permute-start.37
  200.5 1.5 collective-permute-start.42
  202.0 1.1 collective-permute-start.43
  203.1 11.2 %collective-permute-done.37.refs_6_ = bf16[128,2048]{1,0:T(8,128)(2,1)S(1)} collective-permute-done((bf16[128,2048]{1,0:T(8,128)(2,1)S(1)}, bf16[128,2048]{1,0:T(8,128)(2,1)S(1)}, u32[]{:S(2)}, u32[]{:S(2)}) %collective-permute-start.37) | collective-permute-done | bytes 524320 | tf_op jit(solution)/shard_map/ppermute | solution.py:28
  214.3 3.3 %shard_map.68 = (bf16[560,2048]{1,0:T(8,128)(2,1)S(1)}, bf16[560,512]{1,0:T(8,128)(2,1)S(1)}, f32[8,640]{1,0:T(8,128)S(1)}) custom-call(bf16[560,2048]{1,0:T(8,128)(2,1)S(1)} %copy-done.2, bf16[560,2048]{1,0:T(8,128)(2,1)S(1)} %shard_map.67.refs_1_, bf16[560,2048]{1,0:T(8,128)(2,1)S(1)} %collective-permute-done.32.refs_2_, ...), custom_call_target="tpu_custom_call" | custom-call | flops 1174405120 | bytes 8978432 | tf_op jit(solution)/shard_map/pallas_call | solution.py:235
  217.7 1.6 collective-permute-start.38
  219.3 5.0 %collective-permute-done.42 = bf16[128,2048]{1,0:T(8,128)(2,1)S(1)} collective-permute-done((bf16[128,2048]{1,0:T(8,128)(2,1)S(1)}, bf16[128,2048]{1,0:T(8,128)(2,1)S(1)}, u32[]{:S(2)}, u32[]{:S(2)}) %collective-permute-start.42) | collective-permute-done | bytes 524320 | tf_op jit(solution)/shard_map/ppermute | solution.py:28
  224.3 1.0 collective-permute-start.44
  225.4 1.5 collective-permute-start.39
  227.8 8.1 %collective-permute-done.44.refs_10_ = bf16[128,2048]{1,0:T(8,128)(2,1)} collective-permute-done((bf16[128,2048]{1,0:T(8,128)(2,1)S(1)}, bf16[128,2048]{1,0:T(8,128)(2,1)}, u32[]{:S(2)}, u32[]{:S(2)}) %collective-permute-start.44) | collective-permute-done | bytes 524320 | tf_op jit(solution)/shard_map/ppermute | solution.py:28
  236.7 1.1 copy-done.5
  237.7 1.1 copy-done.7
  238.8 1.0 copy-done.9
  239.8 4.4 %shard_map.69 = (bf16[256,2048]{1,0:T(8,128)(2,1)S(1)}, bf16[256,2048]{1,0:T(8,128)(2,1)S(1)}) custom-call(s32[2]{0:T(128)S(1)} %pad_add_fusion.refs_0_, bf16[560,512]{1,0:T(8,128)(2,1)S(1)} %copy-done.5, bf16[560,512]{1,0:T(8,128)(2,1)S(1)} %copy-done.7, f32[8,640]{1,0:T(8,128)S(1)} %get-tuple-element.22.refs_3_, ...), custom_call_target="tpu_custom_call" | custom-call | flops 1174405120 | bytes 8978432 | tf_op jit(solution)/shard_map/pallas_call | solution.py:259
  244.3 2.6 %collective-permute-done.45 = bf16[256,2048]{1,0:T(8,128)(2,1)S(1)} collective-permute-done((bf16[256,2048]{1,0:T(8,128)(2,1)S(1)}, bf16[256,2048]{1,0:T(8,128)(2,1)S(1)}, u32[]{:S(2)}, u32[]{:S(2)}) %collective-permute-start.45) | collective-permute-done | bytes 1048608 | tf_op jit(solution)/shard_map/ppermute | solution.py:28
  247.0 2.7 %add_convert_fusion = bf16[256,2048]{1,0:T(8,128)(2,1)} fusion(bf16[256,2048]{1,0:T(8,128)(2,1)S(1)} %collective-permute-done.45, bf16[256,2048]{1,0:T(8,128)(2,1)S(1)} %get-tuple-element.23, bf16[560,2048]{1,0:T(8,128)(2,1)} %copy-done.3, s32[]{:T(128)S(6)} %select_n.151), kind=kLoop, calls=%fused_computation.2 | loop fusion | flops 3145728 | bytes 4194308 | tf_op jit(solution)/shard_map/convert_element_type | solution.py:275
  (101 shorter events, 12.2 us)
Async XLA Ops:
  0.0 0.8 copy-start
  0.0 5.3 %copy-start.10 = (bf16[256,2048]{1,0:T(8,128)(2,1)S(1)}, bf16[256,2048]{1,0:T(8,128)(2,1)}, u32[]{:S(2)}) copy-start(bf16[256,2048]{1,0:T(8,128)(2,1)} %param.6) | copy-start | bytes 3145732
  0.8 9.3 %copy-start.13 = (f32[3,1024]{1,0:T(4,128)S(1)}, f32[3,1024]{1,0:T(4,128)}, u32[]{:S(2)}) copy-start(f32[3,1024]{1,0:T(4,128)} %param.9) | copy-start | bytes 36868
  3.0 15.1 %collective-permute-start.3 = (bf16[64,2048]{1,0:T(8,128)(2,1)S(1)}, bf16[64,2048]{1,0:T(8,128)(2,1)S(1)}, u32[]{:S(2)}, u32[]{:S(2)}) collective-permute-start(bf16[64,2048]{1,0:T(8,128)(2,1)S(1)} %get-tuple-element.35.refs_1_), channel_id=1, source_target_pairs={{0,8},{2,10},{4,12},{6,14},{8,0},{10,2},{12,4},{14,6},{16,24},{18,... | collective-permute-start | bytes 786440 | tf_op jit(solution)/shard_map/ppermute | solution.py:28
  4.6 14.2 %collective-permute-start.4 = (bf16[64,2048]{1,0:T(8,128)(2,1)S(1)}, bf16[64,2048]{1,0:T(8,128)(2,1)S(1)}, u32[]{:S(2)}, u32[]{:S(2)}) collective-permute-start(bf16[64,2048]{1,0:T(8,128)(2,1)S(1)} %get-tuple-element.35.refs_1_), channel_id=1, source_target_pairs={{8,16},{10,18},{12,20},{14,22},{16,8},{18,10},{20,12},{22,14},{9,1... | collective-permute-start | bytes 786440 | tf_op jit(solution)/shard_map/ppermute | solution.py:28
  5.3 38.4 %collective-permute-start.2 = (bf16[256,2048]{1,0:T(8,128)(2,1)S(1)}, bf16[256,2048]{1,0:T(8,128)(2,1)}, u32[]{:S(2)}, u32[]{:S(2)}) collective-permute-start(bf16[256,2048]{1,0:T(8,128)(2,1)S(1)} %copy-done.10), channel_id=1, source_target_pairs={{0,2},{2,0},{4,6},{6,4},{8,10},{10,8},{12,14},{14,12},{16,18},{18,... | collective-permute-start | bytes 3145736 | tf_op jit(solution)/shard_map/ppermute | solution.py:28
  5.4 7.0 %collective-permute-start = (bf16[48,2048]{1,0:T(8,128)(2,1)S(1)}, bf16[48,2048]{1,0:T(8,128)(2,1)S(1)}, u32[]{:S(2)}, u32[]{:S(2)}) collective-permute-start(bf16[48,2048]{1,0:T(8,128)(2,1)S(1)} %slice.36), channel_id=1, source_target_pairs={{2,4},{6,8},{10,12},{14,16},{18,20},{22,24},{26,28},{3,5},{7,9},{1... | collective-permute-start | bytes 589832 | tf_op jit(solution)/shard_map/ppermute | solution.py:28
  6.7 5.7 %collective-permute-start.1 = (bf16[48,2048]{1,0:T(8,128)(2,1)S(1)}, bf16[48,2048]{1,0:T(8,128)(2,1)S(1)}, u32[]{:S(2)}, u32[]{:S(2)}) collective-permute-start(bf16[48,2048]{1,0:T(8,128)(2,1)S(1)} %slice.36), channel_id=1, source_target_pairs={{2,6},{6,10},{10,14},{14,18},{18,22},{22,26},{26,30},{3,7},{7,11},... | collective-permute-start | bytes 589832 | tf_op jit(solution)/shard_map/ppermute | solution.py:28
  12.4 34.1 %collective-permute-start.8 = (bf16[64,2048]{1,0:T(8,128)(2,1)S(1)}, bf16[64,2048]{1,0:T(8,128)(2,1)S(1)}, u32[]{:S(2)}, u32[]{:S(2)}) collective-permute-start(bf16[64,2048]{1,0:T(8,128)(2,1)S(1)} %get-tuple-element.35.refs_1_), channel_id=1, source_target_pairs={{0,4},{2,6},{4,0},{6,2},{8,12},{10,14},{12,8},{14,10},{16,20},{18,... | collective-permute-start | bytes 786440 | tf_op jit(solution)/shard_map/ppermute | solution.py:28
  12.4 10.8 %collective-permute-start.14 = (bf16[64,2048]{1,0:T(8,128)(2,1)S(1)}, bf16[64,2048]{1,0:T(8,128)(2,1)S(1)}, u32[]{:S(2)}, u32[]{:S(2)}) collective-permute-start(bf16[64,2048]{1,0:T(8,128)(2,1)S(1)} %get-tuple-element.31), channel_id=1, source_target_pairs={{0,8},{2,10},{4,12},{6,14},{8,0},{10,2},{12,4},{14,6},{16,24},{18,... | collective-permute-start | bytes 786440 | tf_op jit(solution)/shard_map/ppermute | solution.py:28
  18.2 5.7 %collective-permute-start.6 = (bf16[64,2048]{1,0:T(8,128)(2,1)S(1)}, bf16[64,2048]{1,0:T(8,128)(2,1)S(1)}, u32[]{:S(2)}, u32[]{:S(2)}) collective-permute-start(bf16[64,2048]{1,0:T(8,128)(2,1)S(1)} %collective-permute-done.3.refs_2_), channel_id=1, source_target_pairs={{8,16},{10,18},{12,20},{14,22},{16,8},{18,10},{20,12},{22,14},{9,1... | collective-permute-start | bytes 786440 | tf_op jit(solution)/shard_map/ppermute | solution.py:28
  18.9 12.3 %collective-permute-start.5 = (bf16[64,2048]{1,0:T(8,128)(2,1)S(1)}, bf16[64,2048]{1,0:T(8,128)(2,1)S(1)}, u32[]{:S(2)}, u32[]{:S(2)}) collective-permute-start(bf16[64,2048]{1,0:T(8,128)(2,1)S(1)} %collective-permute-done.4), channel_id=1, source_target_pairs={{8,0},{10,2},{12,4},{14,6},{16,24},{18,26},{20,28},{22,30},{9,1},{... | collective-permute-start | bytes 786440 | tf_op jit(solution)/shard_map/ppermute | solution.py:28
  23.2 18.6 %collective-permute-start.15 = (bf16[128,2048]{1,0:T(8,128)(2,1)S(1)}, bf16[128,2048]{1,0:T(8,128)(2,1)S(1)}, u32[]{:S(2)}, u32[]{:S(2)}) collective-permute-start(bf16[128,2048]{1,0:T(8,128)(2,1)S(1)} %pad_maximum_fusion.1.refs_7_), channel_id=1, source_target_pairs={{8,16},{10,18},{12,20},{14,22},{16,8},{18,10},{20,12},{22,14},{9,1... | collective-permute-start | bytes 1572872 | tf_op jit(solution)/shard_map/ppermute | solution.py:28
  23.9 25.3 %collective-permute-start.9 = (bf16[64,2048]{1,0:T(8,128)(2,1)S(1)}, bf16[64,2048]{1,0:T(8,128)(2,1)S(1)}, u32[]{:S(2)}, u32[]{:S(2)}) collective-permute-start(bf16[64,2048]{1,0:T(8,128)(2,1)S(1)} %collective-permute-done.3.refs_2_), channel_id=1, source_target_pairs={{0,4},{2,6},{4,0},{6,2},{8,12},{10,14},{12,8},{14,10},{16,20},{18,... | collective-permute-start | bytes 786440 | tf_op jit(solution)/shard_map/ppermute | solution.py:28
  31.2 10.3 %collective-permute-start.7 = (bf16[64,2048]{1,0:T(8,128)(2,1)S(1)}, bf16[64,2048]{1,0:T(8,128)(2,1)S(1)}, u32[]{:S(2)}, u32[]{:S(2)}) collective-permute-start(bf16[64,2048]{1,0:T(8,128)(2,1)S(1)} %collective-permute-done.6), channel_id=1, source_target_pairs={{8,0},{10,2},{12,4},{14,6},{16,24},{18,26},{20,28},{22,30},{9,1},{... | collective-permute-start | bytes 786440 | tf_op jit(solution)/shard_map/ppermute | solution.py:28
  41.5 9.2 %collective-permute-start.10 = (bf16[64,2048]{1,0:T(8,128)(2,1)S(1)}, bf16[64,2048]{1,0:T(8,128)(2,1)S(1)}, u32[]{:S(2)}, u32[]{:S(2)}) collective-permute-start(bf16[64,2048]{1,0:T(8,128)(2,1)S(1)} %broadcast_select_fusion.8.refs_3_), channel_id=1, source_target_pairs={{0,4},{2,6},{4,0},{6,2},{8,12},{10,14},{12,8},{14,10},{16,20},{18,... | collective-permute-start | bytes 786440 | tf_op jit(solution)/shard_map/ppermute | solution.py:28
  41.8 14.5 %collective-permute-start.11 = (bf16[64,2048]{1,0:T(8,128)(2,1)S(1)}, bf16[64,2048]{1,0:T(8,128)(2,1)S(1)}, u32[]{:S(2)}, u32[]{:S(2)}) collective-permute-start(bf16[64,2048]{1,0:T(8,128)(2,1)S(1)} %broadcast_select_fusion.7.refs_4_), channel_id=1, source_target_pairs={{0,4},{2,6},{4,0},{6,2},{8,12},{10,14},{12,8},{14,10},{16,20},{18,... | collective-permute-start | bytes 786440 | tf_op jit(solution)/shard_map/ppermute | solution.py:28
  43.6 17.8 %collective-permute-start.16 = (bf16[128,2048]{1,0:T(8,128)(2,1)S(1)}, bf16[128,2048]{1,0:T(8,128)(2,1)S(1)}, u32[]{:S(2)}, u32[]{:S(2)}) collective-permute-start(bf16[128,2048]{1,0:T(8,128)(2,1)S(1)} %collective-permute-done.15), channel_id=1, source_target_pairs={{8,0},{10,2},{12,4},{14,6},{16,24},{18,26},{20,28},{22,30},{9,1},{... | collective-permute-start | bytes 1572872 | tf_op jit(solution)/shard_map/ppermute | solution.py:28
  46.5 36.2 %collective-permute-start.20 = (bf16[64,2048]{1,0:T(8,128)(2,1)}, bf16[64,2048]{1,0:T(8,128)(2,1)}, u32[]{:S(2)}, u32[]{:S(2)}) collective-permute-start(bf16[64,2048]{1,0:T(8,128)(2,1)} %get-tuple-element.34), channel_id=1, source_target_pairs={{0,8},{2,10},{4,12},{6,14},{8,0},{10,2},{12,4},{14,6},{16,24},{18,... | collective-permute-start | bytes 786440 | tf_op jit(solution)/shard_map/ppermute | solution.py:28
  49.2 18.4 %collective-permute-start.17 = (bf16[128,2048]{1,0:T(8,128)(2,1)S(1)}, bf16[128,2048]{1,0:T(8,128)(2,1)}, u32[]{:S(2)}, u32[]{:S(2)}) collective-permute-start(bf16[128,2048]{1,0:T(8,128)(2,1)S(1)} %pad_maximum_fusion.1.refs_7_), channel_id=1, source_target_pairs={{0,4},{2,6},{4,0},{6,2},{8,12},{10,14},{12,8},{14,10},{16,20},{18,... | collective-permute-start | bytes 1572872 | tf_op jit(solution)/shard_map/ppermute | solution.py:28
  59.9 12.5 %collective-permute-start.12 = (bf16[560,512]{1,0:T(8,128)(2,1)}, bf16[560,512]{1,0:T(8,128)(2,1)}, u32[]{:S(2)}, u32[]{:S(2)}) collective-permute-start(bf16[560,512]{1,0:T(8,128)(2,1)} %get-tuple-element.15.refs_1_), channel_id=1, source_target_pairs={{0,1},{1,0},{2,3},{3,2},{4,5},{5,4},{6,7},{7,6},{8,9},{9,8},{10,11... | collective-permute-start | bytes 1720328 | tf_op jit(solution)/shard_map/ppermute | solution.py:28
  61.5 15.8 %collective-permute-start.18 = (bf16[128,2048]{1,0:T(8,128)(2,1)S(1)}, bf16[128,2048]{1,0:T(8,128)(2,1)}, u32[]{:S(2)}, u32[]{:S(2)}) collective-permute-start(bf16[128,2048]{1,0:T(8,128)(2,1)S(1)} %broadcast_select_fusion.6.refs_8_), channel_id=1, source_target_pairs={{0,4},{2,6},{4,0},{6,2},{8,12},{10,14},{12,8},{14,10},{16,20},{18,... | collective-permute-start | bytes 1572872 | tf_op jit(solution)/shard_map/ppermute | solution.py:28
  62.5 9.9 %collective-permute-start.13 = (f32[8,640]{1,0:T(8,128)S(1)}, f32[8,640]{1,0:T(8,128)S(1)}, u32[]{:S(2)}, u32[]{:S(2)}) collective-permute-start(f32[8,640]{1,0:T(8,128)S(1)} %get-tuple-element.16.refs_3_), channel_id=1, source_target_pairs={{0,1},{1,0},{2,3},{3,2},{4,5},{5,4},{6,7},{7,6},{8,9},{9,8},{10,11... | collective-permute-start | bytes 61448 | tf_op jit(solution)/shard_map/ppermute | solution.py:28
  77.3 8.4 %copy-start.12 = (bf16[64,2048]{1,0:T(8,128)(2,1)S(1)}, bf16[64,2048]{1,0:T(8,128)(2,1)}, u32[]{:S(2)}) copy-start(bf16[64,2048]{1,0:T(8,128)(2,1)} %get-tuple-element.32) | copy-start | bytes 786436
  82.5 51.9 %collective-permute-start.19 = (bf16[560,2048]{1,0:T(8,128)(2,1)S(1)}, bf16[560,2048]{1,0:T(8,128)(2,1)S(1)}, u32[]{:S(2)}, u32[]{:S(2)}) collective-permute-start(bf16[560,2048]{1,0:T(8,128)(2,1)S(1)} %shard_map.65.refs_1_), channel_id=1, source_target_pairs={{0,2},{2,0},{4,6},{6,4},{8,10},{10,8},{12,14},{14,12},{16,18},{18,... | collective-permute-start | bytes 6881288 | tf_op jit(solution)/shard_map/ppermute | solution.py:28
  83.7 0.7 collective-permute-start.21
  84.4 35.1 %collective-permute-start.22 = (bf16[128,2048]{1,0:T(8,128)(2,1)S(1)}, bf16[128,2048]{1,0:T(8,128)(2,1)S(1)}, u32[]{:S(2)}, u32[]{:S(2)}) collective-permute-start(bf16[128,2048]{1,0:T(8,128)(2,1)S(1)} %collective-permute-done.21), channel_id=1, source_target_pairs={{8,0},{10,2},{12,4},{14,6},{16,24},{18,26},{20,28},{22,30},{9,1},{... | collective-permute-start | bytes 1572872 | tf_op jit(solution)/shard_map/ppermute | solution.py:28
  85.7 33.0 %collective-permute-start.27 = (bf16[64,2048]{1,0:T(8,128)(2,1)S(1)}, bf16[64,2048]{1,0:T(8,128)(2,1)S(1)}, u32[]{:S(2)}, u32[]{:S(2)}) collective-permute-start(bf16[64,2048]{1,0:T(8,128)(2,1)S(1)} %copy-done.12), channel_id=1, source_target_pairs={{0,8},{2,10},{4,12},{6,14},{8,0},{10,2},{12,4},{14,6},{16,24},{18,... | collective-permute-start | bytes 786440 | tf_op jit(solution)/shard_map/ppermute | solution.py:28
  101.2 21.8 %collective-permute-start.23 = (bf16[128,2048]{1,0:T(8,128)(2,1)S(1)}, bf16[128,2048]{1,0:T(8,128)(2,1)S(1)}, u32[]{:S(2)}, u32[]{:S(2)}) collective-permute-start(bf16[128,2048]{1,0:T(8,128)(2,1)S(1)} %pad_maximum_fusion.2.refs_3_), channel_id=1, source_target_pairs={{0,4},{2,6},{4,0},{6,2},{8,12},{10,14},{12,8},{14,10},{16,20},{18,... | collective-permute-start | bytes 1572872 | tf_op jit(solution)/shard_map/ppermute | solution.py:28
  118.8 1.8 collective-permute-start.28
  119.5 14.9 %collective-permute-start.24 = (bf16[128,2048]{1,0:T(8,128)(2,1)S(1)}, bf16[128,2048]{1,0:T(8,128)(2,1)S(1)}, u32[]{:S(2)}, u32[]{:S(2)}) collective-permute-start(bf16[128,2048]{1,0:T(8,128)(2,1)S(1)} %broadcast_select_fusion.5.refs_4_), channel_id=1, source_target_pairs={{0,4},{2,6},{4,0},{6,2},{8,12},{10,14},{12,8},{14,10},{16,20},{18,... | collective-permute-start | bytes 1572872 | tf_op jit(solution)/shard_map/ppermute | solution.py:28
  120.6 24.6 %collective-permute-start.29 = (bf16[128,2048]{1,0:T(8,128)(2,1)S(1)}, bf16[128,2048]{1,0:T(8,128)(2,1)S(1)}, u32[]{:S(2)}, u32[]{:S(2)}) collective-permute-start(bf16[128,2048]{1,0:T(8,128)(2,1)S(1)} %collective-permute-done.28), channel_id=1, source_target_pairs={{8,0},{10,2},{12,4},{14,6},{16,24},{18,26},{20,28},{22,30},{9,1},{... | collective-permute-start | bytes 1572872 | tf_op jit(solution)/shard_map/ppermute | solution.py:28
  121.9 26.0 %collective-permute-start.30 = (bf16[128,2048]{1,0:T(8,128)(2,1)S(1)}, bf16[128,2048]{1,0:T(8,128)(2,1)}, u32[]{:S(2)}, u32[]{:S(2)}) collective-permute-start(bf16[128,2048]{1,0:T(8,128)(2,1)S(1)} %pad_maximum_fusion.3.refs_7_), channel_id=1, source_target_pairs={{0,4},{2,6},{4,0},{6,2},{8,12},{10,14},{12,8},{14,10},{16,20},{18,... | collective-permute-start | bytes 1572872 | tf_op jit(solution)/shard_map/ppermute | solution.py:28
  137.8 1.4 copy-start.1
  139.1 18.0 %collective-permute-start.25 = (bf16[560,512]{1,0:T(8,128)(2,1)S(1)}, bf16[560,512]{1,0:T(8,128)(2,1)S(1)}, u32[]{:S(2)}, u32[]{:S(2)}) collective-permute-start(bf16[560,512]{1,0:T(8,128)(2,1)S(1)} %get-tuple-element.18.refs_1_), channel_id=1, source_target_pairs={{0,1},{1,0},{2,3},{3,2},{4,5},{5,4},{6,7},{7,6},{8,9},{9,8},{10,11... | collective-permute-start | bytes 1720328 | tf_op jit(solution)/shard_map/ppermute | solution.py:28
  145.3 11.9 %collective-permute-start.31 = (bf16[128,2048]{1,0:T(8,128)(2,1)S(1)}, bf16[128,2048]{1,0:T(8,128)(2,1)S(1)}, u32[]{:S(2)}, u32[]{:S(2)}) collective-permute-start(bf16[128,2048]{1,0:T(8,128)(2,1)S(1)} %broadcast_select_fusion.4.refs_8_), channel_id=1, source_target_pairs={{0,4},{2,6},{4,0},{6,2},{8,12},{10,14},{12,8},{14,10},{16,20},{18,... | collective-permute-start | bytes 1572872 | tf_op jit(solution)/shard_map/ppermute | solution.py:28
  146.3 15.6 %collective-permute-start.33 = (bf16[64,2048]{1,0:T(8,128)(2,1)}, bf16[64,2048]{1,0:T(8,128)(2,1)S(1)}, u32[]{:S(2)}, u32[]{:S(2)}) collective-permute-start(bf16[64,2048]{1,0:T(8,128)(2,1)} %get-tuple-element.33), channel_id=1, source_target_pairs={{0,8},{2,10},{4,12},{6,14},{8,0},{10,2},{12,4},{14,6},{16,24},{18,... | collective-permute-start | bytes 786440 | tf_op jit(solution)/shard_map/ppermute | solution.py:28
  146.3 10.9 %collective-permute-start.26 = (f32[8,640]{1,0:T(8,128)S(1)}, f32[8,640]{1,0:T(8,128)S(1)}, u32[]{:S(2)}, u32[]{:S(2)}) collective-permute-start(f32[8,640]{1,0:T(8,128)S(1)} %get-tuple-element.19.refs_3_), channel_id=1, source_target_pairs={{0,1},{1,0},{2,3},{3,2},{4,5},{5,4},{6,7},{7,6},{8,9},{9,8},{10,11... | collective-permute-start | bytes 61448 | tf_op jit(solution)/shard_map/ppermute | solution.py:28
  157.2 7.8 %copy-start.11 = (bf16[64,2048]{1,0:T(8,128)(2,1)S(1)}, bf16[64,2048]{1,0:T(8,128)(2,1)}, u32[]{:S(2)}) copy-start(bf16[64,2048]{1,0:T(8,128)(2,1)} %get-tuple-element.30) | copy-start | bytes 786436
  161.7 52.6 %copy-start.2 = (bf16[560,2048]{1,0:T(8,128)(2,1)S(1)}, bf16[560,2048]{1,0:T(8,128)(2,1)}, u32[]{:S(2)}) copy-start(bf16[560,2048]{1,0:T(8,128)(2,1)} %copy-done.1) | copy-start | bytes 6881284
  161.8 52.6 %collective-permute-start.32 = (bf16[560,2048]{1,0:T(8,128)(2,1)S(1)}, bf16[560,2048]{1,0:T(8,128)(2,1)S(1)}, u32[]{:S(2)}, u32[]{:S(2)}) collective-permute-start(bf16[560,2048]{1,0:T(8,128)(2,1)S(1)} %shard_map.67.refs_1_), channel_id=1, source_target_pairs={{0,2},{2,0},{4,6},{6,4},{8,10},{10,8},{12,14},{14,12},{16,18},{18,... | collective-permute-start | bytes 6881288 | tf_op jit(solution)/shard_map/ppermute | solution.py:28
  163.0 0.7 collective-permute-start.34
  163.7 35.7 %collective-permute-start.35 = (bf16[128,2048]{1,0:T(8,128)(2,1)S(1)}, bf16[128,2048]{1,0:T(8,128)(2,1)S(1)}, u32[]{:S(2)}, u32[]{:S(2)}) collective-permute-start(bf16[128,2048]{1,0:T(8,128)(2,1)S(1)} %collective-permute-done.34), channel_id=1, source_target_pairs={{8,0},{10,2},{12,4},{14,6},{16,24},{18,26},{20,28},{22,30},{9,1},{... | collective-permute-start | bytes 1572872 | tf_op jit(solution)/shard_map/ppermute | solution.py:28
  165.0 33.6 %collective-permute-start.40 = (bf16[64,2048]{1,0:T(8,128)(2,1)S(1)}, bf16[64,2048]{1,0:T(8,128)(2,1)S(1)}, u32[]{:S(2)}, u32[]{:S(2)}) collective-permute-start(bf16[64,2048]{1,0:T(8,128)(2,1)S(1)} %copy-done.11), channel_id=1, source_target_pairs={{0,8},{2,10},{4,12},{6,14},{8,0},{10,2},{12,4},{14,6},{16,24},{18,... | collective-permute-start | bytes 786440 | tf_op jit(solution)/shard_map/ppermute | solution.py:28
  181.6 21.5 %collective-permute-start.36 = (bf16[128,2048]{1,0:T(8,128)(2,1)S(1)}, bf16[128,2048]{1,0:T(8,128)(2,1)S(1)}, u32[]{:S(2)}, u32[]{:S(2)}) collective-permute-start(bf16[128,2048]{1,0:T(8,128)(2,1)S(1)} %pad_maximum_fusion.4.refs_3_), channel_id=1, source_target_pairs={{0,4},{2,6},{4,0},{6,2},{8,12},{10,14},{12,8},{14,10},{16,20},{18,... | collective-permute-start | bytes 1572872 | tf_op jit(solution)/shard_map/ppermute | solution.py:28
  198.7 1.8 collective-permute-start.41
  199.5 14.9 %collective-permute-start.37 = (bf16[128,2048]{1,0:T(8,128)(2,1)S(1)}, bf16[128,2048]{1,0:T(8,128)(2,1)S(1)}, u32[]{:S(2)}, u32[]{:S(2)}) collective-permute-start(bf16[128,2048]{1,0:T(8,128)(2,1)S(1)} %broadcast_select_fusion.3.refs_4_), channel_id=1, source_target_pairs={{0,4},{2,6},{4,0},{6,2},{8,12},{10,14},{12,8},{14,10},{16,20},{18,... | collective-permute-start | bytes 1572872 | tf_op jit(solution)/shard_map/ppermute | solution.py:28
  200.5 23.8 %collective-permute-start.42 = (bf16[128,2048]{1,0:T(8,128)(2,1)S(1)}, bf16[128,2048]{1,0:T(8,128)(2,1)S(1)}, u32[]{:S(2)}, u32[]{:S(2)}) collective-permute-start(bf16[128,2048]{1,0:T(8,128)(2,1)S(1)} %collective-permute-done.41), channel_id=1, source_target_pairs={{8,0},{10,2},{12,4},{14,6},{16,24},{18,26},{20,28},{22,30},{9,1},{... | collective-permute-start | bytes 1572872 | tf_op jit(solution)/shard_map/ppermute | solution.py:28
  202.0 25.0 %collective-permute-start.43 = (bf16[128,2048]{1,0:T(8,128)(2,1)S(1)}, bf16[128,2048]{1,0:T(8,128)(2,1)S(1)}, u32[]{:S(2)}, u32[]{:S(2)}) collective-permute-start(bf16[128,2048]{1,0:T(8,128)(2,1)S(1)} %pad_maximum_fusion.5.refs_7_), channel_id=1, source_target_pairs={{0,4},{2,6},{4,0},{6,2},{8,12},{10,14},{12,8},{14,10},{16,20},{18,... | collective-permute-start | bytes 1572872 | tf_op jit(solution)/shard_map/ppermute | solution.py:28
  217.7 6.6 %copy-start.3 = (bf16[560,2048]{1,0:T(8,128)(2,1)}, bf16[560,2048]{1,0:T(8,128)(2,1)S(1)}, u32[]{:S(2)}) copy-start(bf16[560,2048]{1,0:T(8,128)(2,1)S(1)} %get-tuple-element.20) | copy-start | bytes 6881284
  217.7 18.1 %copy-start.4 = (bf16[560,512]{1,0:T(8,128)(2,1)}, bf16[560,512]{1,0:T(8,128)(2,1)S(1)}, u32[]{:S(2)}) copy-start(bf16[560,512]{1,0:T(8,128)(2,1)S(1)} %get-tuple-element.21.refs_1_) | copy-start | bytes 1720324
  217.7 18.1 %collective-permute-start.38 = (bf16[560,512]{1,0:T(8,128)(2,1)S(1)}, bf16[560,512]{1,0:T(8,128)(2,1)S(1)}, u32[]{:S(2)}, u32[]{:S(2)}) collective-permute-start(bf16[560,512]{1,0:T(8,128)(2,1)S(1)} %get-tuple-element.21.refs_1_), channel_id=1, source_target_pairs={{0,1},{1,0},{2,3},{3,2},{4,5},{5,4},{6,7},{7,6},{8,9},{9,8},{10,11... | collective-permute-start | bytes 1720328 | tf_op jit(solution)/shard_map/ppermute | solution.py:28
  224.3 11.5 %collective-permute-start.44 = (bf16[128,2048]{1,0:T(8,128)(2,1)S(1)}, bf16[128,2048]{1,0:T(8,128)(2,1)}, u32[]{:S(2)}, u32[]{:S(2)}) collective-permute-start(bf16[128,2048]{1,0:T(8,128)(2,1)S(1)} %broadcast_select_fusion.2.refs_8_), channel_id=1, source_target_pairs={{0,4},{2,6},{4,0},{6,2},{8,12},{10,14},{12,8},{14,10},{16,20},{18,... | collective-permute-start | bytes 1572872 | tf_op jit(solution)/shard_map/ppermute | solution.py:28
  225.4 10.5 %collective-permute-start.39 = (f32[8,640]{1,0:T(8,128)S(1)}, f32[8,640]{1,0:T(8,128)S(1)}, u32[]{:S(2)}, u32[]{:S(2)}) collective-permute-start(f32[8,640]{1,0:T(8,128)S(1)} %get-tuple-element.22.refs_3_), channel_id=1, source_target_pairs={{0,1},{1,0},{2,3},{3,2},{4,5},{5,4},{6,7},{7,6},{8,9},{9,8},{10,11... | collective-permute-start | bytes 61448 | tf_op jit(solution)/shard_map/ppermute | solution.py:28
  226.9 0.8 copy-start.8
  235.8 0.8 copy-start.6
  236.7 1.1 copy-start.5
  237.7 1.1 copy-start.7
  238.8 1.0 copy-start.9
  244.3 2.7 %collective-permute-start.45 = (bf16[256,2048]{1,0:T(8,128)(2,1)S(1)}, bf16[256,2048]{1,0:T(8,128)(2,1)S(1)}, u32[]{:S(2)}, u32[]{:S(2)}) collective-permute-start(bf16[256,2048]{1,0:T(8,128)(2,1)S(1)} %get-tuple-element.24), channel_id=1, source_target_pairs={{0,2},{2,0},{4,6},{6,4},{8,10},{10,8},{12,14},{14,12},{16,18},{18,... | collective-permute-start | bytes 3145736 | tf_op jit(solution)/shard_map/ppermute | solution.py:28
where the time goes:
time: 252 us; the launch traced here: 250 us
  waiting for transfers between devices  125 us (50%)
  starting transfers between devices  78.6 us (31%)
  Pallas kernels  24.5 us (10%)
  local copies, waits for them, and re-layouts  10.9 us (4%)
  other arithmetic  9.76 us (4%)
    ppermute x46, waiting for transfers between devices, move(): lax.ppermute(value, axis, [(s, t) for s, t in pairs if t is not None])  125 us
    ppermute x46, starting transfers between devices, move(): lax.ppermute(value, axis, [(s, t) for s, t in pairs if t is not None])  78.6 us
    pallas_call x3, Pallas kernels, body(): pl.pallas_call(functools.partial(out_kernel, last, pieces, shard, feature...  14.2 us
    pallas_call x3, Pallas kernels, body(): pl.pallas_call(functools.partial(in_kernel, first, pieces, shard), out_sh...  10.3 us
    unnamed x28, local copies, waits for them, and re-layouts  7.03 us
  transfers between devices with their start and end apart: 46, of which 18 were waited for; matrix products, arithmetic and copies ran while one was open for 4% of the time, Pallas kernels for 8%

commit v1 on v0

v1 whole, which is shorter than its diff:
```python
import functools
import math

import jax
import jax.numpy as jnp
import numpy as np
from jax import lax
from jax.experimental import pallas as pl
from jax.experimental.pallas import tpu as pltpu
from jax.sharding import PartitionSpec as P


epsilon = 1e-06
window = 16
group_count = 4
lanes = 128
row_tile = 16


VMEM = pl.BlockSpec(memory_space=pltpu.VMEM)
SMEM = pl.BlockSpec(memory_space=pltpu.SMEM)
ANY = pl.BlockSpec(memory_space=pl.ANY)
HBM = pl.BlockSpec(memory_space=pltpu.HBM)


def move(value, axis, target):
    pairs = [(s, target(s)) for s in range(lax.axis_size(axis))]
    return lax.ppermute(value, axis, [(s, t) for s, t in pairs if t is not None])


def levels(nz):
    return [1 << b for b in range(nz.bit_length() - 1)]


def next_hop(z, m, step):
    at = z % (2 * m)
    if step == 0:
        return z + 1 if at == m - 1 else z - 1 if at == m else None
    return z - 1 if at == m - step else z + 1 if at == m - 1 + step else None


def order_table(nz):
    table = [[z] for z in range(nz)]
    for m in levels(nz):
        edge = lambda z: z - z % (2 * m) + (m if z % (2 * m) < m else m - 1)
        table = [table[z] + table[edge(z)] for z in range(nz)]
    return table


def across(value):
    return move(value, "sp", lambda s: s ^ 2)


def level(value, m):
    at = lax.axis_index("sp") // 4 % (2 * m)
    steps = jnp.where(at < m, m - 1 - at, at - m)

    def hop(v, step):
        def target(s):
            z = next_hop(s // 4, m, step)
            return None if z is None else 4 * z + s % 4

        return move(v, "sp", target)

    far = got = hop(value, 0)
    for t in range(1, m):
        got = hop(got, t)
        far = jnp.where(steps == t, got, far)
    return far


def lower(stack, nz):
    arrived, near = [], stack
    for m in levels(nz)[:-1]:
        far = level(near, m)
        arrived.append((far, list(range(m, 2 * m))))
        near = jnp.concatenate([near, far], 1)
    return arrived


def gather(own, opposite, arrived, crossed, nz, split):
    half = nz // 2
    pick = lambda e: e[0] if e[2] is None else e[0][e[2]]
    join = lambda parts: (jnp.concatenate([pick(e) for e in parts], 0), sum([e[1] for e in parts], []), None)
    near = [(own, [0], None)] + arrived
    beyond = [opposite] + crossed
    if not split:
        near = [join(near)]
    far = [(level(pick(e), half), [q + half for q in e[1]], None) for e in near]
    return near + far + beyond + [(across(v), [q + nz for q in at], None) for v, at, _ in far]


def load_weight(pieces, refs, shard, w, sems):
    copies = []
    for (places, index), ref in zip(pieces, refs):
        for k, place in enumerate(places):
            rows = pl.ds(k * shard, shard)
            copies.append(
                pltpu.make_async_copy(
                    ref.at[rows] if index is None else ref.at[index, rows],
                    w.at[pl.ds(place * shard, shard)],
                    sems.at[len(copies)],
                )
            )
    for copy in copies:
        copy.start()
    return copies


def in_kernel(first, pieces, shard, *refs):
    refs = list(refs)
    state = refs.pop(0)
    deltas = [] if first else [refs.pop(0), refs.pop(0)]
    arrays = [refs.pop(0) for _ in pieces]
    kept = None if first else refs.pop(0)
    out, squares, w, sq, sems = refs[:5]
    fresh = state if first else refs[5]
    copies = load_weight(pieces, arrays, shard, w, sems)
    rows = state.shape[0]
    tile = 5 * row_tile if rows % (5 * row_tile) == 0 else row_tile

    @pl.loop(0, rows // tile)
    def _(i):
        at = pl.ds(pl.multiple_of(i * tile, row_tile), tile)
        value = state[at, :].astype(jnp.float32)
        if not first:
            value = value + (deltas[0][at, :].astype(jnp.float32) + deltas[1][at, :].astype(jnp.float32))
            rounded = value.astype(jnp.bfloat16)
            fresh[at, :] = rounded
            value = rounded.astype(jnp.float32)
        total = jnp.sum(value * value, axis=1, keepdims=True)
        sq[at, :] = jnp.broadcast_to(total, (tile, lanes))

    if not first:
        keep = pltpu.make_async_copy(fresh, kept, refs[6])
        keep.start()
    if rows < sq.shape[0]:
        sq[rows:, :] = jnp.zeros((sq.shape[0] - rows, lanes), jnp.float32)
    squares[...] = sq[...].T[: squares.shape[0], :]
    for copy in copies:
        copy.wait()
    step = min(256, w.shape[0])
    for n in range(0, w.shape[0], step):
        out[:, n : n + step] = lax.dot_general(
            fresh[...], w[n : n + step, :], (((1,), (1,)), ((), ())), preferred_element_type=jnp.float32
        ).astype(jnp.bfloat16)
    if not first:
        keep.wait()


def pool(place, own, other, sq_own, sq_other, group, scale, mixed, features, halo):
    rows, width = own.shape
    inv = lax.rsqrt((sq_own[...] + sq_other[...]) / features + epsilon)
    inv = jnp.broadcast_to(inv[:1, :], (lanes, inv.shape[1])).T[:rows, :]
    position = place[0] - halo + lax.broadcasted_iota(jnp.int32, (rows, lanes), 0)
    inv = jnp.where(position >= 0, inv, 0.0)
    for n in range(0, width, lanes):
        at = slice(n, n + lanes)
        value = (own[:, at].astype(jnp.float32) + other[:, at].astype(jnp.float32)) * inv
        value = value.astype(jnp.bfloat16).astype(jnp.float32)
        kind = jnp.broadcast_to(group[:1, at], (rows, lanes))
        sums, running, shift = [], value, 1
        while shift < window:
            running = running + pltpu.roll(running, shift, 0)
            sums.append(running)
            shift *= 2
        total = sums[-1]
        for g in range(group_count - 1):
            total = jnp.where(kind == g, sums[g], total)
        length = jnp.left_shift(jnp.int32(2), kind)
        divisor = jnp.maximum(jnp.minimum(position + 1, length), 1).astype(jnp.float32)
        means = total / divisor - value
        mixed[:, at] = (means * scale[:1, at]).astype(jnp.bfloat16)


def pool_kernel(features, halo, *refs):
    pool(*refs, features, halo)


def out_kernel(pieces, shard, features, halo, *refs):
    operands, arrays = refs[:7], refs[7 : 7 + len(pieces)]
    out, w, mixed, sems = refs[7 + len(pieces) :]
    copies = load_weight(pieces, arrays, shard, w, sems)
    pool(*operands, mixed, features, halo)
    for copy in copies:
        copy.wait()
    step = min(256, w.shape[1])

    @pl.loop(0, w.shape[1] // step)
    def _(i):
        at = pl.ds(pl.multiple_of(i * step, step), step)
        out[:, at] = jnp.dot(mixed[...], w[:, at], preferred_element_type=jnp.float32).astype(jnp.bfloat16)


def last_kernel(pieces, shard, halo, *refs):
    place, mixed, state = refs[:3]
    arrays = refs[3 : 3 + len(pieces)]
    mine, theirs, w, kept, sems, kept_sem = refs[3 + len(pieces) :]
    copies = load_weight(pieces, arrays, shard, w, sems)
    count = mine.shape[0]
    here, there = [
        pl.ds(pl.multiple_of(halo + c * count, row_tile), count) for c in (place[1], 1 - place[1])
    ]
    keep = pltpu.make_async_copy(state.at[here], kept, kept_sem)
    keep.start()
    for copy in copies + [keep]:
        copy.wait()
    step = min(256, w.shape[1])

    @pl.loop(0, w.shape[1] // step)
    def _(i):
        at = pl.ds(pl.multiple_of(i * step, step), step)
        theirs[:, at] = jnp.dot(mixed[there, :], w[:, at], preferred_element_type=jnp.float32).astype(jnp.bfloat16)
        value = jnp.dot(mixed[here, :], w[:, at], preferred_element_type=jnp.float32)
        mine[:, at] = value + kept[:, at].astype(jnp.float32)


def body(inputs, norm_gain, in_weight, pool_scale, out_weight):
    rows, feats = inputs.shape
    layers, _, shard = in_weight.shape
    count = lax.axis_size("sp")
    nz = count // 4
    channels = shard * count
    half = channels // 2
    features = norm_gain.shape[1]
    bf16 = jnp.bfloat16
    here = lax.axis_index("sp")
    core = here % 2

    gain = lax.dynamic_slice_in_dim(norm_gain, lax.axis_index("tp") * feats, feats, 1)
    in_t = (jnp.swapaxes(in_weight, 1, 2).astype(jnp.float32) * gain[:, None, :]).astype(bf16)
    in_opposite = across(in_t)
    found = [None] * (2 * layers)

    def gather_group(stack, matrices, merged):
        arrived = lower(stack, nz)
        whole = [(across(v), at) for v, at in arrived] if merged else None
        for j, k in enumerate(matrices):
            l = k // 2
            mine = [(v, at, j) for v, at in arrived]
            if merged:
                crossed = [(v, [q + nz for q in at], j) for v, at in whole]
            else:
                crossed = [(across(v[j]), [q + nz for q in at], None) for v, at in arrived]
            opposite = (across(out_weight[l]), [nz], None) if k % 2 else (in_opposite, [nz], l)
            found[k] = gather(stack[j], opposite, mine, crossed, nz, k == 0)

    gather_group(in_t[:1], [0], True)
    gather_group(out_weight[:1], [1], True)
    gather_group(in_t[1:], list(range(2, 2 * layers, 2)), True)
    gather_group(out_weight[1:], list(range(3, 2 * layers, 2)), False)

    order = order_table(nz)
    table = [[(order[s // 4][b % nz] * 2 + ((s // 2) % 2 ^ (b // nz))) * 2 + s % 2 for b in range(2 * nz)] for s in range(count)]
    shards = jnp.asarray(np.array(table, np.int32))[here]
    channel = (shards[:, None] * shard + jnp.arange(shard, dtype=jnp.int32)[None, :]).reshape(1, half)
    group = jnp.broadcast_to(channel // (channels // group_count), (8, half))
    scale = pool_scale.reshape(layers, count, shard)[:, shards].reshape(layers, 1, half)
    scale = jnp.broadcast_to(scale, (layers, 8, half))
    place = jnp.stack([(here // 2) * 2 * rows, core]).astype(jnp.int32)

    halo = math.ceil(layers * (window - 1) / row_tile) * row_tile
    tail = inputs[rows - halo :]
    before = move(tail, "sp", lambda s: s + 2 if s % 2 == 1 and s + 2 < count else None)
    relay = move(before, "sp", lambda s: s - 1 if s % 2 == 1 else None)
    sibling = move(inputs, "sp", lambda s: s ^ 1)
    low = core == 0
    state = jnp.concatenate(
        [jnp.where(low, relay, before), jnp.where(low, inputs, sibling), jnp.where(low, sibling, inputs)], 0
    )
    total = state.shape[0]
    padded = math.ceil(total / lanes) * lanes
    shape = jax.ShapeDtypeStruct
    params = pltpu.CompilerParams(vmem_limit_bytes=16 * 2**20)
    flops = 2 * total * feats * half
    cost = pl.CostEstimate(flops=flops, bytes_accessed=2 * (half * feats + 3 * total * feats), transcendentals=0)

    deltas = []
    for l in range(layers):
        first, last = l == 0, l == layers - 1
        pieces = [(at, index) for _, at, index in found[2 * l]]
        arrays = [v for v, _, _ in found[2 * l]]
        outs = [shape((total, half), bf16), shape((8, padded), jnp.float32)]
        if not first:
            outs = [shape((total, feats), bf16)] + outs
        results = pl.pallas_call(
            functools.partial(in_kernel, first, pieces, shard),
            out_shape=outs,
            in_specs=[VMEM] * (1 if first else 3) + [ANY] * len(pieces),
            out_specs=([] if first else [HBM]) + [VMEM] * 2,
            scratch_shapes=[
                pltpu.VMEM((half, feats), bf16),
                pltpu.VMEM((padded, lanes), jnp.float32),
                pltpu.SemaphoreType.DMA((2 * nz,)),
            ]
            + ([] if first else [pltpu.VMEM((total, feats), bf16), pltpu.SemaphoreType.DMA]),
            compiler_params=params,
            cost_estimate=cost,
        )(state, *deltas, *arrays)
        if not first:
            state = results[0]
        partial, squares = results[-2:]
        bits = levels(lax.axis_size("tp"))
        for b, bit in enumerate(bits):
            swap = lambda v: move(v, "tp", lambda s: s ^ bit)
            others = [swap(partial), swap(squares)]
            if b < len(bits) - 1:
                partial, squares = partial + others[0], squares + others[1]
        pieces = [(at, index) for _, at, index in found[2 * l + 1]]
        arrays = [v for v, _, _ in found[2 * l + 1]]
        operands = (place, partial, others[0], squares, others[1], group, scale[l])
        weights = pltpu.VMEM((half, feats), bf16)
        sems = pltpu.SemaphoreType.DMA((2 * nz,))
        mixed = (total, half)
        call = dict(compiler_params=params, cost_estimate=cost)
        if not last:
            results = [
                pl.pallas_call(
                    functools.partial(out_kernel, pieces, shard, features, halo),
                    out_shape=shape((total, feats), bf16),
                    in_specs=[SMEM] + [VMEM] * 6 + [ANY] * len(pieces),
                    out_specs=VMEM,
                    scratch_shapes=[weights, pltpu.VMEM(mixed, bf16), sems],
                    **call,
                )(*operands, *arrays)
            ]
        else:
            mixed = pl.pallas_call(
                functools.partial(pool_kernel, features, halo),
                out_shape=shape(mixed, bf16),
                in_specs=[SMEM] + [VMEM] * 6,
                out_specs=VMEM,
                **call,
            )(*operands)
            results = pl.pallas_call(
                functools.partial(last_kernel, pieces, shard, halo),
                out_shape=[shape((rows, feats), jnp.float32), shape((rows, feats), bf16)],
                in_specs=[SMEM, VMEM, HBM] + [ANY] * len(pieces),
                out_specs=[VMEM] * 2,
                scratch_shapes=[weights, pltpu.VMEM((rows, feats), bf16), sems, pltpu.SemaphoreType.DMA],
                **call,
            )(place, mixed, state, *arrays)
        deltas = [results[0], move(results[-1], "sp", lambda s: s ^ 1)]

    return (deltas[0] + deltas[1].astype(jnp.float32)).astype(bf16)


def solution(mesh):
    placed = (P("sp", "tp"), P(), P(None, "tp", "sp"), P(), P(None, "sp", "tp"))

    return jax.shard_map(body, mesh=mesh, in_specs=placed, out_specs=P("sp", "tp"), check_vma=False)
```

time: 252 us -> 258 us (1.024)
  starting transfers between devices: 78.6 us -> 44.6 us
  waiting for transfers between devices: 125 us -> 155 us
  Pallas kernels: 24.5 us -> 29.9 us
  local copies, waits for them, and re-layouts: 10.9 us -> 14.5 us
    ppermute x46, starting transfers between devices: 78.6 us -> 44.6 us  [move(): lax.ppermute(value, axis, [(s, t) for s, t in pairs if t is not None])]
    ppermute x46, waiting for transfers between devices: 125 us -> 155 us  [move(): lax.ppermute(value, axis, [(s, t) for s, t in pairs if t is not None])]
    pallas_call x3 -> x4, Pallas kernels: 14.2 us -> 17.3 us  [the longest x2 10.5 us: body(): pl.pallas_call(functools.partial(out_kernel, pieces, shard, features, hal...]
    squeeze x2 -> x4, local copies, waits for them, and re-layouts: 2.83 us -> 5.78 us  [the longest x2 3.11 us: gather_group(): found[k] = gather(stack[j], opposite, mine, crossed, nz, k == 0)]
    unnamed x28 -> x42, local copies, waits for them, and re-layouts: 7.03 us -> 5.75 us
  transfers between devices with their start and end apart: 46 -> 46, of which waited for: 18 -> 19; matrix products, arithmetic and copies ran while one was open for 4% -> 6% of each run, Pallas kernels for 8% -> 6%
where the time goes in v1:
time: 258 us; the launch traced here: 256 us
  waiting for transfers between devices  155 us (60%)
  starting transfers between devices  44.6 us (17%)
  Pallas kernels  29.9 us (12%)
  local copies, waits for them, and re-layouts  14.5 us (6%)
  other arithmetic  11 us (4%)
    ppermute x46, waiting for transfers between devices, move(): lax.ppermute(value, axis, [(s, t) for s, t in pairs if t is not None])  155 us
    ppermute x46, starting transfers between devices, move(): lax.ppermute(value, axis, [(s, t) for s, t in pairs if t is not None])  44.6 us
    pallas_call x3, Pallas kernels, body(): pl.pallas_call(functools.partial(in_kernel, first, pieces, shard), out_sh...  12.7 us
    pallas_call x2, Pallas kernels, body(): pl.pallas_call(functools.partial(out_kernel, pieces, shard, features, hal...  10.5 us
    unnamed x42, local copies, waits for them, and re-layouts  5.75 us
  transfers between devices with their start and end apart: 46, of which 19 were waited for; matrix products, arithmetic and copies ran while one was open for 6% of the time, Pallas kernels for 6%

profile of v1, /device:TPU:4, one launch (start us, length us, event | category | flops | bytes accessed | tf_op | source)
XLA Modules:
  0.0 255.5 jit_solution(16707795153887928530)
XLA Ops:
  0.8 2.2 fusion
  3.0 2.0 slice_bitcast_fusion.2
  5.1 1.6 collective-permute-start.3
  6.6 1.4 collective-permute-start.4
  8.0 1.3 collective-permute-start
  9.4 1.1 slice_bitcast_fusion.6
  10.4 3.8 %collective-permute-start.14 = (bf16[1,64,2048]{2,1,0:T(8,128)(2,1)}, bf16[1,64,2048]{2,1,0:T(8,128)(2,1)S(1)}, u32[]{:S(2)}, u32[]{:S(2)}) collective-permute-start(bf16[1,64,2048]{2,1,0:T(8,128)(2,1)} %get-tuple-element.33), channel_id=1, source_target_pairs={{0,8},{2,10},{4,12},{6,14},{8,0},{10,2},{12,4},{14,6},{16,24},{18,... | collective-permute-start | bytes 786440 | tf_op jit(solution)/shard_map/ppermute | solution.py:28
  16.6 1.9 slice.84
  19.0 1.3 collective-permute-start.1
  20.3 1.0 collective-permute-done.14
  21.9 1.0 pad_maximum_fusion.1.refs_7_
  23.7 1.3 collective-permute-start.5
  25.6 13.2 %collective-permute-done.5 = bf16[64,2048]{1,0:T(8,128)(2,1)S(1)} collective-permute-done((bf16[64,2048]{1,0:T(8,128)(2,1)}, bf16[64,2048]{1,0:T(8,128)(2,1)S(1)}, u32[]{:S(2)}, u32[]{:S(2)}) %collective-permute-start.5) | collective-permute-done | bytes 262176 | tf_op jit(solution)/shard_map/ppermute | solution.py:28
  38.9 1.3 collective-permute-start.7
  40.2 8.6 %collective-permute-done.7 = bf16[64,2048]{1,0:T(8,128)(2,1)S(1)} collective-permute-done((bf16[64,2048]{1,0:T(8,128)(2,1)S(1)}, bf16[64,2048]{1,0:T(8,128)(2,1)S(1)}, u32[]{:S(2)}, u32[]{:S(2)}) %collective-permute-start.7) | collective-permute-done | bytes 262176 | tf_op jit(solution)/shard_map/ppermute | solution.py:28
  48.8 2.1 collective-permute-start.11
  50.9 1.3 collective-permute-start.16
  52.2 1.4 broadcast_select_fusion.1
  54.0 4.0 %collective-permute-done.10.refs_7_ = bf16[64,2048]{1,0:T(8,128)(2,1)S(1)} collective-permute-done((bf16[64,2048]{1,0:T(8,128)(2,1)S(1)}, bf16[64,2048]{1,0:T(8,128)(2,1)S(1)}, u32[]{:S(2)}, u32[]{:S(2)}) %collective-permute-start.10) | collective-permute-done | bytes 262176 | tf_op jit(solution)/shard_map/ppermute | solution.py:28
  58.0 5.6 %collective-permute-done.11.refs_8_ = bf16[64,2048]{1,0:T(8,128)(2,1)S(1)} collective-permute-done((bf16[64,2048]{1,0:T(8,128)(2,1)S(1)}, bf16[64,2048]{1,0:T(8,128)(2,1)S(1)}, u32[]{:S(2)}, u32[]{:S(2)}) %collective-permute-start.11) | collective-permute-done | bytes 262176 | tf_op jit(solution)/shard_map/ppermute | solution.py:28
  63.6 3.6 %shard_map.64 = (bf16[560,512]{1,0:T(8,128)(2,1)}, f32[8,640]{1,0:T(8,128)S(1)}) custom-call(bf16[560,2048]{1,0:T(8,128)(2,1)S(1)} %pad_maximum_fusion.refs_0_, bf16[64,2048]{1,0:T(8,128)(2,1)S(1)} %get-tuple-element.35.refs_1_, bf16[1,64,2048]{2,1,0:T(8,128)(2,1)} %collective-permute-done.3.refs_2_, bf16[64,2048]{1,0:T(8,128)(2,1)S(1)} %broadcast_select_fusion.8.refs_3_, ...), custom_call_target="tpu_custom_call" | custom-call | flops 1174405120 | bytes 8978432 | tf_op jit(solution)/shard_map/pallas_call | solution.py:286
  67.1 1.6 collective-permute-start.12
  68.7 0.8 broadcast_select_fusion.6.refs_8_
  69.7 2.0 collective-permute-start.18
  71.7 4.7 %collective-permute-done.21 = bf16[2,64,2048]{2,1,0:T(8,128)(2,1)} collective-permute-done((bf16[2,64,2048]{2,1,0:T(8,128)(2,1)}, bf16[2,64,2048]{2,1,0:T(8,128)(2,1)}, u32[]{:S(2)}, u32[]{:S(2)}) %collective-permute-start.21) | collective-permute-done | bytes 524320 | tf_op jit(solution)/shard_map/ppermute | solution.py:28
  76.4 1.5 collective-permute-start.13
  77.9 1.8 slice_bitcast_fusion.1
  79.6 5.4 %collective-permute-done.18.refs_10_ = bf16[1,64,2048]{2,1,0:T(8,128)(2,1)S(1)} collective-permute-done((bf16[1,64,2048]{2,1,0:T(8,128)(2,1)}, bf16[1,64,2048]{2,1,0:T(8,128)(2,1)S(1)}, u32[]{:S(2)}, u32[]{:S(2)}) %collective-permute-start.18) | collective-permute-done | bytes 262176 | tf_op jit(solution)/shard_map/ppermute | solution.py:28
  85.1 1.0 copy-done.8
  86.1 5.3 %shard_map.65.refs_1_ = bf16[560,2048]{1,0:T(8,128)(2,1)S(1)} custom-call(s32[2]{0:T(128)S(1)} %pad_add_fusion.refs_0_, bf16[560,512]{1,0:T(8,128)(2,1)} %get-tuple-element.15.refs_1_, bf16[560,512]{1,0:T(8,128)(2,1)} %collective-permute-done.12.refs_2_, f32[8,640]{1,0:T(8,128)S(1)} %get-tuple-element.16.refs_3_, ...), custom_call_target="tpu_custom_call" | custom-call | flops 1174405120 | bytes 8978432 | tf_op jit(solution)/shard_map/pallas_call | solution.py:318
  92.3 2.0 collective-permute-start.28
  94.3 1.3 collective-permute-start.23
  95.6 11.1 %collective-permute-done.28 = bf16[2,64,2048]{2,1,0:T(8,128)(2,1)S(1)} collective-permute-done((bf16[2,64,2048]{2,1,0:T(8,128)(2,1)S(1)}, bf16[2,64,2048]{2,1,0:T(8,128)(2,1)S(1)}, u32[]{:S(2)}, u32[]{:S(2)}) %collective-permute-start.28) | collective-permute-done | bytes 524320 | tf_op jit(solution)/shard_map/ppermute | solution.py:28
  106.7 0.9 slice_bitcast_fusion
  107.6 1.1 pad_maximum_fusion.3.refs_7_
  110.0 10.3 %collective-permute-done.23 = bf16[128,2048]{1,0:T(8,128)(2,1)S(1)} collective-permute-done((bf16[128,2048]{1,0:T(8,128)(2,1)S(1)}, bf16[128,2048]{1,0:T(8,128)(2,1)S(1)}, u32[]{:S(2)}, u32[]{:S(2)}) %collective-permute-start.23) | collective-permute-done | bytes 524320 | tf_op jit(solution)/shard_map/ppermute | solution.py:28
  121.0 1.3 collective-permute-start.30
  122.3 1.9 collective-permute-done.24.refs_6_
  124.1 10.2 %collective-permute-done.25.refs_7_ = bf16[128,2048]{1,0:T(8,128)(2,1)S(1)} collective-permute-done((bf16[128,2048]{1,0:T(8,128)(2,1)S(1)}, bf16[128,2048]{1,0:T(8,128)(2,1)S(1)}, u32[]{:S(2)}, u32[]{:S(2)}) %collective-permute-start.25) | collective-permute-done | bytes 524320 | tf_op jit(solution)/shard_map/ppermute | solution.py:28
  134.3 4.5 %shard_map.66 = (bf16[560,2048]{1,0:T(8,128)(2,1)S(1)}, bf16[560,512]{1,0:T(8,128)(2,1)}, f32[8,640]{1,0:T(8,128)S(1)}) custom-call(bf16[560,2048]{1,0:T(8,128)(2,1)S(1)} %pad_maximum_fusion.refs_0_, bf16[560,2048]{1,0:T(8,128)(2,1)S(1)} %shard_map.65.refs_1_, bf16[560,2048]{1,0:T(8,128)(2,1)S(1)} %collective-permute-done.20.refs_2_, ...), custom_call_target="tpu_custom_call" | custom-call | flops 1174405120 | bytes 8978432 | tf_op jit(solution)/shard_map/pallas_call | solution.py:286
  138.9 1.4 copy-done.1
  141.5 1.5 collective-permute-start.31
  143.6 1.5 collective-permute-start.27
  145.1 16.3 %collective-permute-done.31.refs_9_ = bf16[64,2048]{1,0:T(8,128)(2,1)S(1)} collective-permute-done((bf16[64,2048]{1,0:T(8,128)(2,1)}, bf16[64,2048]{1,0:T(8,128)(2,1)S(1)}, u32[]{:S(2)}, u32[]{:S(2)}) %collective-permute-start.31) | collective-permute-done | bytes 262176 | tf_op jit(solution)/shard_map/ppermute | solution.py:28
  161.4 3.5 %collective-permute-done.32.refs_10_ = bf16[64,2048]{1,0:T(8,128)(2,1)S(1)} collective-permute-done((bf16[64,2048]{1,0:T(8,128)(2,1)}, bf16[64,2048]{1,0:T(8,128)(2,1)S(1)}, u32[]{:S(2)}, u32[]{:S(2)}) %collective-permute-start.32) | collective-permute-done | bytes 262176 | tf_op jit(solution)/shard_map/ppermute | solution.py:28
  164.9 1.0 copy-done.12
  165.9 5.2 %shard_map.67.refs_1_ = bf16[560,2048]{1,0:T(8,128)(2,1)S(1)} custom-call(s32[2]{0:T(128)S(1)} %pad_add_fusion.refs_0_, bf16[560,512]{1,0:T(8,128)(2,1)} %get-tuple-element.18.refs_1_, bf16[560,512]{1,0:T(8,128)(2,1)S(1)} %collective-permute-done.26.refs_2_, f32[8,640]{1,0:T(8,128)S(1)} %get-tuple-element.19.refs_3_, ...), custom_call_target="tpu_custom_call" | custom-call | flops 1174405120 | bytes 8978432 | tf_op jit(solution)/shard_map/pallas_call | solution.py:318
  171.2 0.8 collective-permute-start.35
  172.1 1.3 collective-permute-start.36
  173.4 1.1 pad_maximum_fusion.5.refs_3_
  175.2 28.5 %collective-permute-done.36 = bf16[128,2048]{1,0:T(8,128)(2,1)S(1)} collective-permute-done((bf16[128,2048]{1,0:T(8,128)(2,1)S(1)}, bf16[128,2048]{1,0:T(8,128)(2,1)S(1)}, u32[]{:S(2)}, u32[]{:S(2)}) %collective-permute-start.36) | collective-permute-done | bytes 524320 | tf_op jit(solution)/shard_map/ppermute | solution.py:28
  204.4 1.5 collective-permute-start.41
  205.9 10.7 %collective-permute-done.37.refs_7_ = bf16[128,2048]{1,0:T(8,128)(2,1)S(1)} collective-permute-done((bf16[128,2048]{1,0:T(8,128)(2,1)S(1)}, bf16[128,2048]{1,0:T(8,128)(2,1)S(1)}, u32[]{:S(2)}, u32[]{:S(2)}) %collective-permute-start.37) | collective-permute-done | bytes 524320 | tf_op jit(solution)/shard_map/ppermute | solution.py:28
  216.6 4.6 %shard_map.68 = (bf16[560,2048]{1,0:T(8,128)(2,1)S(1)}, bf16[560,512]{1,0:T(8,128)(2,1)}, f32[8,640]{1,0:T(8,128)S(1)}) custom-call(bf16[560,2048]{1,0:T(8,128)(2,1)S(1)} %copy-done.2, bf16[560,2048]{1,0:T(8,128)(2,1)S(1)} %shard_map.67.refs_1_, bf16[560,2048]{1,0:T(8,128)(2,1)S(1)} %collective-permute-done.34.refs_2_, ...), custom_call_target="tpu_custom_call" | custom-call | flops 1174405120 | bytes 8978432 | tf_op jit(solution)/shard_map/pallas_call | solution.py:286
  221.2 1.4 copy-done.3
  222.6 1.5 collective-permute-start.38
  224.8 1.5 collective-permute-start.42
  227.4 8.8 %collective-permute-done.39.refs_4_ = f32[8,640]{1,0:T(8,128)S(1)} collective-permute-done((f32[8,640]{1,0:T(8,128)S(1)}, f32[8,640]{1,0:T(8,128)S(1)}, u32[]{:S(2)}, u32[]{:S(2)}) %collective-permute-start.39) | collective-permute-done | bytes 20512 | tf_op jit(solution)/shard_map/ppermute | solution.py:28
  236.2 2.5 shard_map.69.refs_1_
  238.7 5.7 %collective-permute-done.42.refs_5_ = bf16[64,2048]{1,0:T(8,128)(2,1)} collective-permute-done((bf16[64,2048]{1,0:T(8,128)(2,1)}, bf16[64,2048]{1,0:T(8,128)(2,1)}, u32[]{:S(2)}, u32[]{:S(2)}) %collective-permute-start.42) | collective-permute-done | bytes 262176 | tf_op jit(solution)/shard_map/ppermute | solution.py:28
  244.3 2.8 %collective-permute-done.43.refs_6_ = bf16[64,2048]{1,0:T(8,128)(2,1)} collective-permute-done((bf16[64,2048]{1,0:T(8,128)(2,1)}, bf16[64,2048]{1,0:T(8,128)(2,1)}, u32[]{:S(2)}, u32[]{:S(2)}) %collective-permute-start.43) | collective-permute-done | bytes 262176 | tf_op jit(solution)/shard_map/ppermute | solution.py:28
  247.2 4.3 %shard_map.70 = (f32[256,2048]{1,0:T(8,128)S(1)}, bf16[256,2048]{1,0:T(8,128)(2,1)S(1)}) custom-call(s32[2]{0:T(128)S(1)} %pad_add_fusion.refs_0_, bf16[560,512]{1,0:T(8,128)(2,1)S(1)} %shard_map.69.refs_1_, bf16[560,2048]{1,0:T(8,128)(2,1)S(1)} %copy-done.4, bf16[128,2048]{1,0:T(8,128)(2,1)S(1)} %copy-done.10, ...), custom_call_target="tpu_custom_call" | custom-call | flops 1174405120 | bytes 8978432 | tf_op jit(solution)/shard_map/pallas_call | solution.py:335
  251.6 2.6 %collective-permute-done.45 = bf16[256,2048]{1,0:T(8,128)(2,1)S(1)} collective-permute-done((bf16[256,2048]{1,0:T(8,128)(2,1)S(1)}, bf16[256,2048]{1,0:T(8,128)(2,1)S(1)}, u32[]{:S(2)}, u32[]{:S(2)}) %collective-permute-start.45) | collective-permute-done | bytes 1048608 | tf_op jit(solution)/shard_map/ppermute | solution.py:28
  254.2 1.3 add_convert_fusion
  (120 shorter events, 14.5 us)
Async XLA Ops:
  0.0 8.0 %copy-start.15 = (bf16[256,2048]{1,0:T(8,128)(2,1)S(1)}, bf16[256,2048]{1,0:T(8,128)(2,1)}, u32[]{:S(2)}) copy-start(bf16[256,2048]{1,0:T(8,128)(2,1)} %param.6) | copy-start | bytes 3145732
  0.0 9.4 %copy-start.13 = (bf16[3,64,2048]{2,1,0:T(8,128)(2,1)S(1)}, bf16[3,64,2048]{2,1,0:T(8,128)(2,1)}, u32[]{:S(2)}) copy-start(bf16[3,64,2048]{2,1,0:T(8,128)(2,1)} %param.10) | copy-start | bytes 2359300
  3.0 12.8 %copy-start.20 = (f32[3,1024]{1,0:T(4,128)S(1)}, f32[3,1024]{1,0:T(4,128)}, u32[]{:S(2)}) copy-start(f32[3,1024]{1,0:T(4,128)} %param.9) | copy-start | bytes 36868
  5.1 13.9 %collective-permute-start.3 = (bf16[1,64,2048]{2,1,0:T(8,128)(2,1)S(1)}, bf16[1,64,2048]{2,1,0:T(8,128)(2,1)}, u32[]{:S(2)}, u32[]{:S(2)}) collective-permute-start(bf16[1,64,2048]{2,1,0:T(8,128)(2,1)S(1)} %get-tuple-element.37), channel_id=1, source_target_pairs={{0,8},{2,10},{4,12},{6,14},{8,0},{10,2},{12,4},{14,6},{16,24},{18,... | collective-permute-start | bytes 786440 | tf_op jit(solution)/shard_map/ppermute | solution.py:28
  6.6 16.3 %collective-permute-start.4 = (bf16[64,2048]{1,0:T(8,128)(2,1)S(1)}, bf16[64,2048]{1,0:T(8,128)(2,1)}, u32[]{:S(2)}, u32[]{:S(2)}) collective-permute-start(bf16[64,2048]{1,0:T(8,128)(2,1)S(1)} %get-tuple-element.35.refs_1_), channel_id=1, source_target_pairs={{8,16},{10,18},{12,20},{14,22},{16,8},{18,10},{20,12},{22,14},{9,1... | collective-permute-start | bytes 786440 | tf_op jit(solution)/shard_map/ppermute | solution.py:28
  8.0 42.9 %collective-permute-start.2 = (bf16[256,2048]{1,0:T(8,128)(2,1)S(1)}, bf16[256,2048]{1,0:T(8,128)(2,1)}, u32[]{:S(2)}, u32[]{:S(2)}) collective-permute-start(bf16[256,2048]{1,0:T(8,128)(2,1)S(1)} %copy-done.15), channel_id=1, source_target_pairs={{0,2},{2,0},{4,6},{6,4},{8,10},{10,8},{12,14},{14,12},{16,18},{18,... | collective-permute-start | bytes 3145736 | tf_op jit(solution)/shard_map/ppermute | solution.py:28
  8.0 10.4 %collective-permute-start = (bf16[48,2048]{1,0:T(8,128)(2,1)S(1)}, bf16[48,2048]{1,0:T(8,128)(2,1)}, u32[]{:S(2)}, u32[]{:S(2)}) collective-permute-start(bf16[48,2048]{1,0:T(8,128)(2,1)S(1)} %slice.63), channel_id=1, source_target_pairs={{2,6},{6,10},{10,14},{14,18},{18,22},{22,26},{26,30},{3,7},{7,11},... | collective-permute-start | bytes 589832 | tf_op jit(solution)/shard_map/ppermute | solution.py:28
  10.4 10.8 %collective-permute-start.14 = (bf16[1,64,2048]{2,1,0:T(8,128)(2,1)}, bf16[1,64,2048]{2,1,0:T(8,128)(2,1)S(1)}, u32[]{:S(2)}, u32[]{:S(2)}) collective-permute-start(bf16[1,64,2048]{2,1,0:T(8,128)(2,1)} %get-tuple-element.33), channel_id=1, source_target_pairs={{0,8},{2,10},{4,12},{6,14},{8,0},{10,2},{12,4},{14,6},{16,24},{18,... | collective-permute-start | bytes 786440 | tf_op jit(solution)/shard_map/ppermute | solution.py:28
  18.5 39.5 %collective-permute-start.8 = (bf16[3,64,2048]{2,1,0:T(8,128)(2,1)}, bf16[3,64,2048]{2,1,0:T(8,128)(2,1)S(1)}, u32[]{:S(2)}, u32[]{:S(2)}) collective-permute-start(bf16[3,64,2048]{2,1,0:T(8,128)(2,1)} %fusion), channel_id=1, source_target_pairs={{0,4},{2,6},{4,0},{6,2},{8,12},{10,14},{12,8},{14,10},{16,20},{18,... | collective-permute-start | bytes 2359304 | tf_op jit(solution)/shard_map/ppermute | solution.py:28
  19.0 4.7 %collective-permute-start.1 = (bf16[48,2048]{1,0:T(8,128)(2,1)}, bf16[48,2048]{1,0:T(8,128)(2,1)S(1)}, u32[]{:S(2)}, u32[]{:S(2)}) collective-permute-start(bf16[48,2048]{1,0:T(8,128)(2,1)} %collective-permute-done), channel_id=1, source_target_pairs={{2,0},{6,4},{10,8},{14,12},{18,16},{22,20},{26,24},{30,28},{3,1},{... | collective-permute-start | bytes 589832 | tf_op jit(solution)/shard_map/ppermute | solution.py:28
  21.2 32.3 %copy-start.19 = (bf16[1,64,2048]{2,1,0:T(8,128)(2,1)}, bf16[1,64,2048]{2,1,0:T(8,128)(2,1)S(1)}, u32[]{:S(2)}) copy-start(bf16[1,64,2048]{2,1,0:T(8,128)(2,1)S(1)} %collective-permute-done.14) | copy-start | bytes 786436
  21.2 3.7 %collective-permute-start.6 = (bf16[64,2048]{1,0:T(8,128)(2,1)}, bf16[64,2048]{1,0:T(8,128)(2,1)S(1)}, u32[]{:S(2)}, u32[]{:S(2)}) collective-permute-start(bf16[64,2048]{1,0:T(8,128)(2,1)} %bitcast.4), channel_id=1, source_target_pairs={{8,16},{10,18},{12,20},{14,22},{16,8},{18,10},{20,12},{22,14},{9,1... | collective-permute-start | bytes 786440 | tf_op jit(solution)/shard_map/ppermute | solution.py:28
  22.9 30.7 %copy-start.7 = (bf16[128,2048]{1,0:T(8,128)(2,1)}, bf16[128,2048]{1,0:T(8,128)(2,1)S(1)}, u32[]{:S(2)}) copy-start(bf16[128,2048]{1,0:T(8,128)(2,1)S(1)} %pad_maximum_fusion.1.refs_7_) | copy-start | bytes 1572868
  22.9 25.9 %collective-permute-start.15 = (bf16[128,2048]{1,0:T(8,128)(2,1)S(1)}, bf16[128,2048]{1,0:T(8,128)(2,1)S(1)}, u32[]{:S(2)}, u32[]{:S(2)}) collective-permute-start(bf16[128,2048]{1,0:T(8,128)(2,1)S(1)} %pad_maximum_fusion.1.refs_7_), channel_id=1, source_target_pairs={{8,16},{10,18},{12,20},{14,22},{16,8},{18,10},{20,12},{22,14},{9,1... | collective-permute-start | bytes 1572872 | tf_op jit(solution)/shard_map/ppermute | solution.py:28
  23.7 15.2 %collective-permute-start.5 = (bf16[64,2048]{1,0:T(8,128)(2,1)}, bf16[64,2048]{1,0:T(8,128)(2,1)S(1)}, u32[]{:S(2)}, u32[]{:S(2)}) collective-permute-start(bf16[64,2048]{1,0:T(8,128)(2,1)} %collective-permute-done.4), channel_id=1, source_target_pairs={{8,0},{10,2},{12,4},{14,6},{16,24},{18,26},{20,28},{22,30},{9,1},{... | collective-permute-start | bytes 786440 | tf_op jit(solution)/shard_map/ppermute | solution.py:28
  25.0 28.9 %collective-permute-start.9 = (bf16[1,64,2048]{2,1,0:T(8,128)(2,1)}, bf16[1,64,2048]{2,1,0:T(8,128)(2,1)S(1)}, u32[]{:S(2)}, u32[]{:S(2)}) collective-permute-start(bf16[1,64,2048]{2,1,0:T(8,128)(2,1)} %collective-permute-done.3.refs_2_), channel_id=1, source_target_pairs={{0,4},{2,6},{4,0},{6,2},{8,12},{10,14},{12,8},{14,10},{16,20},{18,... | collective-permute-start | bytes 786440 | tf_op jit(solution)/shard_map/ppermute | solution.py:28
  38.9 9.9 %collective-permute-start.7 = (bf16[64,2048]{1,0:T(8,128)(2,1)S(1)}, bf16[64,2048]{1,0:T(8,128)(2,1)S(1)}, u32[]{:S(2)}, u32[]{:S(2)}) collective-permute-start(bf16[64,2048]{1,0:T(8,128)(2,1)S(1)} %collective-permute-done.6), channel_id=1, source_target_pairs={{8,0},{10,2},{12,4},{14,6},{16,24},{18,26},{20,28},{22,30},{9,1},{... | collective-permute-start | bytes 786440 | tf_op jit(solution)/shard_map/ppermute | solution.py:28
  48.8 9.2 %collective-permute-start.10 = (bf16[64,2048]{1,0:T(8,128)(2,1)S(1)}, bf16[64,2048]{1,0:T(8,128)(2,1)S(1)}, u32[]{:S(2)}, u32[]{:S(2)}) collective-permute-start(bf16[64,2048]{1,0:T(8,128)(2,1)S(1)} %broadcast_select_fusion.8.refs_3_), channel_id=1, source_target_pairs={{0,4},{2,6},{4,0},{6,2},{8,12},{10,14},{12,8},{14,10},{16,20},{18,... | collective-permute-start | bytes 786440 | tf_op jit(solution)/shard_map/ppermute | solution.py:28
  48.8 14.7 %collective-permute-start.11 = (bf16[64,2048]{1,0:T(8,128)(2,1)S(1)}, bf16[64,2048]{1,0:T(8,128)(2,1)S(1)}, u32[]{:S(2)}, u32[]{:S(2)}) collective-permute-start(bf16[64,2048]{1,0:T(8,128)(2,1)S(1)} %broadcast_select_fusion.7.refs_4_), channel_id=1, source_target_pairs={{0,4},{2,6},{4,0},{6,2},{8,12},{10,14},{12,8},{14,10},{16,20},{18,... | collective-permute-start | bytes 786440 | tf_op jit(solution)/shard_map/ppermute | solution.py:28
  50.9 17.8 %collective-permute-start.16 = (bf16[128,2048]{1,0:T(8,128)(2,1)S(1)}, bf16[128,2048]{1,0:T(8,128)(2,1)S(1)}, u32[]{:S(2)}, u32[]{:S(2)}) collective-permute-start(bf16[128,2048]{1,0:T(8,128)(2,1)S(1)} %collective-permute-done.15), channel_id=1, source_target_pairs={{8,0},{10,2},{12,4},{14,6},{16,24},{18,26},{20,28},{22,30},{9,1},{... | collective-permute-start | bytes 1572872 | tf_op jit(solution)/shard_map/ppermute | solution.py:28
  53.9 25.8 %collective-permute-start.17 = (bf16[64,2048]{1,0:T(8,128)(2,1)}, bf16[64,2048]{1,0:T(8,128)(2,1)}, u32[]{:S(2)}, u32[]{:S(2)}) collective-permute-start(bf16[64,2048]{1,0:T(8,128)(2,1)} %get-tuple-element.31), channel_id=1, source_target_pairs={{0,4},{2,6},{4,0},{6,2},{8,12},{10,14},{12,8},{14,10},{16,20},{18,... | collective-permute-start | bytes 786440 | tf_op jit(solution)/shard_map/ppermute | solution.py:28
  58.0 18.4 %collective-permute-start.21 = (bf16[2,64,2048]{2,1,0:T(8,128)(2,1)}, bf16[2,64,2048]{2,1,0:T(8,128)(2,1)}, u32[]{:S(2)}, u32[]{:S(2)}) collective-permute-start(bf16[2,64,2048]{2,1,0:T(8,128)(2,1)} %slice.84), channel_id=1, source_target_pairs={{0,8},{2,10},{4,12},{6,14},{8,0},{10,2},{12,4},{14,6},{16,24},{18,... | collective-permute-start | bytes 1572872 | tf_op jit(solution)/shard_map/ppermute | solution.py:28
  67.1 17.9 %collective-permute-start.12 = (bf16[560,512]{1,0:T(8,128)(2,1)}, bf16[560,512]{1,0:T(8,128)(2,1)}, u32[]{:S(2)}, u32[]{:S(2)}) collective-permute-start(bf16[560,512]{1,0:T(8,128)(2,1)} %get-tuple-element.15.refs_1_), channel_id=1, source_target_pairs={{0,1},{1,0},{2,3},{3,2},{4,5},{5,4},{6,7},{7,6},{8,9},{9,8},{10,11... | collective-permute-start | bytes 1720328 | tf_op jit(solution)/shard_map/ppermute | solution.py:28
  69.5 15.5 %collective-permute-start.19 = (bf16[128,2048]{1,0:T(8,128)(2,1)}, bf16[128,2048]{1,0:T(8,128)(2,1)}, u32[]{:S(2)}, u32[]{:S(2)}) collective-permute-start(bf16[128,2048]{1,0:T(8,128)(2,1)} %broadcast_select_fusion.6.refs_8_), channel_id=1, source_target_pairs={{0,4},{2,6},{4,0},{6,2},{8,12},{10,14},{12,8},{14,10},{16,20},{18,... | collective-permute-start | bytes 1572872 | tf_op jit(solution)/shard_map/ppermute | solution.py:28
  69.7 15.3 %collective-permute-start.18 = (bf16[1,64,2048]{2,1,0:T(8,128)(2,1)}, bf16[1,64,2048]{2,1,0:T(8,128)(2,1)S(1)}, u32[]{:S(2)}, u32[]{:S(2)}) collective-permute-start(bf16[1,64,2048]{2,1,0:T(8,128)(2,1)} %copy-done.19), channel_id=1, source_target_pairs={{0,4},{2,6},{4,0},{6,2},{8,12},{10,14},{12,8},{14,10},{16,20},{18,... | collective-permute-start | bytes 786440 | tf_op jit(solution)/shard_map/ppermute | solution.py:28
  76.4 8.7 %collective-permute-start.13 = (f32[8,640]{1,0:T(8,128)S(1)}, f32[8,640]{1,0:T(8,128)S(1)}, u32[]{:S(2)}, u32[]{:S(2)}) collective-permute-start(f32[8,640]{1,0:T(8,128)S(1)} %get-tuple-element.16.refs_3_), channel_id=1, source_target_pairs={{0,1},{1,0},{2,3},{3,2},{4,5},{5,4},{6,7},{7,6},{8,9},{9,8},{10,11... | collective-permute-start | bytes 61448 | tf_op jit(solution)/shard_map/ppermute | solution.py:28
  86.1 5.4 %copy-start.17 = (bf16[64,2048]{1,0:T(8,128)(2,1)S(1)}, bf16[64,2048]{1,0:T(8,128)(2,1)}, u32[]{:S(2)}) copy-start(bf16[64,2048]{1,0:T(8,128)(2,1)} %get-tuple-element.36) | copy-start | bytes 786436
  86.1 6.1 %copy-start.14 = (bf16[3,64,2048]{2,1,0:T(8,128)(2,1)S(1)}, bf16[3,64,2048]{2,1,0:T(8,128)(2,1)}, u32[]{:S(2)}) copy-start(bf16[3,64,2048]{2,1,0:T(8,128)(2,1)} %param.10) | copy-start | bytes 2359300
  91.4 42.9 %collective-permute-start.20 = (bf16[560,2048]{1,0:T(8,128)(2,1)S(1)}, bf16[560,2048]{1,0:T(8,128)(2,1)S(1)}, u32[]{:S(2)}, u32[]{:S(2)}) collective-permute-start(bf16[560,2048]{1,0:T(8,128)(2,1)S(1)} %shard_map.65.refs_1_), channel_id=1, source_target_pairs={{0,2},{2,0},{4,6},{6,4},{8,10},{10,8},{12,14},{14,12},{16,18},{18,... | collective-permute-start | bytes 6881288 | tf_op jit(solution)/shard_map/ppermute | solution.py:28
  91.5 2.7 %collective-permute-start.22 = (bf16[128,2048]{1,0:T(8,128)(2,1)S(1)}, bf16[128,2048]{1,0:T(8,128)(2,1)S(1)}, u32[]{:S(2)}, u32[]{:S(2)}) collective-permute-start(bf16[128,2048]{1,0:T(8,128)(2,1)S(1)} %pad_maximum_fusion.2.refs_3_), channel_id=1, source_target_pairs={{8,16},{10,18},{12,20},{14,22},{16,8},{18,10},{20,12},{22,14},{9,1... | collective-permute-start | bytes 1572872 | tf_op jit(solution)/shard_map/ppermute | solution.py:28
  92.3 14.4 %collective-permute-start.28 = (bf16[2,64,2048]{2,1,0:T(8,128)(2,1)S(1)}, bf16[2,64,2048]{2,1,0:T(8,128)(2,1)S(1)}, u32[]{:S(2)}, u32[]{:S(2)}) collective-permute-start(bf16[2,64,2048]{2,1,0:T(8,128)(2,1)S(1)} %slice.72), channel_id=1, source_target_pairs={{0,8},{2,10},{4,12},{6,14},{8,0},{10,2},{12,4},{14,6},{16,24},{18,... | collective-permute-start | bytes 1572872 | tf_op jit(solution)/shard_map/ppermute | solution.py:28
  94.3 26.0 %collective-permute-start.23 = (bf16[128,2048]{1,0:T(8,128)(2,1)S(1)}, bf16[128,2048]{1,0:T(8,128)(2,1)S(1)}, u32[]{:S(2)}, u32[]{:S(2)}) collective-permute-start(bf16[128,2048]{1,0:T(8,128)(2,1)S(1)} %collective-permute-done.22), channel_id=1, source_target_pairs={{8,0},{10,2},{12,4},{14,6},{16,24},{18,26},{20,28},{22,30},{9,1},{... | collective-permute-start | bytes 1572872 | tf_op jit(solution)/shard_map/ppermute | solution.py:28
  108.6 25.7 %copy-start.11 = (bf16[128,2048]{1,0:T(8,128)(2,1)}, bf16[128,2048]{1,0:T(8,128)(2,1)S(1)}, u32[]{:S(2)}) copy-start(bf16[128,2048]{1,0:T(8,128)(2,1)S(1)} %pad_maximum_fusion.3.refs_7_) | copy-start | bytes 1572868
  108.7 12.3 %collective-permute-start.29 = (bf16[128,2048]{1,0:T(8,128)(2,1)S(1)}, bf16[128,2048]{1,0:T(8,128)(2,1)S(1)}, u32[]{:S(2)}, u32[]{:S(2)}) collective-permute-start(bf16[128,2048]{1,0:T(8,128)(2,1)S(1)} %pad_maximum_fusion.3.refs_7_), channel_id=1, source_target_pairs={{8,16},{10,18},{12,20},{14,22},{16,8},{18,10},{20,12},{22,14},{9,1... | collective-permute-start | bytes 1572872 | tf_op jit(solution)/shard_map/ppermute | solution.py:28
  109.4 14.8 %collective-permute-start.24 = (bf16[2,64,2048]{2,1,0:T(8,128)(2,1)}, bf16[2,64,2048]{2,1,0:T(8,128)(2,1)S(1)}, u32[]{:S(2)}, u32[]{:S(2)}) collective-permute-start(bf16[2,64,2048]{2,1,0:T(8,128)(2,1)} %collective-permute-done.21), channel_id=1, source_target_pairs={{0,4},{2,6},{4,0},{6,2},{8,12},{10,14},{12,8},{14,10},{16,20},{18,... | collective-permute-start | bytes 1572872 | tf_op jit(solution)/shard_map/ppermute | solution.py:28
  120.3 14.0 %collective-permute-start.25 = (bf16[128,2048]{1,0:T(8,128)(2,1)S(1)}, bf16[128,2048]{1,0:T(8,128)(2,1)S(1)}, u32[]{:S(2)}, u32[]{:S(2)}) collective-permute-start(bf16[128,2048]{1,0:T(8,128)(2,1)S(1)} %broadcast_select_fusion.5.refs_4_), channel_id=1, source_target_pairs={{0,4},{2,6},{4,0},{6,2},{8,12},{10,14},{12,8},{14,10},{16,20},{18,... | collective-permute-start | bytes 1572872 | tf_op jit(solution)/shard_map/ppermute | solution.py:28
  121.0 19.9 %collective-permute-start.30 = (bf16[128,2048]{1,0:T(8,128)(2,1)S(1)}, bf16[128,2048]{1,0:T(8,128)(2,1)S(1)}, u32[]{:S(2)}, u32[]{:S(2)}) collective-permute-start(bf16[128,2048]{1,0:T(8,128)(2,1)S(1)} %collective-permute-done.29), channel_id=1, source_target_pairs={{8,0},{10,2},{12,4},{14,6},{16,24},{18,26},{20,28},{22,30},{9,1},{... | collective-permute-start | bytes 1572872 | tf_op jit(solution)/shard_map/ppermute | solution.py:28
  124.1 14.8 %copy-start.5 = (bf16[2,64,2048]{2,1,0:T(8,128)(2,1)}, bf16[2,64,2048]{2,1,0:T(8,128)(2,1)S(1)}, u32[]{:S(2)}) copy-start(bf16[2,64,2048]{2,1,0:T(8,128)(2,1)S(1)} %collective-permute-done.24.refs_6_) | copy-start | bytes 1572868
  138.9 1.4 copy-start.1
  140.3 24.5 %collective-permute-start.26 = (bf16[560,512]{1,0:T(8,128)(2,1)}, bf16[560,512]{1,0:T(8,128)(2,1)S(1)}, u32[]{:S(2)}, u32[]{:S(2)}) collective-permute-start(bf16[560,512]{1,0:T(8,128)(2,1)} %get-tuple-element.18.refs_1_), channel_id=1, source_target_pairs={{0,1},{1,0},{2,3},{3,2},{4,5},{5,4},{6,7},{7,6},{8,9},{9,8},{10,11... | collective-permute-start | bytes 1720328 | tf_op jit(solution)/shard_map/ppermute | solution.py:28
  140.9 23.9 %collective-permute-start.33 = (bf16[128,2048]{1,0:T(8,128)(2,1)S(1)}, bf16[128,2048]{1,0:T(8,128)(2,1)S(1)}, u32[]{:S(2)}, u32[]{:S(2)}) collective-permute-start(bf16[128,2048]{1,0:T(8,128)(2,1)S(1)} %broadcast_select_fusion.4.refs_8_), channel_id=1, source_target_pairs={{0,4},{2,6},{4,0},{6,2},{8,12},{10,14},{12,8},{14,10},{16,20},{18,... | collective-permute-start | bytes 1572872 | tf_op jit(solution)/shard_map/ppermute | solution.py:28
  141.5 19.9 %collective-permute-start.31 = (bf16[64,2048]{1,0:T(8,128)(2,1)}, bf16[64,2048]{1,0:T(8,128)(2,1)S(1)}, u32[]{:S(2)}, u32[]{:S(2)}) collective-permute-start(bf16[64,2048]{1,0:T(8,128)(2,1)} %get-tuple-element.32), channel_id=1, source_target_pairs={{0,4},{2,6},{4,0},{6,2},{8,12},{10,14},{12,8},{14,10},{16,20},{18,... | collective-permute-start | bytes 786440 | tf_op jit(solution)/shard_map/ppermute | solution.py:28
  143.0 21.8 %collective-permute-start.32 = (bf16[64,2048]{1,0:T(8,128)(2,1)}, bf16[64,2048]{1,0:T(8,128)(2,1)S(1)}, u32[]{:S(2)}, u32[]{:S(2)}) collective-permute-start(bf16[64,2048]{1,0:T(8,128)(2,1)} %get-tuple-element.39), channel_id=1, source_target_pairs={{0,4},{2,6},{4,0},{6,2},{8,12},{10,14},{12,8},{14,10},{16,20},{18,... | collective-permute-start | bytes 786440 | tf_op jit(solution)/shard_map/ppermute | solution.py:28
  143.6 21.3 %collective-permute-start.27 = (f32[8,640]{1,0:T(8,128)S(1)}, f32[8,640]{1,0:T(8,128)S(1)}, u32[]{:S(2)}, u32[]{:S(2)}) collective-permute-start(f32[8,640]{1,0:T(8,128)S(1)} %get-tuple-element.19.refs_3_), channel_id=1, source_target_pairs={{0,1},{1,0},{2,3},{3,2},{4,5},{5,4},{6,7},{7,6},{8,9},{9,8},{10,11... | collective-permute-start | bytes 61448 | tf_op jit(solution)/shard_map/ppermute | solution.py:28
  165.9 5.3 %copy-start.16 = (bf16[64,2048]{1,0:T(8,128)(2,1)S(1)}, bf16[64,2048]{1,0:T(8,128)(2,1)}, u32[]{:S(2)}) copy-start(bf16[64,2048]{1,0:T(8,128)(2,1)} %get-tuple-element.34) | copy-start | bytes 786436
  165.9 5.3 %copy-start.18 = (bf16[64,2048]{1,0:T(8,128)(2,1)S(1)}, bf16[64,2048]{1,0:T(8,128)(2,1)}, u32[]{:S(2)}) copy-start(bf16[64,2048]{1,0:T(8,128)(2,1)} %get-tuple-element.40) | copy-start | bytes 786436
  171.1 45.5 %copy-start.2 = (bf16[560,2048]{1,0:T(8,128)(2,1)S(1)}, bf16[560,2048]{1,0:T(8,128)(2,1)}, u32[]{:S(2)}) copy-start(bf16[560,2048]{1,0:T(8,128)(2,1)} %copy-done.1) | copy-start | bytes 6881284
  171.1 45.5 %copy-start.6 = (bf16[2,64,2048]{2,1,0:T(8,128)(2,1)S(1)}, bf16[2,64,2048]{2,1,0:T(8,128)(2,1)}, u32[]{:S(2)}) copy-start(bf16[2,64,2048]{2,1,0:T(8,128)(2,1)} %copy-done.5) | copy-start | bytes 1572868
  171.1 45.5 %collective-permute-start.34 = (bf16[560,2048]{1,0:T(8,128)(2,1)S(1)}, bf16[560,2048]{1,0:T(8,128)(2,1)S(1)}, u32[]{:S(2)}, u32[]{:S(2)}) collective-permute-start(bf16[560,2048]{1,0:T(8,128)(2,1)S(1)} %shard_map.67.refs_1_), channel_id=1, source_target_pairs={{0,2},{2,0},{4,6},{6,4},{8,10},{10,8},{12,14},{14,12},{16,18},{18,... | collective-permute-start | bytes 6881288 | tf_op jit(solution)/shard_map/ppermute | solution.py:28
  171.2 0.8 collective-permute-start.35
  172.1 31.6 %collective-permute-start.36 = (bf16[128,2048]{1,0:T(8,128)(2,1)S(1)}, bf16[128,2048]{1,0:T(8,128)(2,1)S(1)}, u32[]{:S(2)}, u32[]{:S(2)}) collective-permute-start(bf16[128,2048]{1,0:T(8,128)(2,1)S(1)} %collective-permute-done.35), channel_id=1, source_target_pairs={{8,0},{10,2},{12,4},{14,6},{16,24},{18,26},{20,28},{22,30},{9,1},{... | collective-permute-start | bytes 1572872 | tf_op jit(solution)/shard_map/ppermute | solution.py:28
  174.5 46.7 %copy-start.9 = (bf16[128,2048]{1,0:T(8,128)(2,1)}, bf16[128,2048]{1,0:T(8,128)(2,1)S(1)}, u32[]{:S(2)}) copy-start(bf16[128,2048]{1,0:T(8,128)(2,1)S(1)} %pad_maximum_fusion.5.refs_3_) | copy-start | bytes 1572868
  174.5 29.9 %collective-permute-start.40 = (bf16[128,2048]{1,0:T(8,128)(2,1)S(1)}, bf16[128,2048]{1,0:T(8,128)(2,1)S(1)}, u32[]{:S(2)}, u32[]{:S(2)}) collective-permute-start(bf16[128,2048]{1,0:T(8,128)(2,1)S(1)} %pad_maximum_fusion.5.refs_3_), channel_id=1, source_target_pairs={{8,16},{10,18},{12,20},{14,22},{16,8},{18,10},{20,12},{22,14},{9,1... | collective-permute-start | bytes 1572872 | tf_op jit(solution)/shard_map/ppermute | solution.py:28
  203.8 12.8 %collective-permute-start.37 = (bf16[128,2048]{1,0:T(8,128)(2,1)S(1)}, bf16[128,2048]{1,0:T(8,128)(2,1)S(1)}, u32[]{:S(2)}, u32[]{:S(2)}) collective-permute-start(bf16[128,2048]{1,0:T(8,128)(2,1)S(1)} %broadcast_select_fusion.3.refs_4_), channel_id=1, source_target_pairs={{0,4},{2,6},{4,0},{6,2},{8,12},{10,14},{12,8},{14,10},{16,20},{18,... | collective-permute-start | bytes 1572872 | tf_op jit(solution)/shard_map/ppermute | solution.py:28
  204.4 19.7 %collective-permute-start.41 = (bf16[128,2048]{1,0:T(8,128)(2,1)S(1)}, bf16[128,2048]{1,0:T(8,128)(2,1)S(1)}, u32[]{:S(2)}, u32[]{:S(2)}) collective-permute-start(bf16[128,2048]{1,0:T(8,128)(2,1)S(1)} %collective-permute-done.40), channel_id=1, source_target_pairs={{8,0},{10,2},{12,4},{14,6},{16,24},{18,26},{20,28},{22,30},{9,1},{... | collective-permute-start | bytes 1572872 | tf_op jit(solution)/shard_map/ppermute | solution.py:28
  221.2 1.4 copy-start.3
  222.6 13.6 %collective-permute-start.38 = (bf16[560,512]{1,0:T(8,128)(2,1)}, bf16[560,512]{1,0:T(8,128)(2,1)}, u32[]{:S(2)}, u32[]{:S(2)}) collective-permute-start(bf16[560,512]{1,0:T(8,128)(2,1)} %get-tuple-element.20.refs_1_), channel_id=1, source_target_pairs={{0,1},{1,0},{2,3},{3,2},{4,5},{5,4},{6,7},{7,6},{8,9},{9,8},{10,11... | collective-permute-start | bytes 1720328 | tf_op jit(solution)/shard_map/ppermute | solution.py:28
  224.1 23.0 %copy-start.4 = (bf16[560,2048]{1,0:T(8,128)(2,1)S(1)}, bf16[560,2048]{1,0:T(8,128)(2,1)}, u32[]{:S(2)}) copy-start(bf16[560,2048]{1,0:T(8,128)(2,1)} %copy-done.3) | copy-start | bytes 6881284
  224.1 23.0 %copy-start.10 = (bf16[128,2048]{1,0:T(8,128)(2,1)S(1)}, bf16[128,2048]{1,0:T(8,128)(2,1)}, u32[]{:S(2)}) copy-start(bf16[128,2048]{1,0:T(8,128)(2,1)} %copy-done.9) | copy-start | bytes 1572868
  224.1 23.0 %collective-permute-start.44 = (bf16[128,2048]{1,0:T(8,128)(2,1)S(1)}, bf16[128,2048]{1,0:T(8,128)(2,1)}, u32[]{:S(2)}, u32[]{:S(2)}) collective-permute-start(bf16[128,2048]{1,0:T(8,128)(2,1)S(1)} %broadcast_select_fusion.2.refs_4_), channel_id=1, source_target_pairs={{0,4},{2,6},{4,0},{6,2},{8,12},{10,14},{12,8},{14,10},{16,20},{18,... | collective-permute-start | bytes 1572872 | tf_op jit(solution)/shard_map/ppermute | solution.py:28
  224.8 19.6 %collective-permute-start.42 = (bf16[64,2048]{1,0:T(8,128)(2,1)}, bf16[64,2048]{1,0:T(8,128)(2,1)}, u32[]{:S(2)}, u32[]{:S(2)}) collective-permute-start(bf16[64,2048]{1,0:T(8,128)(2,1)} %get-tuple-element.30), channel_id=1, source_target_pairs={{0,4},{2,6},{4,0},{6,2},{8,12},{10,14},{12,8},{14,10},{16,20},{18,... | collective-permute-start | bytes 786440 | tf_op jit(solution)/shard_map/ppermute | solution.py:28
  226.2 20.9 %collective-permute-start.43 = (bf16[64,2048]{1,0:T(8,128)(2,1)}, bf16[64,2048]{1,0:T(8,128)(2,1)}, u32[]{:S(2)}, u32[]{:S(2)}) collective-permute-start(bf16[64,2048]{1,0:T(8,128)(2,1)} %get-tuple-element.38), channel_id=1, source_target_pairs={{0,4},{2,6},{4,0},{6,2},{8,12},{10,14},{12,8},{14,10},{16,20},{18,... | collective-permute-start | bytes 786440 | tf_op jit(solution)/shard_map/ppermute | solution.py:28
  226.8 9.4 %collective-permute-start.39 = (f32[8,640]{1,0:T(8,128)S(1)}, f32[8,640]{1,0:T(8,128)S(1)}, u32[]{:S(2)}, u32[]{:S(2)}) collective-permute-start(f32[8,640]{1,0:T(8,128)S(1)} %get-tuple-element.21.refs_3_), channel_id=1, source_target_pairs={{0,1},{1,0},{2,3},{3,2},{4,5},{5,4},{6,7},{7,6},{8,9},{9,8},{10,11... | collective-permute-start | bytes 61448 | tf_op jit(solution)/shard_map/ppermute | solution.py:28
  251.5 2.7 %collective-permute-start.45 = (bf16[256,2048]{1,0:T(8,128)(2,1)S(1)}, bf16[256,2048]{1,0:T(8,128)(2,1)S(1)}, u32[]{:S(2)}, u32[]{:S(2)}) collective-permute-start(bf16[256,2048]{1,0:T(8,128)(2,1)S(1)} %get-tuple-element.24), channel_id=1, source_target_pairs={{0,2},{2,0},{4,6},{6,4},{8,10},{10,8},{12,14},{14,12},{16,18},{18,... | collective-permute-start | bytes 3145736 | tf_op jit(solution)/shard_map/ppermute | solution.py:28
  (3 other events, 2.9 us)

commit v2 on v1

--- a/solution.py
+++ b/solution.py
@@ -275,14 +275,15 @@
     flops = 2 * total * feats * half
     cost = pl.CostEstimate(flops=flops, bytes_accessed=2 * (half * feats + 3 * total * feats), transcendentals=0)
 
+    in_hbm = lambda v: pltpu.with_memory_space_constraint(v, pltpu.HBM)
     deltas = []
     for l in range(layers):
         first, last = l == 0, l == layers - 1
         pieces = [(at, index) for _, at, index in found[2 * l]]
-        arrays = [v for v, _, _ in found[2 * l]]
+        arrays = [in_hbm(v) for v, _, _ in found[2 * l]]
         outs = [shape((total, half), bf16), shape((8, padded), jnp.float32)]
         if not first:
-            outs = [shape((total, feats), bf16)] + outs
+            outs = [pltpu.HBM((total, feats), bf16)] + outs
         results = pl.pallas_call(
             functools.partial(in_kernel, first, pieces, shard),
             out_shape=outs,
@@ -307,7 +308,7 @@
             if b < len(bits) - 1:
                 partial, squares = partial + others[0], squares + others[1]
         pieces = [(at, index) for _, at, index in found[2 * l + 1]]
-        arrays = [v for v, _, _ in found[2 * l + 1]]
+        arrays = [in_hbm(v) for v, _, _ in found[2 * l + 1]]
         operands = (place, partial, others[0], squares, others[1], group, scale[l])
         weights = pltpu.VMEM((half, feats), bf16)
         sems = pltpu.SemaphoreType.DMA((2 * nz,))
@@ -339,7 +340,7 @@
                 out_specs=[VMEM] * 2,
                 scratch_shapes=[weights, pltpu.VMEM((rows, feats), bf16), sems, pltpu.SemaphoreType.DMA],
                 **call,
-            )(place, mixed, state, *arrays)
+            )(place, mixed, in_hbm(state), *arrays)
         deltas = [results[0], move(results[-1], "sp", lambda s: s ^ 1)]
 
     return (deltas[0] + deltas[1].astype(jnp.float32)).astype(bf16)

time: 258 us -> 252 us (0.977)
  Pallas kernels: 29.9 us -> 25.6 us
    pallas_call x3, Pallas kernels: 12.7 us -> 9.38 us  [body(): pl.pallas_call(functools.partial(in_kernel, first, pieces, shard), out_sh...]
    unnamed x42 -> x72, local copies, waits for them, and re-layouts: 5.75 us -> 5 us
  transfers between devices with their start and end apart: 46 -> 46, of which waited for: 19 -> 19; matrix products, arithmetic and copies ran while one was open for 6% -> 6% of each run, Pallas kernels for 6% -> 4%
where the time goes in v2:
time: 252 us; the launch traced here: 250 us
  waiting for transfers between devices  156 us (62%)
  starting transfers between devices  44.3 us (18%)
  Pallas kernels  25.6 us (10%)
  local copies, waits for them, and re-layouts  12.2 us (5%)
  other arithmetic  10.8 us (4%)
    ppermute x46, waiting for transfers between devices, move(): lax.ppermute(value, axis, [(s, t) for s, t in pairs if t is not None])  156 us
    ppermute x46, starting transfers between devices, move(): lax.ppermute(value, axis, [(s, t) for s, t in pairs if t is not None])  44.3 us
    pallas_call x2, Pallas kernels, body(): pl.pallas_call(functools.partial(out_kernel, pieces, shard, features, hal...  9.49 us
    pallas_call x3, Pallas kernels, body(): pl.pallas_call(functools.partial(in_kernel, first, pieces, shard), out_sh...  9.38 us
  transfers between devices with their start and end apart: 46, of which 19 were waited for; matrix products, arithmetic and copies ran while one was open for 6% of the time, Pallas kernels for 4%

profile of v2, /device:TPU:4, one launch (start us, length us, event | category | flops | bytes accessed | tf_op | source)
XLA Modules:
  0.0 249.9 jit_solution(7184946809748129704)
XLA Ops:
  0.0 0.8 copy-done
  0.8 1.3 fusion
  2.2 0.9 slice_bitcast_fusion.2
  3.1 1.6 collective-permute-start.3
  4.7 1.4 collective-permute-start.4
  6.1 1.4 collective-permute-start
  7.4 1.0 slice_bitcast_fusion.6
  8.4 3.8 %collective-permute-start.14 = (bf16[1,64,2048]{2,1,0:T(8,128)(2,1)}, bf16[1,64,2048]{2,1,0:T(8,128)(2,1)S(1)}, u32[]{:S(2)}, u32[]{:S(2)}) collective-permute-start(bf16[1,64,2048]{2,1,0:T(8,128)(2,1)} %get-tuple-element.33), channel_id=1, source_target_pairs={{0,8},{2,10},{4,12},{6,14},{8,0},{10,2},{12,4},{14,6},{16,24},{18,... | collective-permute-start | bytes 786440 | tf_op jit(solution)/shard_map/ppermute | solution.py:28
  15.1 0.8 slice.84
  16.5 1.3 collective-permute-start.1
  17.8 1.5 collective-permute-done.14
  19.9 1.0 pad_maximum_fusion.1.refs_7_
  21.7 1.3 collective-permute-start.5
  23.2 13.7 %collective-permute-done.5 = bf16[64,2048]{1,0:T(8,128)(2,1)S(1)} collective-permute-done((bf16[64,2048]{1,0:T(8,128)(2,1)}, bf16[64,2048]{1,0:T(8,128)(2,1)S(1)}, u32[]{:S(2)}, u32[]{:S(2)}) %collective-permute-start.5) | collective-permute-done | bytes 262176 | tf_op jit(solution)/shard_map/ppermute | solution.py:28
  36.9 1.3 collective-permute-start.7
  38.2 8.6 %collective-permute-done.7 = bf16[64,2048]{1,0:T(8,128)(2,1)S(1)} collective-permute-done((bf16[64,2048]{1,0:T(8,128)(2,1)S(1)}, bf16[64,2048]{1,0:T(8,128)(2,1)S(1)}, u32[]{:S(2)}, u32[]{:S(2)}) %collective-permute-start.7) | collective-permute-done | bytes 262176 | tf_op jit(solution)/shard_map/ppermute | solution.py:28
  46.9 2.1 collective-permute-start.11
  49.0 1.3 collective-permute-start.16
  50.3 1.4 broadcast_select_fusion.1
  52.1 3.9 %collective-permute-done.10.refs_7_ = bf16[64,2048]{1,0:T(8,128)(2,1)S(1)} collective-permute-done((bf16[64,2048]{1,0:T(8,128)(2,1)S(1)}, bf16[64,2048]{1,0:T(8,128)(2,1)S(1)}, u32[]{:S(2)}, u32[]{:S(2)}) %collective-permute-start.10) | collective-permute-done | bytes 262176 | tf_op jit(solution)/shard_map/ppermute | solution.py:28
  56.0 5.6 %collective-permute-done.11.refs_8_ = bf16[64,2048]{1,0:T(8,128)(2,1)S(1)} collective-permute-done((bf16[64,2048]{1,0:T(8,128)(2,1)S(1)}, bf16[64,2048]{1,0:T(8,128)(2,1)S(1)}, u32[]{:S(2)}, u32[]{:S(2)}) %collective-permute-start.11) | collective-permute-done | bytes 262176 | tf_op jit(solution)/shard_map/ppermute | solution.py:28
  61.6 0.7 copy-done.28
  62.4 3.0 %shard_map.64 = (bf16[560,512]{1,0:T(8,128)(2,1)S(1)}, f32[8,640]{1,0:T(8,128)S(1)}) custom-call(bf16[560,2048]{1,0:T(8,128)(2,1)S(1)} %pad_maximum_fusion.refs_0_, bf16[64,2048]{1,0:T(8,128)(2,1)} %copy-done.16, bf16[1,64,2048]{2,1,0:T(8,128)(2,1)} %collective-permute-done.3.refs_2_, bf16[64,2048]{1,0:T(8,128)(2,1)} %copy-done.19, ...), custom_call_target="tpu_custom_call" | custom-call | flops 1174405120 | bytes 8978432 | tf_op jit(solution)/shard_map/pallas_call | solution.py:287
  65.3 1.6 collective-permute-start.12
  66.9 0.9 broadcast_select_fusion.6.refs_8_
  67.9 2.0 collective-permute-start.18
  69.9 4.5 %collective-permute-done.21 = bf16[2,64,2048]{2,1,0:T(8,128)(2,1)} collective-permute-done((bf16[2,64,2048]{2,1,0:T(8,128)(2,1)}, bf16[2,64,2048]{2,1,0:T(8,128)(2,1)}, u32[]{:S(2)}, u32[]{:S(2)}) %collective-permute-start.21) | collective-permute-done | bytes 524320 | tf_op jit(solution)/shard_map/ppermute | solution.py:28
  74.5 1.5 collective-permute-start.13
  75.9 1.8 slice_bitcast_fusion.1
  77.7 5.6 %collective-permute-done.18.refs_10_ = bf16[1,64,2048]{2,1,0:T(8,128)(2,1)S(1)} collective-permute-done((bf16[1,64,2048]{2,1,0:T(8,128)(2,1)}, bf16[1,64,2048]{2,1,0:T(8,128)(2,1)S(1)}, u32[]{:S(2)}, u32[]{:S(2)}) %collective-permute-start.18) | collective-permute-done | bytes 262176 | tf_op jit(solution)/shard_map/ppermute | solution.py:28
  84.0 4.7 %shard_map.65.refs_1_ = bf16[560,2048]{1,0:T(8,128)(2,1)S(1)} custom-call(s32[2]{0:T(128)S(1)} %pad_add_fusion.refs_0_, bf16[560,512]{1,0:T(8,128)(2,1)S(1)} %get-tuple-element.15.refs_1_, bf16[560,512]{1,0:T(8,128)(2,1)S(1)} %collective-permute-done.12.refs_2_, f32[8,640]{1,0:T(8,128)S(1)} %get-tuple-element.16.refs_3_, ...), custom_call_target="tpu_custom_call" | custom-call | flops 1174405120 | bytes 8978432 | tf_op jit(solution)/shard_map/pallas_call | solution.py:319
  89.7 1.9 collective-permute-start.28
  91.6 1.3 collective-permute-start.23
  92.9 11.1 %collective-permute-done.28 = bf16[2,64,2048]{2,1,0:T(8,128)(2,1)S(1)} collective-permute-done((bf16[2,64,2048]{2,1,0:T(8,128)(2,1)S(1)}, bf16[2,64,2048]{2,1,0:T(8,128)(2,1)S(1)}, u32[]{:S(2)}, u32[]{:S(2)}) %collective-permute-start.28) | collective-permute-done | bytes 524320 | tf_op jit(solution)/shard_map/ppermute | solution.py:28
  104.1 0.8 slice_bitcast_fusion
  104.9 1.1 pad_maximum_fusion.3.refs_7_
  107.3 10.4 %collective-permute-done.23 = bf16[128,2048]{1,0:T(8,128)(2,1)S(1)} collective-permute-done((bf16[128,2048]{1,0:T(8,128)(2,1)S(1)}, bf16[128,2048]{1,0:T(8,128)(2,1)S(1)}, u32[]{:S(2)}, u32[]{:S(2)}) %collective-permute-start.23) | collective-permute-done | bytes 524320 | tf_op jit(solution)/shard_map/ppermute | solution.py:28
  118.4 1.3 collective-permute-start.30
  119.7 1.7 collective-permute-done.24.refs_6_
  121.4 10.3 %collective-permute-done.25.refs_7_ = bf16[128,2048]{1,0:T(8,128)(2,1)S(1)} collective-permute-done((bf16[128,2048]{1,0:T(8,128)(2,1)S(1)}, bf16[128,2048]{1,0:T(8,128)(2,1)S(1)}, u32[]{:S(2)}, u32[]{:S(2)}) %collective-permute-start.25) | collective-permute-done | bytes 524320 | tf_op jit(solution)/shard_map/ppermute | solution.py:28
  131.7 0.8 copy-done.24
  132.5 3.2 %shard_map.66 = (bf16[560,2048]{1,0:T(8,128)(2,1)}, bf16[560,512]{1,0:T(8,128)(2,1)S(1)}, f32[8,640]{1,0:T(8,128)S(1)}) custom-call(bf16[560,2048]{1,0:T(8,128)(2,1)S(1)} %pad_maximum_fusion.refs_0_, bf16[560,2048]{1,0:T(8,128)(2,1)S(1)} %shard_map.65.refs_1_, bf16[560,2048]{1,0:T(8,128)(2,1)S(1)} %collective-permute-done.20.refs_2_, ...), custom_call_target="tpu_custom_call" | custom-call | flops 1174405120 | bytes 8978432 | tf_op jit(solution)/shard_map/pallas_call | solution.py:287
  137.0 1.5 collective-permute-start.31
  139.0 1.5 collective-permute-start.27
  140.6 16.3 %collective-permute-done.31.refs_9_ = bf16[64,2048]{1,0:T(8,128)(2,1)S(1)} collective-permute-done((bf16[64,2048]{1,0:T(8,128)(2,1)}, bf16[64,2048]{1,0:T(8,128)(2,1)S(1)}, u32[]{:S(2)}, u32[]{:S(2)}) %collective-permute-start.31) | collective-permute-done | bytes 262176 | tf_op jit(solution)/shard_map/ppermute | solution.py:28
  156.8 3.5 %collective-permute-done.32.refs_10_ = bf16[64,2048]{1,0:T(8,128)(2,1)S(1)} collective-permute-done((bf16[64,2048]{1,0:T(8,128)(2,1)}, bf16[64,2048]{1,0:T(8,128)(2,1)S(1)}, u32[]{:S(2)}, u32[]{:S(2)}) %collective-permute-start.32) | collective-permute-done | bytes 262176 | tf_op jit(solution)/shard_map/ppermute | solution.py:28
  161.3 4.7 %shard_map.67.refs_1_ = bf16[560,2048]{1,0:T(8,128)(2,1)S(1)} custom-call(s32[2]{0:T(128)S(1)} %pad_add_fusion.refs_0_, bf16[560,512]{1,0:T(8,128)(2,1)S(1)} %get-tuple-element.18.refs_1_, bf16[560,512]{1,0:T(8,128)(2,1)S(1)} %collective-permute-done.26.refs_2_, f32[8,640]{1,0:T(8,128)S(1)} %get-tuple-element.19.refs_3_, ...), custom_call_target="tpu_custom_call" | custom-call | flops 1174405120 | bytes 8978432 | tf_op jit(solution)/shard_map/pallas_call | solution.py:319
  166.2 0.8 collective-permute-start.35
  167.0 1.3 collective-permute-start.36
  168.3 1.1 pad_maximum_fusion.5.refs_3_
  170.1 28.5 %collective-permute-done.36 = bf16[128,2048]{1,0:T(8,128)(2,1)S(1)} collective-permute-done((bf16[128,2048]{1,0:T(8,128)(2,1)S(1)}, bf16[128,2048]{1,0:T(8,128)(2,1)S(1)}, u32[]{:S(2)}, u32[]{:S(2)}) %collective-permute-start.36) | collective-permute-done | bytes 524320 | tf_op jit(solution)/shard_map/ppermute | solution.py:28
  199.3 1.5 collective-permute-start.41
  200.8 10.7 %collective-permute-done.37.refs_7_ = bf16[128,2048]{1,0:T(8,128)(2,1)S(1)} collective-permute-done((bf16[128,2048]{1,0:T(8,128)(2,1)S(1)}, bf16[128,2048]{1,0:T(8,128)(2,1)S(1)}, u32[]{:S(2)}, u32[]{:S(2)}) %collective-permute-start.37) | collective-permute-done | bytes 524320 | tf_op jit(solution)/shard_map/ppermute | solution.py:28
  211.5 0.8 copy-done.25
  212.3 3.2 %shard_map.68 = (bf16[560,2048]{1,0:T(8,128)(2,1)}, bf16[560,512]{1,0:T(8,128)(2,1)S(1)}, f32[8,640]{1,0:T(8,128)S(1)}) custom-call(bf16[560,2048]{1,0:T(8,128)(2,1)S(1)} %copy-done.1, bf16[560,2048]{1,0:T(8,128)(2,1)S(1)} %shard_map.67.refs_1_, bf16[560,2048]{1,0:T(8,128)(2,1)S(1)} %collective-permute-done.34.refs_2_, bf16[128,2048]{1,0:T(8,128)(2,1)} %copy-done.11, ...), custom_call_target="tpu_custom_call" | custom-call | flops 1174405120 | bytes 8978432 | tf_op jit(solution)/shard_map/pallas_call | solution.py:287
  215.5 1.6 collective-permute-start.38
  217.8 1.5 collective-permute-start.42
  220.4 8.5 %collective-permute-done.39.refs_4_ = f32[8,640]{1,0:T(8,128)S(1)} collective-permute-done((f32[8,640]{1,0:T(8,128)S(1)}, f32[8,640]{1,0:T(8,128)S(1)}, u32[]{:S(2)}, u32[]{:S(2)}) %collective-permute-start.39) | collective-permute-done | bytes 20512 | tf_op jit(solution)/shard_map/ppermute | solution.py:28
  229.0 1.8 shard_map.69.refs_1_
  230.8 6.5 %collective-permute-done.42.refs_5_ = bf16[64,2048]{1,0:T(8,128)(2,1)S(1)} collective-permute-done((bf16[64,2048]{1,0:T(8,128)(2,1)}, bf16[64,2048]{1,0:T(8,128)(2,1)S(1)}, u32[]{:S(2)}, u32[]{:S(2)}) %collective-permute-start.42) | collective-permute-done | bytes 262176 | tf_op jit(solution)/shard_map/ppermute | solution.py:28
  237.3 2.8 %collective-permute-done.43.refs_6_ = bf16[64,2048]{1,0:T(8,128)(2,1)S(1)} collective-permute-done((bf16[64,2048]{1,0:T(8,128)(2,1)}, bf16[64,2048]{1,0:T(8,128)(2,1)S(1)}, u32[]{:S(2)}, u32[]{:S(2)}) %collective-permute-start.43) | collective-permute-done | bytes 262176 | tf_op jit(solution)/shard_map/ppermute | solution.py:28
  241.0 4.9 %shard_map.70 = (f32[256,2048]{1,0:T(8,128)S(1)}, bf16[256,2048]{1,0:T(8,128)(2,1)S(1)}) custom-call(s32[2]{0:T(128)S(1)} %pad_add_fusion.refs_0_, bf16[560,512]{1,0:T(8,128)(2,1)S(1)} %shard_map.69.refs_1_, bf16[560,2048]{1,0:T(8,128)(2,1)} %get-tuple-element.22.refs_2_, bf16[128,2048]{1,0:T(8,128)(2,1)} %copy-done.7, bf16[128,2048]{1,0:T(8,128)(2,1)} %copy-done.10, ...), custom_call_target="tpu_custom_call" | custom-call | flops 1174405120 | bytes 8978432 | tf_op jit(solution)/shard_map/pallas_call | solution.py:336
  246.0 2.6 %collective-permute-done.45 = bf16[256,2048]{1,0:T(8,128)(2,1)S(1)} collective-permute-done((bf16[256,2048]{1,0:T(8,128)(2,1)S(1)}, bf16[256,2048]{1,0:T(8,128)(2,1)S(1)}, u32[]{:S(2)}, u32[]{:S(2)}) %collective-permute-start.45) | collective-permute-done | bytes 1048608 | tf_op jit(solution)/shard_map/ppermute | solution.py:28
  248.7 1.3 add_convert_fusion
  (150 shorter events, 16.4 us)
Async XLA Ops:
  0.0 6.0 %copy-start.15 = (bf16[256,2048]{1,0:T(8,128)(2,1)S(1)}, bf16[256,2048]{1,0:T(8,128)(2,1)}, u32[]{:S(2)}) copy-start(bf16[256,2048]{1,0:T(8,128)(2,1)} %param.6) | copy-start | bytes 3145732
  0.0 7.4 %copy-start.3 = (bf16[3,64,2048]{2,1,0:T(8,128)(2,1)S(1)}, bf16[3,64,2048]{2,1,0:T(8,128)(2,1)}, u32[]{:S(2)}) copy-start(bf16[3,64,2048]{2,1,0:T(8,128)(2,1)} %param.10) | copy-start | bytes 2359300
  2.1 12.2 %copy-start.35 = (f32[3,1024]{1,0:T(4,128)S(1)}, f32[3,1024]{1,0:T(4,128)}, u32[]{:S(2)}) copy-start(f32[3,1024]{1,0:T(4,128)} %param.9) | copy-start | bytes 36868
  3.1 17.8 %copy-start.16 = (bf16[64,2048]{1,0:T(8,128)(2,1)}, bf16[64,2048]{1,0:T(8,128)(2,1)S(1)}, u32[]{:S(2)}) copy-start(bf16[64,2048]{1,0:T(8,128)(2,1)S(1)} %get-tuple-element.35.refs_1_) | copy-start | bytes 786436
  3.1 13.4 %collective-permute-start.3 = (bf16[1,64,2048]{2,1,0:T(8,128)(2,1)S(1)}, bf16[1,64,2048]{2,1,0:T(8,128)(2,1)}, u32[]{:S(2)}, u32[]{:S(2)}) collective-permute-start(bf16[1,64,2048]{2,1,0:T(8,128)(2,1)S(1)} %get-tuple-element.37), channel_id=1, source_target_pairs={{0,8},{2,10},{4,12},{6,14},{8,0},{10,2},{12,4},{14,6},{16,24},{18,... | collective-permute-start | bytes 786440 | tf_op jit(solution)/shard_map/ppermute | solution.py:28
  4.7 16.3 %collective-permute-start.4 = (bf16[64,2048]{1,0:T(8,128)(2,1)S(1)}, bf16[64,2048]{1,0:T(8,128)(2,1)}, u32[]{:S(2)}, u32[]{:S(2)}) collective-permute-start(bf16[64,2048]{1,0:T(8,128)(2,1)S(1)} %get-tuple-element.35.refs_1_), channel_id=1, source_target_pairs={{8,16},{10,18},{12,20},{14,22},{16,8},{18,10},{20,12},{22,14},{9,1... | collective-permute-start | bytes 786440 | tf_op jit(solution)/shard_map/ppermute | solution.py:28
  6.0 42.9 %collective-permute-start.2 = (bf16[256,2048]{1,0:T(8,128)(2,1)S(1)}, bf16[256,2048]{1,0:T(8,128)(2,1)}, u32[]{:S(2)}, u32[]{:S(2)}) collective-permute-start(bf16[256,2048]{1,0:T(8,128)(2,1)S(1)} %copy-done.15), channel_id=1, source_target_pairs={{0,2},{2,0},{4,6},{6,4},{8,10},{10,8},{12,14},{14,12},{16,18},{18,... | collective-permute-start | bytes 3145736 | tf_op jit(solution)/shard_map/ppermute | solution.py:28
  6.1 9.9 %collective-permute-start = (bf16[48,2048]{1,0:T(8,128)(2,1)S(1)}, bf16[48,2048]{1,0:T(8,128)(2,1)}, u32[]{:S(2)}, u32[]{:S(2)}) collective-permute-start(bf16[48,2048]{1,0:T(8,128)(2,1)S(1)} %slice.63), channel_id=1, source_target_pairs={{2,6},{6,10},{10,14},{14,18},{18,22},{22,26},{26,30},{3,7},{7,11},... | collective-permute-start | bytes 589832 | tf_op jit(solution)/shard_map/ppermute | solution.py:28
  8.4 10.8 %collective-permute-start.14 = (bf16[1,64,2048]{2,1,0:T(8,128)(2,1)}, bf16[1,64,2048]{2,1,0:T(8,128)(2,1)S(1)}, u32[]{:S(2)}, u32[]{:S(2)}) collective-permute-start(bf16[1,64,2048]{2,1,0:T(8,128)(2,1)} %get-tuple-element.33), channel_id=1, source_target_pairs={{0,8},{2,10},{4,12},{6,14},{8,0},{10,2},{12,4},{14,6},{16,24},{18,... | collective-permute-start | bytes 786440 | tf_op jit(solution)/shard_map/ppermute | solution.py:28
  16.0 40.0 %collective-permute-start.8 = (bf16[3,64,2048]{2,1,0:T(8,128)(2,1)S(1)}, bf16[3,64,2048]{2,1,0:T(8,128)(2,1)S(1)}, u32[]{:S(2)}, u32[]{:S(2)}) collective-permute-start(bf16[3,64,2048]{2,1,0:T(8,128)(2,1)S(1)} %fusion), channel_id=1, source_target_pairs={{0,4},{2,6},{4,0},{6,2},{8,12},{10,14},{12,8},{14,10},{16,20},{18,... | collective-permute-start | bytes 2359304 | tf_op jit(solution)/shard_map/ppermute | solution.py:28
  16.5 5.2 %collective-permute-start.1 = (bf16[48,2048]{1,0:T(8,128)(2,1)}, bf16[48,2048]{1,0:T(8,128)(2,1)S(1)}, u32[]{:S(2)}, u32[]{:S(2)}) collective-permute-start(bf16[48,2048]{1,0:T(8,128)(2,1)} %collective-permute-done), channel_id=1, source_target_pairs={{2,0},{6,4},{10,8},{14,12},{18,16},{22,20},{26,24},{30,28},{3,1},{... | collective-permute-start | bytes 589832 | tf_op jit(solution)/shard_map/ppermute | solution.py:28
  19.2 32.4 %copy-start.34 = (bf16[1,64,2048]{2,1,0:T(8,128)(2,1)}, bf16[1,64,2048]{2,1,0:T(8,128)(2,1)S(1)}, u32[]{:S(2)}) copy-start(bf16[1,64,2048]{2,1,0:T(8,128)(2,1)S(1)} %collective-permute-done.14) | copy-start | bytes 786436
  19.2 3.8 %collective-permute-start.6 = (bf16[64,2048]{1,0:T(8,128)(2,1)}, bf16[64,2048]{1,0:T(8,128)(2,1)S(1)}, u32[]{:S(2)}, u32[]{:S(2)}) collective-permute-start(bf16[64,2048]{1,0:T(8,128)(2,1)} %bitcast.4), channel_id=1, source_target_pairs={{8,16},{10,18},{12,20},{14,22},{16,8},{18,10},{20,12},{22,14},{9,1... | collective-permute-start | bytes 786440 | tf_op jit(solution)/shard_map/ppermute | solution.py:28
  20.9 30.7 %copy-start.6 = (bf16[128,2048]{1,0:T(8,128)(2,1)}, bf16[128,2048]{1,0:T(8,128)(2,1)S(1)}, u32[]{:S(2)}) copy-start(bf16[128,2048]{1,0:T(8,128)(2,1)S(1)} %pad_maximum_fusion.1.refs_7_) | copy-start | bytes 1572868
  20.9 25.9 %collective-permute-start.15 = (bf16[128,2048]{1,0:T(8,128)(2,1)S(1)}, bf16[128,2048]{1,0:T(8,128)(2,1)S(1)}, u32[]{:S(2)}, u32[]{:S(2)}) collective-permute-start(bf16[128,2048]{1,0:T(8,128)(2,1)S(1)} %pad_maximum_fusion.1.refs_7_), channel_id=1, source_target_pairs={{8,16},{10,18},{12,20},{14,22},{16,8},{18,10},{20,12},{22,14},{9,1... | collective-permute-start | bytes 1572872 | tf_op jit(solution)/shard_map/ppermute | solution.py:28
  21.7 15.2 %collective-permute-start.5 = (bf16[64,2048]{1,0:T(8,128)(2,1)}, bf16[64,2048]{1,0:T(8,128)(2,1)S(1)}, u32[]{:S(2)}, u32[]{:S(2)}) collective-permute-start(bf16[64,2048]{1,0:T(8,128)(2,1)} %collective-permute-done.4), channel_id=1, source_target_pairs={{8,0},{10,2},{12,4},{14,6},{16,24},{18,26},{20,28},{22,30},{9,1},{... | collective-permute-start | bytes 786440 | tf_op jit(solution)/shard_map/ppermute | solution.py:28
  23.0 28.9 %collective-permute-start.9 = (bf16[1,64,2048]{2,1,0:T(8,128)(2,1)}, bf16[1,64,2048]{2,1,0:T(8,128)(2,1)S(1)}, u32[]{:S(2)}, u32[]{:S(2)}) collective-permute-start(bf16[1,64,2048]{2,1,0:T(8,128)(2,1)} %collective-permute-done.3.refs_2_), channel_id=1, source_target_pairs={{0,4},{2,6},{4,0},{6,2},{8,12},{10,14},{12,8},{14,10},{16,20},{18,... | collective-permute-start | bytes 786440 | tf_op jit(solution)/shard_map/ppermute | solution.py:28
  36.9 9.9 %collective-permute-start.7 = (bf16[64,2048]{1,0:T(8,128)(2,1)S(1)}, bf16[64,2048]{1,0:T(8,128)(2,1)S(1)}, u32[]{:S(2)}, u32[]{:S(2)}) collective-permute-start(bf16[64,2048]{1,0:T(8,128)(2,1)S(1)} %collective-permute-done.6), channel_id=1, source_target_pairs={{8,0},{10,2},{12,4},{14,6},{16,24},{18,26},{20,28},{22,30},{9,1},{... | collective-permute-start | bytes 786440 | tf_op jit(solution)/shard_map/ppermute | solution.py:28
  38.2 13.4 %copy-start.19 = (bf16[64,2048]{1,0:T(8,128)(2,1)}, bf16[64,2048]{1,0:T(8,128)(2,1)S(1)}, u32[]{:S(2)}) copy-start(bf16[64,2048]{1,0:T(8,128)(2,1)S(1)} %broadcast_select_fusion.8.refs_3_) | copy-start | bytes 786436
  46.8 9.2 %collective-permute-start.10 = (bf16[64,2048]{1,0:T(8,128)(2,1)S(1)}, bf16[64,2048]{1,0:T(8,128)(2,1)S(1)}, u32[]{:S(2)}, u32[]{:S(2)}) collective-permute-start(bf16[64,2048]{1,0:T(8,128)(2,1)S(1)} %broadcast_select_fusion.8.refs_3_), channel_id=1, source_target_pairs={{0,4},{2,6},{4,0},{6,2},{8,12},{10,14},{12,8},{14,10},{16,20},{18,... | collective-permute-start | bytes 786440 | tf_op jit(solution)/shard_map/ppermute | solution.py:28
  46.9 14.7 %collective-permute-start.11 = (bf16[64,2048]{1,0:T(8,128)(2,1)S(1)}, bf16[64,2048]{1,0:T(8,128)(2,1)S(1)}, u32[]{:S(2)}, u32[]{:S(2)}) collective-permute-start(bf16[64,2048]{1,0:T(8,128)(2,1)S(1)} %broadcast_select_fusion.7.refs_4_), channel_id=1, source_target_pairs={{0,4},{2,6},{4,0},{6,2},{8,12},{10,14},{12,8},{14,10},{16,20},{18,... | collective-permute-start | bytes 786440 | tf_op jit(solution)/shard_map/ppermute | solution.py:28
  49.0 17.9 %collective-permute-start.16 = (bf16[128,2048]{1,0:T(8,128)(2,1)S(1)}, bf16[128,2048]{1,0:T(8,128)(2,1)S(1)}, u32[]{:S(2)}, u32[]{:S(2)}) collective-permute-start(bf16[128,2048]{1,0:T(8,128)(2,1)S(1)} %collective-permute-done.15), channel_id=1, source_target_pairs={{8,0},{10,2},{12,4},{14,6},{16,24},{18,26},{20,28},{22,30},{9,1},{... | collective-permute-start | bytes 1572872 | tf_op jit(solution)/shard_map/ppermute | solution.py:28
  52.0 9.7 %copy-start.26 = (bf16[1,64,2048]{2,1,0:T(8,128)(2,1)}, bf16[1,64,2048]{2,1,0:T(8,128)(2,1)S(1)}, u32[]{:S(2)}) copy-start(bf16[1,64,2048]{2,1,0:T(8,128)(2,1)S(1)} %collective-permute-done.9.refs_6_) | copy-start | bytes 786436
  52.0 25.8 %collective-permute-start.17 = (bf16[64,2048]{1,0:T(8,128)(2,1)}, bf16[64,2048]{1,0:T(8,128)(2,1)}, u32[]{:S(2)}, u32[]{:S(2)}) collective-permute-start(bf16[64,2048]{1,0:T(8,128)(2,1)} %get-tuple-element.31), channel_id=1, source_target_pairs={{0,4},{2,6},{4,0},{6,2},{8,12},{10,14},{12,8},{14,10},{16,20},{18,... | collective-permute-start | bytes 786440 | tf_op jit(solution)/shard_map/ppermute | solution.py:28
  56.0 18.5 %collective-permute-start.21 = (bf16[2,64,2048]{2,1,0:T(8,128)(2,1)}, bf16[2,64,2048]{2,1,0:T(8,128)(2,1)}, u32[]{:S(2)}, u32[]{:S(2)}) collective-permute-start(bf16[2,64,2048]{2,1,0:T(8,128)(2,1)} %slice.84), channel_id=1, source_target_pairs={{0,8},{2,10},{4,12},{6,14},{8,0},{10,2},{12,4},{14,6},{16,24},{18,... | collective-permute-start | bytes 1572872 | tf_op jit(solution)/shard_map/ppermute | solution.py:28
  65.3 18.0 %collective-permute-start.12 = (bf16[560,512]{1,0:T(8,128)(2,1)S(1)}, bf16[560,512]{1,0:T(8,128)(2,1)S(1)}, u32[]{:S(2)}, u32[]{:S(2)}) collective-permute-start(bf16[560,512]{1,0:T(8,128)(2,1)S(1)} %get-tuple-element.15.refs_1_), channel_id=1, source_target_pairs={{0,1},{1,0},{2,3},{3,2},{4,5},{5,4},{6,7},{7,6},{8,9},{9,8},{10,11... | collective-permute-start | bytes 1720328 | tf_op jit(solution)/shard_map/ppermute | solution.py:28
  67.8 15.6 %collective-permute-start.19 = (bf16[128,2048]{1,0:T(8,128)(2,1)}, bf16[128,2048]{1,0:T(8,128)(2,1)}, u32[]{:S(2)}, u32[]{:S(2)}) collective-permute-start(bf16[128,2048]{1,0:T(8,128)(2,1)} %broadcast_select_fusion.6.refs_8_), channel_id=1, source_target_pairs={{0,4},{2,6},{4,0},{6,2},{8,12},{10,14},{12,8},{14,10},{16,20},{18,... | collective-permute-start | bytes 1572872 | tf_op jit(solution)/shard_map/ppermute | solution.py:28
  67.9 15.4 %collective-permute-start.18 = (bf16[1,64,2048]{2,1,0:T(8,128)(2,1)}, bf16[1,64,2048]{2,1,0:T(8,128)(2,1)S(1)}, u32[]{:S(2)}, u32[]{:S(2)}) collective-permute-start(bf16[1,64,2048]{2,1,0:T(8,128)(2,1)} %copy-done.34), channel_id=1, source_target_pairs={{0,4},{2,6},{4,0},{6,2},{8,12},{10,14},{12,8},{14,10},{16,20},{18,... | collective-permute-start | bytes 786440 | tf_op jit(solution)/shard_map/ppermute | solution.py:28
  74.5 8.8 %collective-permute-start.13 = (f32[8,640]{1,0:T(8,128)S(1)}, f32[8,640]{1,0:T(8,128)S(1)}, u32[]{:S(2)}, u32[]{:S(2)}) collective-permute-start(f32[8,640]{1,0:T(8,128)S(1)} %get-tuple-element.16.refs_3_), channel_id=1, source_target_pairs={{0,1},{1,0},{2,3},{3,2},{4,5},{5,4},{6,7},{7,6},{8,9},{9,8},{10,11... | collective-permute-start | bytes 61448 | tf_op jit(solution)/shard_map/ppermute | solution.py:28
  88.8 42.9 %collective-permute-start.20 = (bf16[560,2048]{1,0:T(8,128)(2,1)S(1)}, bf16[560,2048]{1,0:T(8,128)(2,1)S(1)}, u32[]{:S(2)}, u32[]{:S(2)}) collective-permute-start(bf16[560,2048]{1,0:T(8,128)(2,1)S(1)} %shard_map.65.refs_1_), channel_id=1, source_target_pairs={{0,2},{2,0},{4,6},{6,4},{8,10},{10,8},{12,14},{14,12},{16,18},{18,... | collective-permute-start | bytes 6881288 | tf_op jit(solution)/shard_map/ppermute | solution.py:28
  88.9 28.8 %copy-start.9 = (bf16[128,2048]{1,0:T(8,128)(2,1)}, bf16[128,2048]{1,0:T(8,128)(2,1)S(1)}, u32[]{:S(2)}) copy-start(bf16[128,2048]{1,0:T(8,128)(2,1)S(1)} %pad_maximum_fusion.2.refs_3_) | copy-start | bytes 1572868
  88.9 2.7 %collective-permute-start.22 = (bf16[128,2048]{1,0:T(8,128)(2,1)S(1)}, bf16[128,2048]{1,0:T(8,128)(2,1)S(1)}, u32[]{:S(2)}, u32[]{:S(2)}) collective-permute-start(bf16[128,2048]{1,0:T(8,128)(2,1)S(1)} %pad_maximum_fusion.2.refs_3_), channel_id=1, source_target_pairs={{8,16},{10,18},{12,20},{14,22},{16,8},{18,10},{20,12},{22,14},{9,1... | collective-permute-start | bytes 1572872 | tf_op jit(solution)/shard_map/ppermute | solution.py:28
  89.7 14.4 %collective-permute-start.28 = (bf16[2,64,2048]{2,1,0:T(8,128)(2,1)S(1)}, bf16[2,64,2048]{2,1,0:T(8,128)(2,1)S(1)}, u32[]{:S(2)}, u32[]{:S(2)}) collective-permute-start(bf16[2,64,2048]{2,1,0:T(8,128)(2,1)S(1)} %slice.72), channel_id=1, source_target_pairs={{0,8},{2,10},{4,12},{6,14},{8,0},{10,2},{12,4},{14,6},{16,24},{18,... | collective-permute-start | bytes 1572872 | tf_op jit(solution)/shard_map/ppermute | solution.py:28
  91.6 26.0 %collective-permute-start.23 = (bf16[128,2048]{1,0:T(8,128)(2,1)S(1)}, bf16[128,2048]{1,0:T(8,128)(2,1)S(1)}, u32[]{:S(2)}, u32[]{:S(2)}) collective-permute-start(bf16[128,2048]{1,0:T(8,128)(2,1)S(1)} %collective-permute-done.22), channel_id=1, source_target_pairs={{8,0},{10,2},{12,4},{14,6},{16,24},{18,26},{20,28},{22,30},{9,1},{... | collective-permute-start | bytes 1572872 | tf_op jit(solution)/shard_map/ppermute | solution.py:28
  106.0 25.7 %copy-start.8 = (bf16[128,2048]{1,0:T(8,128)(2,1)}, bf16[128,2048]{1,0:T(8,128)(2,1)S(1)}, u32[]{:S(2)}) copy-start(bf16[128,2048]{1,0:T(8,128)(2,1)S(1)} %pad_maximum_fusion.3.refs_7_) | copy-start | bytes 1572868
  106.0 12.4 %collective-permute-start.29 = (bf16[128,2048]{1,0:T(8,128)(2,1)S(1)}, bf16[128,2048]{1,0:T(8,128)(2,1)S(1)}, u32[]{:S(2)}, u32[]{:S(2)}) collective-permute-start(bf16[128,2048]{1,0:T(8,128)(2,1)S(1)} %pad_maximum_fusion.3.refs_7_), channel_id=1, source_target_pairs={{8,16},{10,18},{12,20},{14,22},{16,8},{18,10},{20,12},{22,14},{9,1... | collective-permute-start | bytes 1572872 | tf_op jit(solution)/shard_map/ppermute | solution.py:28
  106.7 14.7 %collective-permute-start.24 = (bf16[2,64,2048]{2,1,0:T(8,128)(2,1)}, bf16[2,64,2048]{2,1,0:T(8,128)(2,1)S(1)}, u32[]{:S(2)}, u32[]{:S(2)}) collective-permute-start(bf16[2,64,2048]{2,1,0:T(8,128)(2,1)} %collective-permute-done.21), channel_id=1, source_target_pairs={{0,4},{2,6},{4,0},{6,2},{8,12},{10,14},{12,8},{14,10},{16,20},{18,... | collective-permute-start | bytes 1572872 | tf_op jit(solution)/shard_map/ppermute | solution.py:28
  117.7 13.9 %copy-start.13 = (bf16[128,2048]{1,0:T(8,128)(2,1)}, bf16[128,2048]{1,0:T(8,128)(2,1)S(1)}, u32[]{:S(2)}) copy-start(bf16[128,2048]{1,0:T(8,128)(2,1)S(1)} %broadcast_select_fusion.5.refs_4_) | copy-start | bytes 1572868
  117.8 13.9 %collective-permute-start.25 = (bf16[128,2048]{1,0:T(8,128)(2,1)S(1)}, bf16[128,2048]{1,0:T(8,128)(2,1)S(1)}, u32[]{:S(2)}, u32[]{:S(2)}) collective-permute-start(bf16[128,2048]{1,0:T(8,128)(2,1)S(1)} %broadcast_select_fusion.5.refs_4_), channel_id=1, source_target_pairs={{0,4},{2,6},{4,0},{6,2},{8,12},{10,14},{12,8},{14,10},{16,20},{18,... | collective-permute-start | bytes 1572872 | tf_op jit(solution)/shard_map/ppermute | solution.py:28
  118.4 17.9 %collective-permute-start.30 = (bf16[128,2048]{1,0:T(8,128)(2,1)S(1)}, bf16[128,2048]{1,0:T(8,128)(2,1)S(1)}, u32[]{:S(2)}, u32[]{:S(2)}) collective-permute-start(bf16[128,2048]{1,0:T(8,128)(2,1)S(1)} %collective-permute-done.29), channel_id=1, source_target_pairs={{8,0},{10,2},{12,4},{14,6},{16,24},{18,26},{20,28},{22,30},{9,1},{... | collective-permute-start | bytes 1572872 | tf_op jit(solution)/shard_map/ppermute | solution.py:28
  121.4 10.3 %copy-start.5 = (bf16[2,64,2048]{2,1,0:T(8,128)(2,1)}, bf16[2,64,2048]{2,1,0:T(8,128)(2,1)S(1)}, u32[]{:S(2)}) copy-start(bf16[2,64,2048]{2,1,0:T(8,128)(2,1)S(1)} %collective-permute-done.24.refs_6_) | copy-start | bytes 1572868
  135.7 24.7 %collective-permute-start.26 = (bf16[560,512]{1,0:T(8,128)(2,1)S(1)}, bf16[560,512]{1,0:T(8,128)(2,1)S(1)}, u32[]{:S(2)}, u32[]{:S(2)}) collective-permute-start(bf16[560,512]{1,0:T(8,128)(2,1)S(1)} %get-tuple-element.18.refs_1_), channel_id=1, source_target_pairs={{0,1},{1,0},{2,3},{3,2},{4,5},{5,4},{6,7},{7,6},{8,9},{9,8},{10,11... | collective-permute-start | bytes 1720328 | tf_op jit(solution)/shard_map/ppermute | solution.py:28
  136.4 24.0 %copy-start.12 = (bf16[128,2048]{1,0:T(8,128)(2,1)}, bf16[128,2048]{1,0:T(8,128)(2,1)S(1)}, u32[]{:S(2)}) copy-start(bf16[128,2048]{1,0:T(8,128)(2,1)S(1)} %broadcast_select_fusion.4.refs_8_) | copy-start | bytes 1572868
  136.4 24.0 %collective-permute-start.33 = (bf16[128,2048]{1,0:T(8,128)(2,1)S(1)}, bf16[128,2048]{1,0:T(8,128)(2,1)S(1)}, u32[]{:S(2)}, u32[]{:S(2)}) collective-permute-start(bf16[128,2048]{1,0:T(8,128)(2,1)S(1)} %broadcast_select_fusion.4.refs_8_), channel_id=1, source_target_pairs={{0,4},{2,6},{4,0},{6,2},{8,12},{10,14},{12,8},{14,10},{16,20},{18,... | collective-permute-start | bytes 1572872 | tf_op jit(solution)/shard_map/ppermute | solution.py:28
  137.0 19.8 %collective-permute-start.31 = (bf16[64,2048]{1,0:T(8,128)(2,1)}, bf16[64,2048]{1,0:T(8,128)(2,1)S(1)}, u32[]{:S(2)}, u32[]{:S(2)}) collective-permute-start(bf16[64,2048]{1,0:T(8,128)(2,1)} %get-tuple-element.32), channel_id=1, source_target_pairs={{0,4},{2,6},{4,0},{6,2},{8,12},{10,14},{12,8},{14,10},{16,20},{18,... | collective-permute-start | bytes 786440 | tf_op jit(solution)/shard_map/ppermute | solution.py:28
  138.5 21.9 %collective-permute-start.32 = (bf16[64,2048]{1,0:T(8,128)(2,1)}, bf16[64,2048]{1,0:T(8,128)(2,1)S(1)}, u32[]{:S(2)}, u32[]{:S(2)}) collective-permute-start(bf16[64,2048]{1,0:T(8,128)(2,1)} %get-tuple-element.39), channel_id=1, source_target_pairs={{0,4},{2,6},{4,0},{6,2},{8,12},{10,14},{12,8},{14,10},{16,20},{18,... | collective-permute-start | bytes 786440 | tf_op jit(solution)/shard_map/ppermute | solution.py:28
  139.0 21.3 %collective-permute-start.27 = (f32[8,640]{1,0:T(8,128)S(1)}, f32[8,640]{1,0:T(8,128)S(1)}, u32[]{:S(2)}, u32[]{:S(2)}) collective-permute-start(f32[8,640]{1,0:T(8,128)S(1)} %get-tuple-element.19.refs_3_), channel_id=1, source_target_pairs={{0,1},{1,0},{2,3},{3,2},{4,5},{5,4},{6,7},{7,6},{8,9},{9,8},{10,11... | collective-permute-start | bytes 61448 | tf_op jit(solution)/shard_map/ppermute | solution.py:28
  166.0 46.3 %copy-start.1 = (bf16[560,2048]{1,0:T(8,128)(2,1)S(1)}, bf16[560,2048]{1,0:T(8,128)(2,1)}, u32[]{:S(2)}) copy-start(bf16[560,2048]{1,0:T(8,128)(2,1)} %get-tuple-element.17.refs_0_) | copy-start | bytes 6881284
  166.0 45.5 %collective-permute-start.34 = (bf16[560,2048]{1,0:T(8,128)(2,1)S(1)}, bf16[560,2048]{1,0:T(8,128)(2,1)S(1)}, u32[]{:S(2)}, u32[]{:S(2)}) collective-permute-start(bf16[560,2048]{1,0:T(8,128)(2,1)S(1)} %shard_map.67.refs_1_), channel_id=1, source_target_pairs={{0,2},{2,0},{4,6},{6,4},{8,10},{10,8},{12,14},{14,12},{16,18},{18,... | collective-permute-start | bytes 6881288 | tf_op jit(solution)/shard_map/ppermute | solution.py:28
  166.2 45.3 %copy-start.11 = (bf16[128,2048]{1,0:T(8,128)(2,1)}, bf16[128,2048]{1,0:T(8,128)(2,1)S(1)}, u32[]{:S(2)}) copy-start(bf16[128,2048]{1,0:T(8,128)(2,1)S(1)} %pad_maximum_fusion.4.refs_3_) | copy-start | bytes 1572868
  166.2 0.8 collective-permute-start.35
  167.0 31.6 %collective-permute-start.36 = (bf16[128,2048]{1,0:T(8,128)(2,1)S(1)}, bf16[128,2048]{1,0:T(8,128)(2,1)S(1)}, u32[]{:S(2)}, u32[]{:S(2)}) collective-permute-start(bf16[128,2048]{1,0:T(8,128)(2,1)S(1)} %collective-permute-done.35), channel_id=1, source_target_pairs={{8,0},{10,2},{12,4},{14,6},{16,24},{18,26},{20,28},{22,30},{9,1},{... | collective-permute-start | bytes 1572872 | tf_op jit(solution)/shard_map/ppermute | solution.py:28
  169.4 46.1 %copy-start.7 = (bf16[128,2048]{1,0:T(8,128)(2,1)}, bf16[128,2048]{1,0:T(8,128)(2,1)S(1)}, u32[]{:S(2)}) copy-start(bf16[128,2048]{1,0:T(8,128)(2,1)S(1)} %pad_maximum_fusion.5.refs_3_) | copy-start | bytes 1572868
  169.4 29.9 %collective-permute-start.40 = (bf16[128,2048]{1,0:T(8,128)(2,1)S(1)}, bf16[128,2048]{1,0:T(8,128)(2,1)S(1)}, u32[]{:S(2)}, u32[]{:S(2)}) collective-permute-start(bf16[128,2048]{1,0:T(8,128)(2,1)S(1)} %pad_maximum_fusion.5.refs_3_), channel_id=1, source_target_pairs={{8,16},{10,18},{12,20},{14,22},{16,8},{18,10},{20,12},{22,14},{9,1... | collective-permute-start | bytes 1572872 | tf_op jit(solution)/shard_map/ppermute | solution.py:28
  198.7 12.8 %copy-start.14 = (bf16[128,2048]{1,0:T(8,128)(2,1)}, bf16[128,2048]{1,0:T(8,128)(2,1)S(1)}, u32[]{:S(2)}) copy-start(bf16[128,2048]{1,0:T(8,128)(2,1)S(1)} %broadcast_select_fusion.3.refs_4_) | copy-start | bytes 1572868
  198.7 12.8 %collective-permute-start.37 = (bf16[128,2048]{1,0:T(8,128)(2,1)S(1)}, bf16[128,2048]{1,0:T(8,128)(2,1)S(1)}, u32[]{:S(2)}, u32[]{:S(2)}) collective-permute-start(bf16[128,2048]{1,0:T(8,128)(2,1)S(1)} %broadcast_select_fusion.3.refs_4_), channel_id=1, source_target_pairs={{0,4},{2,6},{4,0},{6,2},{8,12},{10,14},{12,8},{14,10},{16,20},{18,... | collective-permute-start | bytes 1572872 | tf_op jit(solution)/shard_map/ppermute | solution.py:28
  199.3 17.8 %collective-permute-start.41 = (bf16[128,2048]{1,0:T(8,128)(2,1)S(1)}, bf16[128,2048]{1,0:T(8,128)(2,1)S(1)}, u32[]{:S(2)}, u32[]{:S(2)}) collective-permute-start(bf16[128,2048]{1,0:T(8,128)(2,1)S(1)} %collective-permute-done.40), channel_id=1, source_target_pairs={{8,0},{10,2},{12,4},{14,6},{16,24},{18,26},{20,28},{22,30},{9,1},{... | collective-permute-start | bytes 1572872 | tf_op jit(solution)/shard_map/ppermute | solution.py:28
  215.5 13.4 %collective-permute-start.38 = (bf16[560,512]{1,0:T(8,128)(2,1)S(1)}, bf16[560,512]{1,0:T(8,128)(2,1)S(1)}, u32[]{:S(2)}, u32[]{:S(2)}) collective-permute-start(bf16[560,512]{1,0:T(8,128)(2,1)S(1)} %get-tuple-element.20.refs_1_), channel_id=1, source_target_pairs={{0,1},{1,0},{2,3},{3,2},{4,5},{5,4},{6,7},{7,6},{8,9},{9,8},{10,11... | collective-permute-start | bytes 1720328 | tf_op jit(solution)/shard_map/ppermute | solution.py:28
  217.2 22.9 %copy-start.10 = (bf16[128,2048]{1,0:T(8,128)(2,1)}, bf16[128,2048]{1,0:T(8,128)(2,1)S(1)}, u32[]{:S(2)}) copy-start(bf16[128,2048]{1,0:T(8,128)(2,1)S(1)} %broadcast_select_fusion.2.refs_4_) | copy-start | bytes 1572868
  217.2 22.9 %collective-permute-start.44 = (bf16[128,2048]{1,0:T(8,128)(2,1)S(1)}, bf16[128,2048]{1,0:T(8,128)(2,1)S(1)}, u32[]{:S(2)}, u32[]{:S(2)}) collective-permute-start(bf16[128,2048]{1,0:T(8,128)(2,1)S(1)} %broadcast_select_fusion.2.refs_4_), channel_id=1, source_target_pairs={{0,4},{2,6},{4,0},{6,2},{8,12},{10,14},{12,8},{14,10},{16,20},{18,... | collective-permute-start | bytes 1572872 | tf_op jit(solution)/shard_map/ppermute | solution.py:28
  217.8 19.5 %collective-permute-start.42 = (bf16[64,2048]{1,0:T(8,128)(2,1)}, bf16[64,2048]{1,0:T(8,128)(2,1)S(1)}, u32[]{:S(2)}, u32[]{:S(2)}) collective-permute-start(bf16[64,2048]{1,0:T(8,128)(2,1)} %get-tuple-element.30), channel_id=1, source_target_pairs={{0,4},{2,6},{4,0},{6,2},{8,12},{10,14},{12,8},{14,10},{16,20},{18,... | collective-permute-start | bytes 786440 | tf_op jit(solution)/shard_map/ppermute | solution.py:28
  219.3 20.8 %collective-permute-start.43 = (bf16[64,2048]{1,0:T(8,128)(2,1)}, bf16[64,2048]{1,0:T(8,128)(2,1)S(1)}, u32[]{:S(2)}, u32[]{:S(2)}) collective-permute-start(bf16[64,2048]{1,0:T(8,128)(2,1)} %get-tuple-element.38), channel_id=1, source_target_pairs={{0,4},{2,6},{4,0},{6,2},{8,12},{10,14},{12,8},{14,10},{16,20},{18,... | collective-permute-start | bytes 786440 | tf_op jit(solution)/shard_map/ppermute | solution.py:28
  219.8 9.1 %collective-permute-start.39 = (f32[8,640]{1,0:T(8,128)S(1)}, f32[8,640]{1,0:T(8,128)S(1)}, u32[]{:S(2)}, u32[]{:S(2)}) collective-permute-start(f32[8,640]{1,0:T(8,128)S(1)} %get-tuple-element.21.refs_3_), channel_id=1, source_target_pairs={{0,1},{1,0},{2,3},{3,2},{4,5},{5,4},{6,7},{7,6},{8,9},{9,8},{10,11... | collective-permute-start | bytes 61448 | tf_op jit(solution)/shard_map/ppermute | solution.py:28
  245.9 2.7 %collective-permute-start.45 = (bf16[256,2048]{1,0:T(8,128)(2,1)S(1)}, bf16[256,2048]{1,0:T(8,128)(2,1)S(1)}, u32[]{:S(2)}, u32[]{:S(2)}) collective-permute-start(bf16[256,2048]{1,0:T(8,128)(2,1)S(1)} %get-tuple-element.24), channel_id=1, source_target_pairs={{0,2},{2,0},{4,6},{6,4},{8,10},{10,8},{12,14},{14,12},{16,18},{18,... | collective-permute-start | bytes 3145736 | tf_op jit(solution)/shard_map/ppermute | solution.py:28
  (18 other events, 50.0 us)

commit v3 on v2

--- a/solution.py
+++ b/solution.py
@@ -11,6 +11,7 @@
 
 
 epsilon = 1e-06
+z_from = 4
 window = 16
 group_count = 4
 lanes = 128
@@ -87,7 +88,7 @@
     if not split:
         near = [join(near)]
     far = [(level(pick(e), half), [q + half for q in e[1]], None) for e in near]
-    return near + far + beyond + [(across(v), [q + nz for q in at], None) for v, at, _ in far]
+    return near + far + beyond + [(across(v), [q + nz for q in at], -1) for v, at, _ in far]
 
 
 def load_weight(pieces, refs, shard, w, sems):
@@ -97,7 +98,7 @@
             rows = pl.ds(k * shard, shard)
             copies.append(
                 pltpu.make_async_copy(
-                    ref.at[rows] if index is None else ref.at[index, rows],
+                    ref.at[rows] if index in (None, -1) else ref.at[index, rows],
                     w.at[pl.ds(place * shard, shard)],
                     sems.at[len(copies)],
                 )
@@ -232,23 +233,23 @@
     in_opposite = across(in_t)
     found = [None] * (2 * layers)
 
-    def gather_group(stack, matrices, merged):
-        arrived = lower(stack, nz)
-        whole = [(across(v), at) for v, at in arrived] if merged else None
+    def gather_group(stack, matrices, arrived):
         for j, k in enumerate(matrices):
             l = k // 2
             mine = [(v, at, j) for v, at in arrived]
-            if merged:
-                crossed = [(v, [q + nz for q in at], j) for v, at in whole]
+            opposite = (across(out_weight[l]), [nz], None) if k % 2 else (in_opposite, [nz], l)
+            if k < z_from:
+                crossed = [(across(v[j]), at) for v, at in arrived]
             else:
-                crossed = [(across(v[j]), [q + nz for q in at], None) for v, at in arrived]
-            opposite = (across(out_weight[l]), [nz], None) if k % 2 else (in_opposite, [nz], l)
+                whole = opposite[0][l : l + 1] if k % 2 == 0 else opposite[0][None]
+                crossed = [(v[0], at) for v, at in lower(whole, nz)]
+            crossed = [(v, [q + nz for q in at], None) for v, at in crossed]
             found[k] = gather(stack[j], opposite, mine, crossed, nz, k == 0)
 
-    gather_group(in_t[:1], [0], True)
-    gather_group(out_weight[:1], [1], True)
-    gather_group(in_t[1:], list(range(2, 2 * layers, 2)), True)
-    gather_group(out_weight[1:], list(range(3, 2 * layers, 2)), False)
+    gather_group(in_t[:1], [0], lower(in_t[:1], nz))
+    gather_group(out_weight[:1], [1], lower(out_weight[:1], nz))
+    gather_group(in_t[1:], list(range(2, 2 * layers, 2)), lower(in_t[1:], nz))
+    later = lower(out_weight[1:], nz)
 
     order = order_table(nz)
     table = [[(order[s // 4][b % nz] * 2 + ((s // 2) % 2 ^ (b // nz))) * 2 + s % 2 for b in range(2 * nz)] for s in range(count)]
@@ -280,7 +281,7 @@
     for l in range(layers):
         first, last = l == 0, l == layers - 1
         pieces = [(at, index) for _, at, index in found[2 * l]]
-        arrays = [in_hbm(v) for v, _, _ in found[2 * l]]
+        arrays = [v if i == -1 else in_hbm(v) for v, _, i in found[2 * l]]
         outs = [shape((total, half), bf16), shape((8, padded), jnp.float32)]
         if not first:
             outs = [pltpu.HBM((total, feats), bf16)] + outs
@@ -301,6 +302,10 @@
         if not first:
             state = results[0]
         partial, squares = results[-2:]
+        if first:
+            partial, *held = lax.optimization_barrier([partial] + [v for v, _ in later])
+            later = [(v, at) for v, (_, at) in zip(held, later)]
+            gather_group(out_weight[1:], list(range(3, 2 * layers, 2)), later)
         bits = levels(lax.axis_size("tp"))
         for b, bit in enumerate(bits):
             swap = lambda v: move(v, "tp", lambda s: s ^ bit)
@@ -308,7 +313,7 @@
             if b < len(bits) - 1:
                 partial, squares = partial + others[0], squares + others[1]
         pieces = [(at, index) for _, at, index in found[2 * l + 1]]
-        arrays = [in_hbm(v) for v, _, _ in found[2 * l + 1]]
+        arrays = [v if i == -1 else in_hbm(v) for v, _, i in found[2 * l + 1]]
         operands = (place, partial, others[0], squares, others[1], group, scale[l])
         weights = pltpu.VMEM((half, feats), bf16)
         sems = pltpu.SemaphoreType.DMA((2 * nz,))

time: 252 us -> 265 us (1.052)
  waiting for transfers between devices: 156 us -> 165 us
  starting transfers between devices: 44.3 us -> 47.1 us
    ppermute x46 -> x47, waiting for transfers between devices: 156 us -> 165 us  [move(): lax.ppermute(value, axis, [(s, t) for s, t in pairs if t is not None])]
    ppermute x46 -> x47, starting transfers between devices: 44.3 us -> 47.1 us  [move(): lax.ppermute(value, axis, [(s, t) for s, t in pairs if t is not None])]
  transfers between devices with their start and end apart: 46 -> 47, of which waited for: 19 -> 16; matrix products, arithmetic and copies ran while one was open for 6% -> 7% of each run, Pallas kernels for 4% -> 4%
where the time goes in v3:
time: 265 us; the launch traced here: 263 us
  waiting for transfers between devices  165 us (62%)
  starting transfers between devices  47.1 us (18%)
  Pallas kernels  25.1 us (9%)
  local copies, waits for them, and re-layouts  14.6 us (6%)
  other arithmetic  9.77 us (4%)
    ppermute x47, waiting for transfers between devices, move(): lax.ppermute(value, axis, [(s, t) for s, t in pairs if t is not None])  165 us
    ppermute x47, starting transfers between devices, move(): lax.ppermute(value, axis, [(s, t) for s, t in pairs if t is not None])  47.1 us
    pallas_call x3, Pallas kernels, body(): pl.pallas_call(functools.partial(in_kernel, first, pieces, shard), out_sh...  9.28 us
    pallas_call x2, Pallas kernels, body(): pl.pallas_call(functools.partial(out_kernel, pieces, shard, features, hal...  9.27 us
  transfers between devices with their start and end apart: 47, of which 16 were waited for; matrix products, arithmetic and copies ran while one was open for 7% of the time, Pallas kernels for 4%

profile of v3, /device:TPU:4, one launch (start us, length us, event | category | flops | bytes accessed | tf_op | source)
XLA Modules:
  0.0 262.7 jit_solution(14669618544232530488)
XLA Ops:
  0.0 1.0 slice.70
  1.0 1.4 collective-permute-start
  2.4 1.3 fusion
  3.7 1.0 slice_bitcast_fusion.1
  4.7 1.6 collective-permute-start.3
  6.3 1.4 collective-permute-start.4
  7.7 1.0 slice_bitcast_fusion.5
  8.7 3.7 %collective-permute-start.15 = (bf16[1,64,2048]{2,1,0:T(8,128)(2,1)}, bf16[1,64,2048]{2,1,0:T(8,128)(2,1)}, u32[]{:S(2)}, u32[]{:S(2)}) collective-permute-start(bf16[1,64,2048]{2,1,0:T(8,128)(2,1)} %get-tuple-element.36), channel_id=1, source_target_pairs={{0,8},{2,10},{4,12},{6,14},{8,0},{10,2},{12,4},{14,6},{16,24},{18,... | collective-permute-start | bytes 786440 | tf_op jit(solution)/shard_map/ppermute | solution.py:29
  15.3 0.8 slice.72
  16.1 0.8 slice.92
  17.5 2.1 collective-permute-done.15
  19.6 1.3 collective-permute-start.1
  20.9 1.1 pad_maximum_fusion.1.refs_7_
  22.0 1.7 collective-permute-start.12
  24.4 1.3 collective-permute-start.5
  25.8 16.8 %collective-permute-done.5 = bf16[64,2048]{1,0:T(8,128)(2,1)S(1)} collective-permute-done((bf16[64,2048]{1,0:T(8,128)(2,1)}, bf16[64,2048]{1,0:T(8,128)(2,1)S(1)}, u32[]{:S(2)}, u32[]{:S(2)}) %collective-permute-start.5) | collective-permute-done | bytes 262176 | tf_op jit(solution)/shard_map/ppermute | solution.py:29
  43.2 1.3 collective-permute-start.7
  44.6 9.9 %collective-permute-done.7 = bf16[64,2048]{1,0:T(8,128)(2,1)S(1)} collective-permute-done((bf16[64,2048]{1,0:T(8,128)(2,1)S(1)}, bf16[64,2048]{1,0:T(8,128)(2,1)S(1)}, u32[]{:S(2)}, u32[]{:S(2)}) %collective-permute-start.7) | collective-permute-done | bytes 262176 | tf_op jit(solution)/shard_map/ppermute | solution.py:29
  54.6 2.1 collective-permute-start.10
  56.7 1.3 collective-permute-start.17
  58.0 1.4 broadcast_select_fusion.1
  59.4 4.3 %collective-permute-done.9.refs_6_ = bf16[64,2048]{1,0:T(8,128)(2,1)S(1)} collective-permute-done((bf16[64,2048]{1,0:T(8,128)(2,1)S(1)}, bf16[64,2048]{1,0:T(8,128)(2,1)S(1)}, u32[]{:S(2)}, u32[]{:S(2)}) %collective-permute-start.9) | collective-permute-done | bytes 262176 | tf_op jit(solution)/shard_map/ppermute | solution.py:29
  64.4 4.9 %collective-permute-done.10.refs_7_ = bf16[64,2048]{1,0:T(8,128)(2,1)S(1)} collective-permute-done((bf16[64,2048]{1,0:T(8,128)(2,1)S(1)}, bf16[64,2048]{1,0:T(8,128)(2,1)S(1)}, u32[]{:S(2)}, u32[]{:S(2)}) %collective-permute-start.10) | collective-permute-done | bytes 262176 | tf_op jit(solution)/shard_map/ppermute | solution.py:29
  69.4 5.5 %collective-permute-done.11.refs_8_ = bf16[64,2048]{1,0:T(8,128)(2,1)S(1)} collective-permute-done((bf16[64,2048]{1,0:T(8,128)(2,1)S(1)}, bf16[64,2048]{1,0:T(8,128)(2,1)S(1)}, u32[]{:S(2)}, u32[]{:S(2)}) %collective-permute-start.11) | collective-permute-done | bytes 262176 | tf_op jit(solution)/shard_map/ppermute | solution.py:29
  74.9 2.8 %shard_map.64 = (bf16[560,512]{1,0:T(8,128)(2,1)S(1)}, f32[8,640]{1,0:T(8,128)S(1)}) custom-call(bf16[560,2048]{1,0:T(8,128)(2,1)S(1)} %pad_maximum_fusion.refs_0_, bf16[64,2048]{1,0:T(8,128)(2,1)} %copy-done.14, bf16[1,64,2048]{2,1,0:T(8,128)(2,1)} %copy-done.24, bf16[64,2048]{1,0:T(8,128)(2,1)} %copy-done.18, bf16[64,2048]{1,0:T(8,128)(2,1)} %copy-done.19, ...), custom_call_target="tpu_custom_call" | custom-call | flops 1174405120 | bytes 8978432 | tf_op jit(solution)/shard_map/pallas_call | solution.py:288
  77.8 1.6 collective-permute-start.13
  79.3 0.9 broadcast_select_fusion.6.refs_8_
  80.9 2.0 collective-permute-start.19
  83.5 1.5 collective-permute-start.14
  85.0 1.8 slice_bitcast_fusion
  86.8 9.8 %collective-permute-done.19.refs_10_ = bf16[64,2048]{1,0:T(8,128)(2,1)S(1)} collective-permute-done((bf16[64,2048]{1,0:T(8,128)(2,1)}, bf16[64,2048]{1,0:T(8,128)(2,1)S(1)}, u32[]{:S(2)}, u32[]{:S(2)}) %collective-permute-start.19) | collective-permute-done | bytes 262176 | tf_op jit(solution)/shard_map/ppermute | solution.py:29
  96.6 0.7 broadcast_in_dim.26.refs_5_
  98.0 4.7 %shard_map.65.refs_1_ = bf16[560,2048]{1,0:T(8,128)(2,1)S(1)} custom-call(s32[2]{0:T(128)S(1)} %pad_add_fusion.refs_0_, bf16[560,512]{1,0:T(8,128)(2,1)S(1)} %get-tuple-element.18.refs_1_, bf16[560,512]{1,0:T(8,128)(2,1)S(1)} %collective-permute-done.13.refs_2_, f32[8,640]{1,0:T(8,128)S(1)} %get-tuple-element.19.refs_3_, ...), custom_call_target="tpu_custom_call" | custom-call | flops 1174405120 | bytes 8978432 | tf_op jit(solution)/shard_map/pallas_call | solution.py:324
  103.6 1.3 collective-permute-start.24
  104.9 0.8 slice_bitcast_fusion.4
  105.8 1.1 pad_maximum_fusion.3.refs_7_
  107.5 24.7 %collective-permute-done.24 = bf16[128,2048]{1,0:T(8,128)(2,1)S(1)} collective-permute-done((bf16[128,2048]{1,0:T(8,128)(2,1)S(1)}, bf16[128,2048]{1,0:T(8,128)(2,1)S(1)}, u32[]{:S(2)}, u32[]{:S(2)}) %collective-permute-start.24) | collective-permute-done | bytes 524320 | tf_op jit(solution)/shard_map/ppermute | solution.py:29
  132.9 1.3 collective-permute-start.30
  134.2 1.5 collective-permute-start.25
  135.7 15.1 %collective-permute-done.25.refs_6_ = bf16[64,2048]{1,0:T(8,128)(2,1)S(1)} collective-permute-done((bf16[64,2048]{1,0:T(8,128)(2,1)S(1)}, bf16[64,2048]{1,0:T(8,128)(2,1)S(1)}, u32[]{:S(2)}, u32[]{:S(2)}) %collective-permute-start.25) | collective-permute-done | bytes 262176 | tf_op jit(solution)/shard_map/ppermute | solution.py:29
  151.6 3.2 %shard_map.66 = (bf16[560,2048]{1,0:T(8,128)(2,1)}, bf16[560,512]{1,0:T(8,128)(2,1)S(1)}, f32[8,640]{1,0:T(8,128)S(1)}) custom-call(bf16[560,2048]{1,0:T(8,128)(2,1)S(1)} %pad_maximum_fusion.refs_0_, bf16[560,2048]{1,0:T(8,128)(2,1)S(1)} %shard_map.65.refs_1_, bf16[560,2048]{1,0:T(8,128)(2,1)S(1)} %collective-permute-done.21.refs_2_, ...), custom_call_target="tpu_custom_call" | custom-call | flops 1174405120 | bytes 8978432 | tf_op jit(solution)/shard_map/pallas_call | solution.py:288
  156.1 1.5 collective-permute-start.31
  158.1 1.5 collective-permute-start.28
  159.7 16.0 %collective-permute-done.31.refs_9_ = bf16[64,2048]{1,0:T(8,128)(2,1)S(1)} collective-permute-done((bf16[64,2048]{1,0:T(8,128)(2,1)}, bf16[64,2048]{1,0:T(8,128)(2,1)S(1)}, u32[]{:S(2)}, u32[]{:S(2)}) %collective-permute-start.31) | collective-permute-done | bytes 262176 | tf_op jit(solution)/shard_map/ppermute | solution.py:29
  175.7 2.8 %collective-permute-done.32.refs_10_ = bf16[64,2048]{1,0:T(8,128)(2,1)S(1)} collective-permute-done((bf16[64,2048]{1,0:T(8,128)(2,1)}, bf16[64,2048]{1,0:T(8,128)(2,1)S(1)}, u32[]{:S(2)}, u32[]{:S(2)}) %collective-permute-start.32) | collective-permute-done | bytes 262176 | tf_op jit(solution)/shard_map/ppermute | solution.py:29
  179.3 4.5 %shard_map.67.refs_1_ = bf16[560,2048]{1,0:T(8,128)(2,1)S(1)} custom-call(s32[2]{0:T(128)S(1)} %pad_add_fusion.refs_0_, bf16[560,512]{1,0:T(8,128)(2,1)S(1)} %get-tuple-element.21.refs_1_, bf16[560,512]{1,0:T(8,128)(2,1)S(1)} %collective-permute-done.27.refs_2_, f32[8,640]{1,0:T(8,128)S(1)} %get-tuple-element.22.refs_3_, ...), custom_call_target="tpu_custom_call" | custom-call | flops 1174405120 | bytes 8978432 | tf_op jit(solution)/shard_map/pallas_call | solution.py:324
  184.0 0.8 collective-permute-start.35
  184.8 1.3 collective-permute-start.36
  186.9 25.7 %collective-permute-done.36 = bf16[128,2048]{1,0:T(8,128)(2,1)S(1)} collective-permute-done((bf16[128,2048]{1,0:T(8,128)(2,1)S(1)}, bf16[128,2048]{1,0:T(8,128)(2,1)S(1)}, u32[]{:S(2)}, u32[]{:S(2)}) %collective-permute-start.36) | collective-permute-done | bytes 524320 | tf_op jit(solution)/shard_map/ppermute | solution.py:29
  213.3 1.5 collective-permute-start.42
  214.7 1.0 slice.97
  215.7 3.2 %collective-permute-start.37 = (bf16[1,64,2048]{2,1,0:T(8,128)(2,1)S(1)}, bf16[1,64,2048]{2,1,0:T(8,128)(2,1)S(1)}, u32[]{:S(2)}, u32[]{:S(2)}) collective-permute-start(bf16[1,64,2048]{2,1,0:T(8,128)(2,1)S(1)} %slice.97), channel_id=1, source_target_pairs={{0,8},{2,10},{4,12},{6,14},{8,0},{10,2},{12,4},{14,6},{16,24},{18,... | collective-permute-start | bytes 786440 | tf_op jit(solution)/shard_map/ppermute | solution.py:29
  218.9 1.0 collective-permute-start.43
  219.9 14.0 %collective-permute-done.37 = bf16[1,64,2048]{2,1,0:T(8,128)(2,1)S(1)} collective-permute-done((bf16[1,64,2048]{2,1,0:T(8,128)(2,1)S(1)}, bf16[1,64,2048]{2,1,0:T(8,128)(2,1)S(1)}, u32[]{:S(2)}, u32[]{:S(2)}) %collective-permute-start.37) | collective-permute-done | bytes 262176 | tf_op jit(solution)/shard_map/ppermute | solution.py:29
  234.0 0.7 copy-done.30
  234.7 3.2 %shard_map.68 = (bf16[560,2048]{1,0:T(8,128)(2,1)}, bf16[560,512]{1,0:T(8,128)(2,1)S(1)}, f32[8,640]{1,0:T(8,128)S(1)}) custom-call(bf16[560,2048]{1,0:T(8,128)(2,1)S(1)} %copy-done.1, bf16[560,2048]{1,0:T(8,128)(2,1)S(1)} %shard_map.67.refs_1_, bf16[560,2048]{1,0:T(8,128)(2,1)S(1)} %collective-permute-done.34.refs_2_, bf16[128,2048]{1,0:T(8,128)(2,1)} %copy-done.7, ...), custom_call_target="tpu_custom_call" | custom-call | flops 1174405120 | bytes 8978432 | tf_op jit(solution)/shard_map/pallas_call | solution.py:288
  237.9 1.6 collective-permute-start.39
  239.5 0.8 collective-permute-start.45
  241.0 10.4 %collective-permute-done.40.refs_4_ = f32[8,640]{1,0:T(8,128)S(1)} collective-permute-done((f32[8,640]{1,0:T(8,128)S(1)}, f32[8,640]{1,0:T(8,128)S(1)}, u32[]{:S(2)}, u32[]{:S(2)}) %collective-permute-start.40) | collective-permute-done | bytes 20512 | tf_op jit(solution)/shard_map/ppermute | solution.py:29
  251.4 1.8 shard_map.69.refs_1_
  253.2 0.7 copy-done.27
  253.9 4.8 %shard_map.70 = (f32[256,2048]{1,0:T(8,128)S(1)}, bf16[256,2048]{1,0:T(8,128)(2,1)S(1)}) custom-call(s32[2]{0:T(128)S(1)} %pad_add_fusion.refs_0_, bf16[560,512]{1,0:T(8,128)(2,1)S(1)} %shard_map.69.refs_1_, bf16[560,2048]{1,0:T(8,128)(2,1)} %get-tuple-element.26.refs_2_, bf16[128,2048]{1,0:T(8,128)(2,1)} %copy-done.5, bf16[128,2048]{1,0:T(8,128)(2,1)} %copy-done.9, ...), custom_call_target="tpu_custom_call" | custom-call | flops 1174405120 | bytes 8978432 | tf_op jit(solution)/shard_map/pallas_call | solution.py:341
  258.8 2.6 %collective-permute-done.46 = bf16[256,2048]{1,0:T(8,128)(2,1)S(1)} collective-permute-done((bf16[256,2048]{1,0:T(8,128)(2,1)S(1)}, bf16[256,2048]{1,0:T(8,128)(2,1)S(1)}, u32[]{:S(2)}, u32[]{:S(2)}) %collective-permute-start.46) | collective-permute-done | bytes 1048608 | tf_op jit(solution)/shard_map/ppermute | solution.py:29
  261.4 1.3 add_convert_fusion
  (147 shorter events, 15.5 us)
Async XLA Ops:
  0.0 7.7 %copy-start.3 = (bf16[3,64,2048]{2,1,0:T(8,128)(2,1)S(1)}, bf16[3,64,2048]{2,1,0:T(8,128)(2,1)}, u32[]{:S(2)}) copy-start(bf16[3,64,2048]{2,1,0:T(8,128)(2,1)} %param.10) | copy-start | bytes 2359300
  0.0 56.7 %collective-permute-start.2 = (bf16[256,2048]{1,0:T(8,128)(2,1)}, bf16[256,2048]{1,0:T(8,128)(2,1)}, u32[]{:S(2)}, u32[]{:S(2)}) collective-permute-start(bf16[256,2048]{1,0:T(8,128)(2,1)} %param.6), channel_id=1, source_target_pairs={{0,2},{2,0},{4,6},{6,4},{8,10},{10,8},{12,14},{14,12},{16,18},{18,... | collective-permute-start | bytes 3145736 | tf_op jit(solution)/shard_map/ppermute | solution.py:29
  1.0 15.9 %collective-permute-start = (bf16[48,2048]{1,0:T(8,128)(2,1)S(1)}, bf16[48,2048]{1,0:T(8,128)(2,1)}, u32[]{:S(2)}, u32[]{:S(2)}) collective-permute-start(bf16[48,2048]{1,0:T(8,128)(2,1)S(1)} %slice.70), channel_id=1, source_target_pairs={{2,6},{6,10},{10,14},{14,18},{18,22},{22,26},{26,30},{3,7},{7,11},... | collective-permute-start | bytes 589832 | tf_op jit(solution)/shard_map/ppermute | solution.py:29
  2.4 12.1 %copy-start.32 = (f32[3,1024]{1,0:T(4,128)S(1)}, f32[3,1024]{1,0:T(4,128)}, u32[]{:S(2)}) copy-start(f32[3,1024]{1,0:T(4,128)} %param.9) | copy-start | bytes 36868
  4.7 17.3 %copy-start.14 = (bf16[64,2048]{1,0:T(8,128)(2,1)}, bf16[64,2048]{1,0:T(8,128)(2,1)S(1)}, u32[]{:S(2)}) copy-start(bf16[64,2048]{1,0:T(8,128)(2,1)S(1)} %get-tuple-element.39.refs_1_) | copy-start | bytes 786436
  4.7 17.3 %collective-permute-start.3 = (bf16[1,64,2048]{2,1,0:T(8,128)(2,1)S(1)}, bf16[1,64,2048]{2,1,0:T(8,128)(2,1)S(1)}, u32[]{:S(2)}, u32[]{:S(2)}) collective-permute-start(bf16[1,64,2048]{2,1,0:T(8,128)(2,1)S(1)} %get-tuple-element.41), channel_id=1, source_target_pairs={{0,8},{2,10},{4,12},{6,14},{8,0},{10,2},{12,4},{14,6},{16,24},{18,... | collective-permute-start | bytes 786440 | tf_op jit(solution)/shard_map/ppermute | solution.py:29
  6.3 17.5 %collective-permute-start.4 = (bf16[64,2048]{1,0:T(8,128)(2,1)S(1)}, bf16[64,2048]{1,0:T(8,128)(2,1)}, u32[]{:S(2)}, u32[]{:S(2)}) collective-permute-start(bf16[64,2048]{1,0:T(8,128)(2,1)S(1)} %get-tuple-element.39.refs_1_), channel_id=1, source_target_pairs={{8,16},{10,18},{12,20},{14,22},{16,8},{18,10},{20,12},{22,14},{9,1... | collective-permute-start | bytes 786440 | tf_op jit(solution)/shard_map/ppermute | solution.py:29
  8.7 10.9 %collective-permute-start.15 = (bf16[1,64,2048]{2,1,0:T(8,128)(2,1)}, bf16[1,64,2048]{2,1,0:T(8,128)(2,1)}, u32[]{:S(2)}, u32[]{:S(2)}) collective-permute-start(bf16[1,64,2048]{2,1,0:T(8,128)(2,1)} %get-tuple-element.36), channel_id=1, source_target_pairs={{0,8},{2,10},{4,12},{6,14},{8,0},{10,2},{12,4},{14,6},{16,24},{18,... | collective-permute-start | bytes 786440 | tf_op jit(solution)/shard_map/ppermute | solution.py:29
  16.1 41.8 %copy-start.13 = (bf16[256,2048]{1,0:T(8,128)(2,1)S(1)}, bf16[256,2048]{1,0:T(8,128)(2,1)}, u32[]{:S(2)}) copy-start(bf16[256,2048]{1,0:T(8,128)(2,1)} %param.6) | copy-start | bytes 3145732
  17.0 52.4 %collective-permute-start.8 = (bf16[3,64,2048]{2,1,0:T(8,128)(2,1)S(1)}, bf16[3,64,2048]{2,1,0:T(8,128)(2,1)S(1)}, u32[]{:S(2)}, u32[]{:S(2)}) collective-permute-start(bf16[3,64,2048]{2,1,0:T(8,128)(2,1)S(1)} %fusion), channel_id=1, source_target_pairs={{0,4},{2,6},{4,0},{6,2},{8,12},{10,14},{12,8},{14,10},{16,20},{18,... | collective-permute-start | bytes 2359304 | tf_op jit(solution)/shard_map/ppermute | solution.py:29
  19.6 4.8 %collective-permute-start.1 = (bf16[48,2048]{1,0:T(8,128)(2,1)}, bf16[48,2048]{1,0:T(8,128)(2,1)S(1)}, u32[]{:S(2)}, u32[]{:S(2)}) collective-permute-start(bf16[48,2048]{1,0:T(8,128)(2,1)} %collective-permute-done), channel_id=1, source_target_pairs={{2,0},{6,4},{10,8},{14,12},{18,16},{22,20},{26,24},{30,28},{3,1},{... | collective-permute-start | bytes 589832 | tf_op jit(solution)/shard_map/ppermute | solution.py:29
  22.0 37.4 %copy-start.4 = (bf16[128,2048]{1,0:T(8,128)(2,1)}, bf16[128,2048]{1,0:T(8,128)(2,1)S(1)}, u32[]{:S(2)}) copy-start(bf16[128,2048]{1,0:T(8,128)(2,1)S(1)} %pad_maximum_fusion.1.refs_7_) | copy-start | bytes 1572868
  22.0 37.4 %copy-start.24 = (bf16[1,64,2048]{2,1,0:T(8,128)(2,1)}, bf16[1,64,2048]{2,1,0:T(8,128)(2,1)S(1)}, u32[]{:S(2)}) copy-start(bf16[1,64,2048]{2,1,0:T(8,128)(2,1)S(1)} %collective-permute-done.3.refs_2_) | copy-start | bytes 786436
  22.0 55.7 %collective-permute-start.12 = (bf16[2,64,2048]{2,1,0:T(8,128)(2,1)}, bf16[2,64,2048]{2,1,0:T(8,128)(2,1)S(1)}, u32[]{:S(2)}, u32[]{:S(2)}) collective-permute-start(bf16[2,64,2048]{2,1,0:T(8,128)(2,1)} %slice.72), channel_id=1, source_target_pairs={{0,8},{2,10},{4,12},{6,14},{8,0},{10,2},{12,4},{14,6},{16,24},{18,... | collective-permute-start | bytes 1572872 | tf_op jit(solution)/shard_map/ppermute | solution.py:29
  23.7 19.5 %collective-permute-start.6 = (bf16[64,2048]{1,0:T(8,128)(2,1)S(1)}, bf16[64,2048]{1,0:T(8,128)(2,1)S(1)}, u32[]{:S(2)}, u32[]{:S(2)}) collective-permute-start(bf16[64,2048]{1,0:T(8,128)(2,1)S(1)} %bitcast.36), channel_id=1, source_target_pairs={{8,16},{10,18},{12,20},{14,22},{16,8},{18,10},{20,12},{22,14},{9,1... | collective-permute-start | bytes 786440 | tf_op jit(solution)/shard_map/ppermute | solution.py:29
  24.4 18.1 %collective-permute-start.5 = (bf16[64,2048]{1,0:T(8,128)(2,1)}, bf16[64,2048]{1,0:T(8,128)(2,1)S(1)}, u32[]{:S(2)}, u32[]{:S(2)}) collective-permute-start(bf16[64,2048]{1,0:T(8,128)(2,1)} %collective-permute-done.4), channel_id=1, source_target_pairs={{8,0},{10,2},{12,4},{14,6},{16,24},{18,26},{20,28},{22,30},{9,1},{... | collective-permute-start | bytes 786440 | tf_op jit(solution)/shard_map/ppermute | solution.py:29
  42.5 12.0 %collective-permute-start.16 = (bf16[128,2048]{1,0:T(8,128)(2,1)S(1)}, bf16[128,2048]{1,0:T(8,128)(2,1)S(1)}, u32[]{:S(2)}, u32[]{:S(2)}) collective-permute-start(bf16[128,2048]{1,0:T(8,128)(2,1)S(1)} %pad_maximum_fusion.1.refs_7_), channel_id=1, source_target_pairs={{8,16},{10,18},{12,20},{14,22},{16,8},{18,10},{20,12},{22,14},{9,1... | collective-permute-start | bytes 1572872 | tf_op jit(solution)/shard_map/ppermute | solution.py:29
  43.2 11.3 %collective-permute-start.7 = (bf16[64,2048]{1,0:T(8,128)(2,1)S(1)}, bf16[64,2048]{1,0:T(8,128)(2,1)S(1)}, u32[]{:S(2)}, u32[]{:S(2)}) collective-permute-start(bf16[64,2048]{1,0:T(8,128)(2,1)S(1)} %collective-permute-done.6), channel_id=1, source_target_pairs={{8,0},{10,2},{12,4},{14,6},{16,24},{18,26},{20,28},{22,30},{9,1},{... | collective-permute-start | bytes 786440 | tf_op jit(solution)/shard_map/ppermute | solution.py:29
  44.6 14.8 %copy-start.18 = (bf16[64,2048]{1,0:T(8,128)(2,1)}, bf16[64,2048]{1,0:T(8,128)(2,1)S(1)}, u32[]{:S(2)}) copy-start(bf16[64,2048]{1,0:T(8,128)(2,1)S(1)} %broadcast_select_fusion.8.refs_3_) | copy-start | bytes 786436
  54.5 9.2 %collective-permute-start.9 = (bf16[64,2048]{1,0:T(8,128)(2,1)S(1)}, bf16[64,2048]{1,0:T(8,128)(2,1)S(1)}, u32[]{:S(2)}, u32[]{:S(2)}) collective-permute-start(bf16[64,2048]{1,0:T(8,128)(2,1)S(1)} %bitcast.37), channel_id=1, source_target_pairs={{0,4},{2,6},{4,0},{6,2},{8,12},{10,14},{12,8},{14,10},{16,20},{18,... | collective-permute-start | bytes 786440 | tf_op jit(solution)/shard_map/ppermute | solution.py:29
  54.6 9.4 %copy-start.19 = (bf16[64,2048]{1,0:T(8,128)(2,1)}, bf16[64,2048]{1,0:T(8,128)(2,1)S(1)}, u32[]{:S(2)}) copy-start(bf16[64,2048]{1,0:T(8,128)(2,1)S(1)} %broadcast_select_fusion.7.refs_4_) | copy-start | bytes 786436
  54.6 14.7 %collective-permute-start.10 = (bf16[64,2048]{1,0:T(8,128)(2,1)S(1)}, bf16[64,2048]{1,0:T(8,128)(2,1)S(1)}, u32[]{:S(2)}, u32[]{:S(2)}) collective-permute-start(bf16[64,2048]{1,0:T(8,128)(2,1)S(1)} %broadcast_select_fusion.8.refs_3_), channel_id=1, source_target_pairs={{0,4},{2,6},{4,0},{6,2},{8,12},{10,14},{12,8},{14,10},{16,20},{18,... | collective-permute-start | bytes 786440 | tf_op jit(solution)/shard_map/ppermute | solution.py:29
  56.7 22.7 %collective-permute-start.17 = (bf16[128,2048]{1,0:T(8,128)(2,1)S(1)}, bf16[128,2048]{1,0:T(8,128)(2,1)S(1)}, u32[]{:S(2)}, u32[]{:S(2)}) collective-permute-start(bf16[128,2048]{1,0:T(8,128)(2,1)S(1)} %collective-permute-done.16), channel_id=1, source_target_pairs={{8,0},{10,2},{12,4},{14,6},{16,24},{18,26},{20,28},{22,30},{9,1},{... | collective-permute-start | bytes 1572872 | tf_op jit(solution)/shard_map/ppermute | solution.py:29
  63.7 11.2 %collective-permute-start.11 = (bf16[64,2048]{1,0:T(8,128)(2,1)S(1)}, bf16[64,2048]{1,0:T(8,128)(2,1)S(1)}, u32[]{:S(2)}, u32[]{:S(2)}) collective-permute-start(bf16[64,2048]{1,0:T(8,128)(2,1)S(1)} %broadcast_select_fusion.7.refs_4_), channel_id=1, source_target_pairs={{0,4},{2,6},{4,0},{6,2},{8,12},{10,14},{12,8},{14,10},{16,20},{18,... | collective-permute-start | bytes 786440 | tf_op jit(solution)/shard_map/ppermute | solution.py:29
  69.3 17.5 %collective-permute-start.18 = (bf16[64,2048]{1,0:T(8,128)(2,1)}, bf16[64,2048]{1,0:T(8,128)(2,1)}, u32[]{:S(2)}, u32[]{:S(2)}) collective-permute-start(bf16[64,2048]{1,0:T(8,128)(2,1)} %get-tuple-element.35), channel_id=1, source_target_pairs={{0,4},{2,6},{4,0},{6,2},{8,12},{10,14},{12,8},{14,10},{16,20},{18,... | collective-permute-start | bytes 786440 | tf_op jit(solution)/shard_map/ppermute | solution.py:29
  69.3 14.2 %collective-permute-start.22 = (bf16[2,64,2048]{2,1,0:T(8,128)(2,1)}, bf16[2,64,2048]{2,1,0:T(8,128)(2,1)}, u32[]{:S(2)}, u32[]{:S(2)}) collective-permute-start(bf16[2,64,2048]{2,1,0:T(8,128)(2,1)} %slice.92), channel_id=1, source_target_pairs={{0,8},{2,10},{4,12},{6,14},{8,0},{10,2},{12,4},{14,6},{16,24},{18,... | collective-permute-start | bytes 1572872 | tf_op jit(solution)/shard_map/ppermute | solution.py:29
  77.8 18.8 %collective-permute-start.13 = (bf16[560,512]{1,0:T(8,128)(2,1)S(1)}, bf16[560,512]{1,0:T(8,128)(2,1)S(1)}, u32[]{:S(2)}, u32[]{:S(2)}) collective-permute-start(bf16[560,512]{1,0:T(8,128)(2,1)S(1)} %get-tuple-element.18.refs_1_), channel_id=1, source_target_pairs={{0,1},{1,0},{2,3},{3,2},{4,5},{5,4},{6,7},{7,6},{8,9},{9,8},{10,11... | collective-permute-start | bytes 1720328 | tf_op jit(solution)/shard_map/ppermute | solution.py:29
  80.2 16.4 %collective-permute-start.20 = (bf16[128,2048]{1,0:T(8,128)(2,1)}, bf16[128,2048]{1,0:T(8,128)(2,1)}, u32[]{:S(2)}, u32[]{:S(2)}) collective-permute-start(bf16[128,2048]{1,0:T(8,128)(2,1)} %broadcast_select_fusion.6.refs_8_), channel_id=1, source_target_pairs={{0,4},{2,6},{4,0},{6,2},{8,12},{10,14},{12,8},{14,10},{16,20},{18,... | collective-permute-start | bytes 1572872 | tf_op jit(solution)/shard_map/ppermute | solution.py:29
  80.9 15.7 %collective-permute-start.19 = (bf16[64,2048]{1,0:T(8,128)(2,1)}, bf16[64,2048]{1,0:T(8,128)(2,1)S(1)}, u32[]{:S(2)}, u32[]{:S(2)}) collective-permute-start(bf16[64,2048]{1,0:T(8,128)(2,1)} %bitcast.10), channel_id=1, source_target_pairs={{0,4},{2,6},{4,0},{6,2},{8,12},{10,14},{12,8},{14,10},{16,20},{18,... | collective-permute-start | bytes 786440 | tf_op jit(solution)/shard_map/ppermute | solution.py:29
  83.5 13.1 %collective-permute-start.14 = (f32[8,640]{1,0:T(8,128)S(1)}, f32[8,640]{1,0:T(8,128)S(1)}, u32[]{:S(2)}, u32[]{:S(2)}) collective-permute-start(f32[8,640]{1,0:T(8,128)S(1)} %get-tuple-element.19.refs_3_), channel_id=1, source_target_pairs={{0,1},{1,0},{2,3},{3,2},{4,5},{5,4},{6,7},{7,6},{8,9},{9,8},{10,11... | collective-permute-start | bytes 61448 | tf_op jit(solution)/shard_map/ppermute | solution.py:29
  102.8 48.1 %collective-permute-start.21 = (bf16[560,2048]{1,0:T(8,128)(2,1)S(1)}, bf16[560,2048]{1,0:T(8,128)(2,1)S(1)}, u32[]{:S(2)}, u32[]{:S(2)}) collective-permute-start(bf16[560,2048]{1,0:T(8,128)(2,1)S(1)} %shard_map.65.refs_1_), channel_id=1, source_target_pairs={{0,2},{2,0},{4,6},{6,4},{8,10},{10,8},{12,14},{14,12},{16,18},{18,... | collective-permute-start | bytes 6881288 | tf_op jit(solution)/shard_map/ppermute | solution.py:29
  102.9 48.0 %copy-start.8 = (bf16[128,2048]{1,0:T(8,128)(2,1)}, bf16[128,2048]{1,0:T(8,128)(2,1)S(1)}, u32[]{:S(2)}) copy-start(bf16[128,2048]{1,0:T(8,128)(2,1)S(1)} %pad_maximum_fusion.2.refs_3_) | copy-start | bytes 1572868
  102.9 0.7 collective-permute-start.23
  103.6 28.6 %collective-permute-start.24 = (bf16[128,2048]{1,0:T(8,128)(2,1)S(1)}, bf16[128,2048]{1,0:T(8,128)(2,1)S(1)}, u32[]{:S(2)}, u32[]{:S(2)}) collective-permute-start(bf16[128,2048]{1,0:T(8,128)(2,1)S(1)} %collective-permute-done.23), channel_id=1, source_target_pairs={{8,0},{10,2},{12,4},{14,6},{16,24},{18,26},{20,28},{22,30},{9,1},{... | collective-permute-start | bytes 1572872 | tf_op jit(solution)/shard_map/ppermute | solution.py:29
  106.8 48.0 %copy-start.6 = (bf16[128,2048]{1,0:T(8,128)(2,1)}, bf16[128,2048]{1,0:T(8,128)(2,1)S(1)}, u32[]{:S(2)}) copy-start(bf16[128,2048]{1,0:T(8,128)(2,1)S(1)} %pad_maximum_fusion.3.refs_7_) | copy-start | bytes 1572868
  106.8 26.1 %collective-permute-start.29 = (bf16[128,2048]{1,0:T(8,128)(2,1)S(1)}, bf16[128,2048]{1,0:T(8,128)(2,1)S(1)}, u32[]{:S(2)}, u32[]{:S(2)}) collective-permute-start(bf16[128,2048]{1,0:T(8,128)(2,1)S(1)} %pad_maximum_fusion.3.refs_7_), channel_id=1, source_target_pairs={{8,16},{10,18},{12,20},{14,22},{16,8},{18,10},{20,12},{22,14},{9,1... | collective-permute-start | bytes 1572872 | tf_op jit(solution)/shard_map/ppermute | solution.py:29
  132.3 18.6 %copy-start.12 = (bf16[128,2048]{1,0:T(8,128)(2,1)}, bf16[128,2048]{1,0:T(8,128)(2,1)S(1)}, u32[]{:S(2)}) copy-start(bf16[128,2048]{1,0:T(8,128)(2,1)S(1)} %broadcast_select_fusion.5.refs_4_) | copy-start | bytes 1572868
  132.3 18.6 %collective-permute-start.26 = (bf16[128,2048]{1,0:T(8,128)(2,1)S(1)}, bf16[128,2048]{1,0:T(8,128)(2,1)S(1)}, u32[]{:S(2)}, u32[]{:S(2)}) collective-permute-start(bf16[128,2048]{1,0:T(8,128)(2,1)S(1)} %broadcast_select_fusion.5.refs_4_), channel_id=1, source_target_pairs={{0,4},{2,6},{4,0},{6,2},{8,12},{10,14},{12,8},{14,10},{16,20},{18,... | collective-permute-start | bytes 1572872 | tf_op jit(solution)/shard_map/ppermute | solution.py:29
  132.9 22.5 %collective-permute-start.30 = (bf16[128,2048]{1,0:T(8,128)(2,1)S(1)}, bf16[128,2048]{1,0:T(8,128)(2,1)S(1)}, u32[]{:S(2)}, u32[]{:S(2)}) collective-permute-start(bf16[128,2048]{1,0:T(8,128)(2,1)S(1)} %collective-permute-done.29), channel_id=1, source_target_pairs={{8,0},{10,2},{12,4},{14,6},{16,24},{18,26},{20,28},{22,30},{9,1},{... | collective-permute-start | bytes 1572872 | tf_op jit(solution)/shard_map/ppermute | solution.py:29
  134.2 16.6 %collective-permute-start.25 = (bf16[64,2048]{1,0:T(8,128)(2,1)S(1)}, bf16[64,2048]{1,0:T(8,128)(2,1)S(1)}, u32[]{:S(2)}, u32[]{:S(2)}) collective-permute-start(bf16[64,2048]{1,0:T(8,128)(2,1)S(1)} %get-tuple-element.45), channel_id=1, source_target_pairs={{0,4},{2,6},{4,0},{6,2},{8,12},{10,14},{12,8},{14,10},{16,20},{18,... | collective-permute-start | bytes 786440 | tf_op jit(solution)/shard_map/ppermute | solution.py:29
  154.8 23.7 %collective-permute-start.27 = (bf16[560,512]{1,0:T(8,128)(2,1)S(1)}, bf16[560,512]{1,0:T(8,128)(2,1)S(1)}, u32[]{:S(2)}, u32[]{:S(2)}) collective-permute-start(bf16[560,512]{1,0:T(8,128)(2,1)S(1)} %get-tuple-element.21.refs_1_), channel_id=1, source_target_pairs={{0,1},{1,0},{2,3},{3,2},{4,5},{5,4},{6,7},{7,6},{8,9},{9,8},{10,11... | collective-permute-start | bytes 1720328 | tf_op jit(solution)/shard_map/ppermute | solution.py:29
  155.5 23.1 %copy-start.10 = (bf16[128,2048]{1,0:T(8,128)(2,1)}, bf16[128,2048]{1,0:T(8,128)(2,1)S(1)}, u32[]{:S(2)}) copy-start(bf16[128,2048]{1,0:T(8,128)(2,1)S(1)} %broadcast_select_fusion.4.refs_8_) | copy-start | bytes 1572868
  155.5 23.1 %collective-permute-start.33 = (bf16[128,2048]{1,0:T(8,128)(2,1)S(1)}, bf16[128,2048]{1,0:T(8,128)(2,1)S(1)}, u32[]{:S(2)}, u32[]{:S(2)}) collective-permute-start(bf16[128,2048]{1,0:T(8,128)(2,1)S(1)} %broadcast_select_fusion.4.refs_8_), channel_id=1, source_target_pairs={{0,4},{2,6},{4,0},{6,2},{8,12},{10,14},{12,8},{14,10},{16,20},{18,... | collective-permute-start | bytes 1572872 | tf_op jit(solution)/shard_map/ppermute | solution.py:29
  156.1 19.6 %collective-permute-start.31 = (bf16[64,2048]{1,0:T(8,128)(2,1)}, bf16[64,2048]{1,0:T(8,128)(2,1)S(1)}, u32[]{:S(2)}, u32[]{:S(2)}) collective-permute-start(bf16[64,2048]{1,0:T(8,128)(2,1)} %get-tuple-element.37), channel_id=1, source_target_pairs={{0,4},{2,6},{4,0},{6,2},{8,12},{10,14},{12,8},{14,10},{16,20},{18,... | collective-permute-start | bytes 786440 | tf_op jit(solution)/shard_map/ppermute | solution.py:29
  157.6 21.0 %collective-permute-start.32 = (bf16[64,2048]{1,0:T(8,128)(2,1)}, bf16[64,2048]{1,0:T(8,128)(2,1)S(1)}, u32[]{:S(2)}, u32[]{:S(2)}) collective-permute-start(bf16[64,2048]{1,0:T(8,128)(2,1)} %get-tuple-element.43), channel_id=1, source_target_pairs={{0,4},{2,6},{4,0},{6,2},{8,12},{10,14},{12,8},{14,10},{16,20},{18,... | collective-permute-start | bytes 786440 | tf_op jit(solution)/shard_map/ppermute | solution.py:29
  158.1 20.4 %collective-permute-start.28 = (f32[8,640]{1,0:T(8,128)S(1)}, f32[8,640]{1,0:T(8,128)S(1)}, u32[]{:S(2)}, u32[]{:S(2)}) collective-permute-start(f32[8,640]{1,0:T(8,128)S(1)} %get-tuple-element.22.refs_3_), channel_id=1, source_target_pairs={{0,1},{1,0},{2,3},{3,2},{4,5},{5,4},{6,7},{7,6},{8,9},{9,8},{10,11... | collective-permute-start | bytes 61448 | tf_op jit(solution)/shard_map/ppermute | solution.py:29
  183.8 50.9 %copy-start.1 = (bf16[560,2048]{1,0:T(8,128)(2,1)S(1)}, bf16[560,2048]{1,0:T(8,128)(2,1)}, u32[]{:S(2)}) copy-start(bf16[560,2048]{1,0:T(8,128)(2,1)} %get-tuple-element.20.refs_0_) | copy-start | bytes 6881284
  183.8 50.1 %collective-permute-start.34 = (bf16[560,2048]{1,0:T(8,128)(2,1)S(1)}, bf16[560,2048]{1,0:T(8,128)(2,1)S(1)}, u32[]{:S(2)}, u32[]{:S(2)}) collective-permute-start(bf16[560,2048]{1,0:T(8,128)(2,1)S(1)} %shard_map.67.refs_1_), channel_id=1, source_target_pairs={{0,2},{2,0},{4,6},{6,4},{8,10},{10,8},{12,14},{14,12},{16,18},{18,... | collective-permute-start | bytes 6881288 | tf_op jit(solution)/shard_map/ppermute | solution.py:29
  183.9 50.0 %copy-start.7 = (bf16[128,2048]{1,0:T(8,128)(2,1)}, bf16[128,2048]{1,0:T(8,128)(2,1)S(1)}, u32[]{:S(2)}) copy-start(bf16[128,2048]{1,0:T(8,128)(2,1)S(1)} %pad_maximum_fusion.4.refs_3_) | copy-start | bytes 1572868
  184.0 0.8 collective-permute-start.35
  184.8 27.7 %collective-permute-start.36 = (bf16[128,2048]{1,0:T(8,128)(2,1)S(1)}, bf16[128,2048]{1,0:T(8,128)(2,1)S(1)}, u32[]{:S(2)}, u32[]{:S(2)}) collective-permute-start(bf16[128,2048]{1,0:T(8,128)(2,1)S(1)} %collective-permute-done.35), channel_id=1, source_target_pairs={{8,0},{10,2},{12,4},{14,6},{16,24},{18,26},{20,28},{22,30},{9,1},{... | collective-permute-start | bytes 1572872 | tf_op jit(solution)/shard_map/ppermute | solution.py:29
  186.2 51.7 %copy-start.5 = (bf16[128,2048]{1,0:T(8,128)(2,1)}, bf16[128,2048]{1,0:T(8,128)(2,1)S(1)}, u32[]{:S(2)}) copy-start(bf16[128,2048]{1,0:T(8,128)(2,1)S(1)} %pad_maximum_fusion.5.refs_3_) | copy-start | bytes 1572868
  186.2 27.1 %collective-permute-start.41 = (bf16[128,2048]{1,0:T(8,128)(2,1)S(1)}, bf16[128,2048]{1,0:T(8,128)(2,1)S(1)}, u32[]{:S(2)}, u32[]{:S(2)}) collective-permute-start(bf16[128,2048]{1,0:T(8,128)(2,1)S(1)} %pad_maximum_fusion.5.refs_3_), channel_id=1, source_target_pairs={{8,16},{10,18},{12,20},{14,22},{16,8},{18,10},{20,12},{22,14},{9,1... | collective-permute-start | bytes 1572872 | tf_op jit(solution)/shard_map/ppermute | solution.py:29
  212.6 21.3 %copy-start.11 = (bf16[128,2048]{1,0:T(8,128)(2,1)}, bf16[128,2048]{1,0:T(8,128)(2,1)S(1)}, u32[]{:S(2)}) copy-start(bf16[128,2048]{1,0:T(8,128)(2,1)S(1)} %broadcast_select_fusion.3.refs_4_) | copy-start | bytes 1572868
  212.6 21.3 %collective-permute-start.38 = (bf16[128,2048]{1,0:T(8,128)(2,1)S(1)}, bf16[128,2048]{1,0:T(8,128)(2,1)S(1)}, u32[]{:S(2)}, u32[]{:S(2)}) collective-permute-start(bf16[128,2048]{1,0:T(8,128)(2,1)S(1)} %broadcast_select_fusion.3.refs_4_), channel_id=1, source_target_pairs={{0,4},{2,6},{4,0},{6,2},{8,12},{10,14},{12,8},{14,10},{16,20},{18,... | collective-permute-start | bytes 1572872 | tf_op jit(solution)/shard_map/ppermute | solution.py:29
  213.3 26.2 %collective-permute-start.42 = (bf16[128,2048]{1,0:T(8,128)(2,1)S(1)}, bf16[128,2048]{1,0:T(8,128)(2,1)S(1)}, u32[]{:S(2)}, u32[]{:S(2)}) collective-permute-start(bf16[128,2048]{1,0:T(8,128)(2,1)S(1)} %collective-permute-done.41), channel_id=1, source_target_pairs={{8,0},{10,2},{12,4},{14,6},{16,24},{18,26},{20,28},{22,30},{9,1},{... | collective-permute-start | bytes 1572872 | tf_op jit(solution)/shard_map/ppermute | solution.py:29
  215.7 18.2 %collective-permute-start.37 = (bf16[1,64,2048]{2,1,0:T(8,128)(2,1)S(1)}, bf16[1,64,2048]{2,1,0:T(8,128)(2,1)S(1)}, u32[]{:S(2)}, u32[]{:S(2)}) collective-permute-start(bf16[1,64,2048]{2,1,0:T(8,128)(2,1)S(1)} %slice.97), channel_id=1, source_target_pairs={{0,8},{2,10},{4,12},{6,14},{8,0},{10,2},{12,4},{14,6},{16,24},{18,... | collective-permute-start | bytes 786440 | tf_op jit(solution)/shard_map/ppermute | solution.py:29
  218.9 21.5 %collective-permute-start.43 = (bf16[64,2048]{1,0:T(8,128)(2,1)S(1)}, bf16[64,2048]{1,0:T(8,128)(2,1)}, u32[]{:S(2)}, u32[]{:S(2)}) collective-permute-start(bf16[64,2048]{1,0:T(8,128)(2,1)S(1)} %copy-done.15), channel_id=1, source_target_pairs={{0,4},{2,6},{4,0},{6,2},{8,12},{10,14},{12,8},{14,10},{16,20},{18,... | collective-permute-start | bytes 786440 | tf_op jit(solution)/shard_map/ppermute | solution.py:29
  237.9 13.4 %collective-permute-start.39 = (bf16[560,512]{1,0:T(8,128)(2,1)S(1)}, bf16[560,512]{1,0:T(8,128)(2,1)S(1)}, u32[]{:S(2)}, u32[]{:S(2)}) collective-permute-start(bf16[560,512]{1,0:T(8,128)(2,1)S(1)} %get-tuple-element.24.refs_1_), channel_id=1, source_target_pairs={{0,1},{1,0},{2,3},{3,2},{4,5},{5,4},{6,7},{7,6},{8,9},{9,8},{10,11... | collective-permute-start | bytes 1720328 | tf_op jit(solution)/shard_map/ppermute | solution.py:29
  239.5 13.7 %copy-start.9 = (bf16[128,2048]{1,0:T(8,128)(2,1)}, bf16[128,2048]{1,0:T(8,128)(2,1)S(1)}, u32[]{:S(2)}) copy-start(bf16[128,2048]{1,0:T(8,128)(2,1)S(1)} %broadcast_select_fusion.2.refs_4_) | copy-start | bytes 1572868
  239.5 13.6 %collective-permute-start.45 = (bf16[128,2048]{1,0:T(8,128)(2,1)S(1)}, bf16[128,2048]{1,0:T(8,128)(2,1)S(1)}, u32[]{:S(2)}, u32[]{:S(2)}) collective-permute-start(bf16[128,2048]{1,0:T(8,128)(2,1)S(1)} %broadcast_select_fusion.2.refs_4_), channel_id=1, source_target_pairs={{0,4},{2,6},{4,0},{6,2},{8,12},{10,14},{12,8},{14,10},{16,20},{18,... | collective-permute-start | bytes 1572872 | tf_op jit(solution)/shard_map/ppermute | solution.py:29
  240.4 12.8 %collective-permute-start.44 = (bf16[1,64,2048]{2,1,0:T(8,128)(2,1)}, bf16[1,64,2048]{2,1,0:T(8,128)(2,1)S(1)}, u32[]{:S(2)}, u32[]{:S(2)}) collective-permute-start(bf16[1,64,2048]{2,1,0:T(8,128)(2,1)} %bitcast.20), channel_id=1, source_target_pairs={{0,8},{2,10},{4,12},{6,14},{8,0},{10,2},{12,4},{14,6},{16,24},{18,... | collective-permute-start | bytes 786440 | tf_op jit(solution)/shard_map/ppermute | solution.py:29
  240.4 11.0 %collective-permute-start.40 = (f32[8,640]{1,0:T(8,128)S(1)}, f32[8,640]{1,0:T(8,128)S(1)}, u32[]{:S(2)}, u32[]{:S(2)}) collective-permute-start(f32[8,640]{1,0:T(8,128)S(1)} %get-tuple-element.25.refs_3_), channel_id=1, source_target_pairs={{0,1},{1,0},{2,3},{3,2},{4,5},{5,4},{6,7},{7,6},{8,9},{9,8},{10,11... | collective-permute-start | bytes 61448 | tf_op jit(solution)/shard_map/ppermute | solution.py:29
  258.7 2.7 %collective-permute-start.46 = (bf16[256,2048]{1,0:T(8,128)(2,1)S(1)}, bf16[256,2048]{1,0:T(8,128)(2,1)S(1)}, u32[]{:S(2)}, u32[]{:S(2)}) collective-permute-start(bf16[256,2048]{1,0:T(8,128)(2,1)S(1)} %get-tuple-element.28), channel_id=1, source_target_pairs={{0,2},{2,0},{4,6},{6,4},{8,10},{10,8},{12,14},{14,12},{16,18},{18,... | collective-permute-start | bytes 3145736 | tf_op jit(solution)/shard_map/ppermute | solution.py:29
  (16 other events, 53.1 us)

commit v4 on v3

--- a/solution.py
+++ b/solution.py
@@ -117,21 +117,27 @@
     out, squares, w, sq, sems = refs[:5]
     fresh = state if first else refs[5]
     copies = load_weight(pieces, arrays, shard, w, sems)
-    rows = state.shape[0]
-    tile = 5 * row_tile if rows % (5 * row_tile) == 0 else row_tile
-
-    @pl.loop(0, rows // tile)
-    def _(i):
-        at = pl.ds(pl.multiple_of(i * tile, row_tile), tile)
-        value = state[at, :].astype(jnp.float32)
+    rows = out.shape[0]
+    skip = state.shape[0] - rows
+    tile = 5 * row_tile
+
+    def update(start, count):
+        at = pl.ds(start, count)
+        value = state[pl.ds(pl.multiple_of(start + skip, row_tile), count), :].astype(jnp.float32)
         if not first:
             value = value + (deltas[0][at, :].astype(jnp.float32) + deltas[1][at, :].astype(jnp.float32))
             rounded = value.astype(jnp.bfloat16)
             fresh[at, :] = rounded
             value = rounded.astype(jnp.float32)
         total = jnp.sum(value * value, axis=1, keepdims=True)
-        sq[at, :] = jnp.broadcast_to(total, (tile, lanes))
-
+        sq[at, :] = jnp.broadcast_to(total, (count, lanes))
+
+    @pl.loop(0, rows // tile)
+    def _(i):
+        update(pl.multiple_of(i * tile, row_tile), tile)
+
+    if rows % tile:
+        update(rows - rows % tile, rows % tile)
     if not first:
         keep = pltpu.make_async_copy(fresh, kept, refs[6])
         keep.start()
@@ -186,11 +192,12 @@
     for copy in copies:
         copy.wait()
     step = min(256, w.shape[1])
+    skip = mixed.shape[0] - out.shape[0]
 
     @pl.loop(0, w.shape[1] // step)
     def _(i):
         at = pl.ds(pl.multiple_of(i * step, step), step)
-        out[:, at] = jnp.dot(mixed[...], w[:, at], preferred_element_type=jnp.float32).astype(jnp.bfloat16)
+        out[:, at] = jnp.dot(mixed[skip:, :], w[:, at], preferred_element_type=jnp.float32).astype(jnp.bfloat16)
 
 
 def last_kernel(pieces, shard, halo, *refs):
@@ -260,8 +267,8 @@
     scale = jnp.broadcast_to(scale, (layers, 8, half))
     place = jnp.stack([(here // 2) * 2 * rows, core]).astype(jnp.int32)
 
-    halo = math.ceil(layers * (window - 1) / row_tile) * row_tile
-    tail = inputs[rows - halo :]
+    halos = [math.ceil((layers - l) * (window - 1) / row_tile) * row_tile for l in range(layers)]
+    tail = inputs[rows - halos[0] :]
     before = move(tail, "sp", lambda s: s + 2 if s % 2 == 1 and s + 2 < count else None)
     relay = move(before, "sp", lambda s: s - 1 if s % 2 == 1 else None)
     sibling = move(inputs, "sp", lambda s: s ^ 1)
@@ -269,17 +276,17 @@
     state = jnp.concatenate(
         [jnp.where(low, relay, before), jnp.where(low, inputs, sibling), jnp.where(low, sibling, inputs)], 0
     )
-    total = state.shape[0]
-    padded = math.ceil(total / lanes) * lanes
     shape = jax.ShapeDtypeStruct
     params = pltpu.CompilerParams(vmem_limit_bytes=16 * 2**20)
-    flops = 2 * total * feats * half
-    cost = pl.CostEstimate(flops=flops, bytes_accessed=2 * (half * feats + 3 * total * feats), transcendentals=0)
-
     in_hbm = lambda v: pltpu.with_memory_space_constraint(v, pltpu.HBM)
     deltas = []
     for l in range(layers):
         first, last = l == 0, l == layers - 1
+        halo = halos[l]
+        total = 2 * rows + halo
+        padded = math.ceil(total / lanes) * lanes
+        flops, moved = 2 * total * feats * half, 2 * (half * feats + 3 * total * feats)
+        cost = pl.CostEstimate(flops=flops, bytes_accessed=moved, transcendentals=0)
         pieces = [(at, index) for _, at, index in found[2 * l]]
         arrays = [v if i == -1 else in_hbm(v) for v, _, i in found[2 * l]]
         outs = [shape((total, half), bf16), shape((8, padded), jnp.float32)]
@@ -323,7 +330,7 @@
             results = [
                 pl.pallas_call(
                     functools.partial(out_kernel, pieces, shard, features, halo),
-                    out_shape=shape((total, feats), bf16),
+                    out_shape=shape((2 * rows + halos[l + 1], feats), bf16),
                     in_specs=[SMEM] + [VMEM] * 6 + [ANY] * len(pieces),
                     out_specs=VMEM,
                     scratch_shapes=[weights, pltpu.VMEM(mixed, bf16), sems],

time: 265 us -> 251 us (0.947)
  waiting for transfers between devices: 165 us -> 159 us
  local copies, waits for them, and re-layouts: 14.6 us -> 10.6 us
    ppermute x47, waiting for transfers between devices: 165 us -> 159 us  [move(): lax.ppermute(value, axis, [(s, t) for s, t in pairs if t is not None])]
  transfers between devices with their start and end apart: 47 -> 47, of which waited for: 16 -> 18; matrix products, arithmetic and copies ran while one was open for 7% -> 6% of each run, Pallas kernels for 4% -> 6%
where the time goes in v4:
time: 251 us; the launch traced here: 249 us
  waiting for transfers between devices  159 us (63%)
  starting transfers between devices  46.9 us (19%)
  Pallas kernels  24.4 us (10%)
  local copies, waits for them, and re-layouts  10.6 us (4%)
  other arithmetic  7.14 us (3%)
    ppermute x47, waiting for transfers between devices, move(): lax.ppermute(value, axis, [(s, t) for s, t in pairs if t is not None])  159 us
    ppermute x47, starting transfers between devices, move(): lax.ppermute(value, axis, [(s, t) for s, t in pairs if t is not None])  46.9 us
    pallas_call x2, Pallas kernels, body(): pl.pallas_call(functools.partial(out_kernel, pieces, shard, features, hal...  8.95 us
    pallas_call x3, Pallas kernels, body(): pl.pallas_call(functools.partial(in_kernel, first, pieces, shard), out_sh...  8.93 us
  transfers between devices with their start and end apart: 47, of which 18 were waited for; matrix products, arithmetic and copies ran while one was open for 6% of the time, Pallas kernels for 6%

profile of v4, /device:TPU:4, one launch (start us, length us, event | category | flops | bytes accessed | tf_op | source)
XLA Modules:
  0.0 248.5 jit_solution(14860698284209631841)
XLA Ops:
  0.0 1.7 slice.70
  1.7 1.3 collective-permute-start
  3.1 1.3 fusion
  4.4 1.0 slice_bitcast_fusion.1
  5.4 1.6 collective-permute-start.3
  6.9 1.4 collective-permute-start.4
  8.3 1.0 slice_bitcast_fusion.5
  9.3 3.7 %collective-permute-start.15 = (bf16[1,64,2048]{2,1,0:T(8,128)(2,1)}, bf16[1,64,2048]{2,1,0:T(8,128)(2,1)}, u32[]{:S(2)}, u32[]{:S(2)}) collective-permute-start(bf16[1,64,2048]{2,1,0:T(8,128)(2,1)} %get-tuple-element.36), channel_id=1, source_target_pairs={{0,8},{2,10},{4,12},{6,14},{8,0},{10,2},{12,4},{14,6},{16,24},{18,... | collective-permute-start | bytes 786440 | tf_op jit(solution)/shard_map/ppermute | solution.py:29
  13.7 0.7 fusion.3
  15.4 0.8 slice.72
  16.2 0.8 slice.92
  17.6 2.8 %collective-permute-done.15 = bf16[1,64,2048]{2,1,0:T(8,128)(2,1)} collective-permute-done((bf16[1,64,2048]{2,1,0:T(8,128)(2,1)}, bf16[1,64,2048]{2,1,0:T(8,128)(2,1)}, u32[]{:S(2)}, u32[]{:S(2)}) %collective-permute-start.15) | collective-permute-done | bytes 262176 | tf_op jit(solution)/shard_map/ppermute | solution.py:29
  20.4 1.3 collective-permute-start.1
  21.7 1.1 pad_maximum_fusion.1.refs_7_
  22.8 1.7 collective-permute-start.12
  25.2 1.3 collective-permute-start.5
  26.5 16.8 %collective-permute-done.5 = bf16[64,2048]{1,0:T(8,128)(2,1)S(1)} collective-permute-done((bf16[64,2048]{1,0:T(8,128)(2,1)}, bf16[64,2048]{1,0:T(8,128)(2,1)S(1)}, u32[]{:S(2)}, u32[]{:S(2)}) %collective-permute-start.5) | collective-permute-done | bytes 262176 | tf_op jit(solution)/shard_map/ppermute | solution.py:29
  44.1 1.3 collective-permute-start.7
  45.4 10.0 %collective-permute-done.7 = bf16[64,2048]{1,0:T(8,128)(2,1)S(1)} collective-permute-done((bf16[64,2048]{1,0:T(8,128)(2,1)S(1)}, bf16[64,2048]{1,0:T(8,128)(2,1)S(1)}, u32[]{:S(2)}, u32[]{:S(2)}) %collective-permute-start.7) | collective-permute-done | bytes 262176 | tf_op jit(solution)/shard_map/ppermute | solution.py:29
  55.4 2.1 collective-permute-start.10
  57.5 1.3 collective-permute-start.17
  59.0 5.8 %collective-permute-done.9.refs_6_ = bf16[64,2048]{1,0:T(8,128)(2,1)S(1)} collective-permute-done((bf16[64,2048]{1,0:T(8,128)(2,1)}, bf16[64,2048]{1,0:T(8,128)(2,1)S(1)}, u32[]{:S(2)}, u32[]{:S(2)}) %collective-permute-start.9) | collective-permute-done | bytes 262176 | tf_op jit(solution)/shard_map/ppermute | solution.py:29
  65.5 4.9 %collective-permute-done.10.refs_7_ = bf16[64,2048]{1,0:T(8,128)(2,1)S(1)} collective-permute-done((bf16[64,2048]{1,0:T(8,128)(2,1)S(1)}, bf16[64,2048]{1,0:T(8,128)(2,1)S(1)}, u32[]{:S(2)}, u32[]{:S(2)}) %collective-permute-start.10) | collective-permute-done | bytes 262176 | tf_op jit(solution)/shard_map/ppermute | solution.py:29
  70.5 5.5 %collective-permute-done.11.refs_8_ = bf16[64,2048]{1,0:T(8,128)(2,1)S(1)} collective-permute-done((bf16[64,2048]{1,0:T(8,128)(2,1)S(1)}, bf16[64,2048]{1,0:T(8,128)(2,1)S(1)}, u32[]{:S(2)}, u32[]{:S(2)}) %collective-permute-start.11) | collective-permute-done | bytes 262176 | tf_op jit(solution)/shard_map/ppermute | solution.py:29
  76.0 2.8 %shard_map.64 = (bf16[560,512]{1,0:T(8,128)(2,1)S(1)}, f32[8,640]{1,0:T(8,128)S(1)}) custom-call(bf16[560,2048]{1,0:T(8,128)(2,1)S(1)} %pad_maximum_fusion.refs_0_, bf16[64,2048]{1,0:T(8,128)(2,1)} %copy-done.15, bf16[1,64,2048]{2,1,0:T(8,128)(2,1)} %collective-permute-done.3.refs_2_, bf16[64,2048]{1,0:T(8,128)(2,1)} %copy-done.20, ...), custom_call_target="tpu_custom_call" | custom-call | flops 1174405120 | bytes 8978432 | tf_op jit(solution)/shard_map/pallas_call | solution.py:295
  78.8 1.6 collective-permute-start.13
  80.5 2.1 collective-permute-start.20
  82.6 1.7 collective-permute-done.22
  84.3 1.6 collective-permute-start.14
  86.0 0.7 collective-permute-start.23
  87.2 4.3 %collective-permute-done.14.refs_4_ = f32[8,640]{1,0:T(8,128)S(1)} collective-permute-done((f32[8,640]{1,0:T(8,128)S(1)}, f32[8,640]{1,0:T(8,128)S(1)}, u32[]{:S(2)}, u32[]{:S(2)}) %collective-permute-start.14) | collective-permute-done | bytes 20512 | tf_op jit(solution)/shard_map/ppermute | solution.py:29
  91.5 5.4 %collective-permute-done.20.refs_11_ = bf16[128,2048]{1,0:T(8,128)(2,1)S(1)} collective-permute-done((bf16[128,2048]{1,0:T(8,128)(2,1)S(1)}, bf16[128,2048]{1,0:T(8,128)(2,1)S(1)}, u32[]{:S(2)}, u32[]{:S(2)}) %collective-permute-start.20) | collective-permute-done | bytes 524320 | tf_op jit(solution)/shard_map/ppermute | solution.py:29
  97.0 4.5 %shard_map.65.refs_1_ = bf16[544,2048]{1,0:T(8,128)(2,1)S(1)} custom-call(s32[2]{0:T(128)S(1)} %pad_add_fusion.refs_0_, bf16[560,512]{1,0:T(8,128)(2,1)S(1)} %get-tuple-element.18.refs_1_, bf16[560,512]{1,0:T(8,128)(2,1)S(1)} %collective-permute-done.13.refs_2_, f32[8,640]{1,0:T(8,128)S(1)} %get-tuple-element.19.refs_3_, ...), custom_call_target="tpu_custom_call" | custom-call | flops 1174405120 | bytes 8978432 | tf_op jit(solution)/shard_map/pallas_call | solution.py:331
  101.6 1.3 collective-permute-start.24
  102.9 0.7 slice_bitcast_fusion.4
  103.6 1.0 pad_maximum_fusion.3.refs_7_
  104.6 0.7 collective-permute-start.29
  105.4 12.4 %collective-permute-done.24 = bf16[128,2048]{1,0:T(8,128)(2,1)S(1)} collective-permute-done((bf16[128,2048]{1,0:T(8,128)(2,1)S(1)}, bf16[128,2048]{1,0:T(8,128)(2,1)S(1)}, u32[]{:S(2)}, u32[]{:S(2)}) %collective-permute-start.24) | collective-permute-done | bytes 524320 | tf_op jit(solution)/shard_map/ppermute | solution.py:29
  118.2 1.3 collective-permute-start.30
  119.5 1.8 collective-permute-start.25
  121.3 15.7 %collective-permute-done.25.refs_6_ = bf16[64,2048]{1,0:T(8,128)(2,1)S(1)} collective-permute-done((bf16[64,2048]{1,0:T(8,128)(2,1)S(1)}, bf16[64,2048]{1,0:T(8,128)(2,1)S(1)}, u32[]{:S(2)}, u32[]{:S(2)}) %collective-permute-start.25) | collective-permute-done | bytes 262176 | tf_op jit(solution)/shard_map/ppermute | solution.py:29
  137.7 3.1 %shard_map.66 = (bf16[544,2048]{1,0:T(8,128)(2,1)}, bf16[544,512]{1,0:T(8,128)(2,1)S(1)}, f32[8,640]{1,0:T(8,128)S(1)}) custom-call(bf16[560,2048]{1,0:T(8,128)(2,1)S(1)} %pad_maximum_fusion.refs_0_, bf16[544,2048]{1,0:T(8,128)(2,1)S(1)} %shard_map.65.refs_1_, bf16[544,2048]{1,0:T(8,128)(2,1)S(1)} %collective-permute-done.21.refs_2_, ...), custom_call_target="tpu_custom_call" | custom-call | flops 1140850688 | bytes 8781824 | tf_op jit(solution)/shard_map/pallas_call | solution.py:295
  140.8 1.6 collective-permute-start.27
  142.8 1.7 collective-permute-start.31
  145.4 17.6 %collective-permute-done.31.refs_9_ = bf16[64,2048]{1,0:T(8,128)(2,1)} collective-permute-done((bf16[64,2048]{1,0:T(8,128)(2,1)S(1)}, bf16[64,2048]{1,0:T(8,128)(2,1)}, u32[]{:S(2)}, u32[]{:S(2)}) %collective-permute-start.31) | collective-permute-done | bytes 262176 | tf_op jit(solution)/shard_map/ppermute | solution.py:29
  163.0 3.1 %collective-permute-done.32.refs_10_ = bf16[64,2048]{1,0:T(8,128)(2,1)} collective-permute-done((bf16[64,2048]{1,0:T(8,128)(2,1)}, bf16[64,2048]{1,0:T(8,128)(2,1)}, u32[]{:S(2)}, u32[]{:S(2)}) %collective-permute-start.32) | collective-permute-done | bytes 262176 | tf_op jit(solution)/shard_map/ppermute | solution.py:29
  166.2 4.5 %shard_map.67.refs_1_ = bf16[528,2048]{1,0:T(8,128)(2,1)S(1)} custom-call(s32[2]{0:T(128)S(1)} %pad_add_fusion.refs_0_, bf16[544,512]{1,0:T(8,128)(2,1)S(1)} %get-tuple-element.21.refs_1_, bf16[544,512]{1,0:T(8,128)(2,1)S(1)} %collective-permute-done.27.refs_2_, f32[8,640]{1,0:T(8,128)S(1)} %get-tuple-element.22.refs_3_, ...), custom_call_target="tpu_custom_call" | custom-call | flops 1140850688 | bytes 8781824 | tf_op jit(solution)/shard_map/pallas_call | solution.py:331
  170.8 0.8 collective-permute-start.35
  171.6 1.3 collective-permute-start.36
  173.0 0.7 collective-permute-start.41
  173.7 25.7 %collective-permute-done.36 = bf16[128,2048]{1,0:T(8,128)(2,1)S(1)} collective-permute-done((bf16[128,2048]{1,0:T(8,128)(2,1)S(1)}, bf16[128,2048]{1,0:T(8,128)(2,1)S(1)}, u32[]{:S(2)}, u32[]{:S(2)}) %collective-permute-start.36) | collective-permute-done | bytes 524320 | tf_op jit(solution)/shard_map/ppermute | solution.py:29
  199.8 1.5 collective-permute-start.42
  201.3 1.0 slice.97
  202.3 3.4 %collective-permute-start.37 = (bf16[1,64,2048]{2,1,0:T(8,128)(2,1)S(1)}, bf16[1,64,2048]{2,1,0:T(8,128)(2,1)S(1)}, u32[]{:S(2)}, u32[]{:S(2)}) collective-permute-start(bf16[1,64,2048]{2,1,0:T(8,128)(2,1)S(1)} %slice.97), channel_id=1, source_target_pairs={{0,8},{2,10},{4,12},{6,14},{8,0},{10,2},{12,4},{14,6},{16,24},{18,... | collective-permute-start | bytes 786440 | tf_op jit(solution)/shard_map/ppermute | solution.py:29
  205.7 1.1 collective-permute-start.43
  206.8 14.0 %collective-permute-done.37 = bf16[1,64,2048]{2,1,0:T(8,128)(2,1)S(1)} collective-permute-done((bf16[1,64,2048]{2,1,0:T(8,128)(2,1)S(1)}, bf16[1,64,2048]{2,1,0:T(8,128)(2,1)S(1)}, u32[]{:S(2)}, u32[]{:S(2)}) %collective-permute-start.37) | collective-permute-done | bytes 262176 | tf_op jit(solution)/shard_map/ppermute | solution.py:29
  221.5 3.0 %shard_map.68 = (bf16[528,2048]{1,0:T(8,128)(2,1)}, bf16[528,512]{1,0:T(8,128)(2,1)S(1)}, f32[8,640]{1,0:T(8,128)S(1)}) custom-call(bf16[544,2048]{1,0:T(8,128)(2,1)S(1)} %copy-done.1, bf16[528,2048]{1,0:T(8,128)(2,1)S(1)} %shard_map.67.refs_1_, bf16[528,2048]{1,0:T(8,128)(2,1)S(1)} %collective-permute-done.34.refs_2_, bf16[128,2048]{1,0:T(8,128)(2,1)} %copy-done.7, ...), custom_call_target="tpu_custom_call" | custom-call | flops 1107296256 | bytes 8585216 | tf_op jit(solution)/shard_map/pallas_call | solution.py:295
  225.2 0.8 collective-permute-start.45
  226.1 1.6 collective-permute-start.40
  227.7 9.6 %collective-permute-done.40.refs_4_ = f32[8,640]{1,0:T(8,128)S(1)} collective-permute-done((f32[8,640]{1,0:T(8,128)S(1)}, f32[8,640]{1,0:T(8,128)S(1)}, u32[]{:S(2)}, u32[]{:S(2)}) %collective-permute-start.40) | collective-permute-done | bytes 20512 | tf_op jit(solution)/shard_map/ppermute | solution.py:29
  237.3 1.7 shard_map.69.refs_1_
  239.7 4.8 %shard_map.70 = (f32[256,2048]{1,0:T(8,128)S(1)}, bf16[256,2048]{1,0:T(8,128)(2,1)S(1)}) custom-call(s32[2]{0:T(128)S(1)} %pad_add_fusion.refs_0_, bf16[528,512]{1,0:T(8,128)(2,1)S(1)} %shard_map.69.refs_1_, bf16[528,2048]{1,0:T(8,128)(2,1)} %get-tuple-element.26.refs_2_, bf16[128,2048]{1,0:T(8,128)(2,1)} %copy-done.5, bf16[128,2048]{1,0:T(8,128)(2,1)} %copy-done.9, ...), custom_call_target="tpu_custom_call" | custom-call | flops 1107296256 | bytes 8585216 | tf_op jit(solution)/shard_map/pallas_call | solution.py:348
  244.6 2.6 %collective-permute-done.46 = bf16[256,2048]{1,0:T(8,128)(2,1)S(1)} collective-permute-done((bf16[256,2048]{1,0:T(8,128)(2,1)S(1)}, bf16[256,2048]{1,0:T(8,128)(2,1)S(1)}, u32[]{:S(2)}, u32[]{:S(2)}) %collective-permute-start.46) | collective-permute-done | bytes 1048608 | tf_op jit(solution)/shard_map/ppermute | solution.py:29
  247.2 1.3 add_convert_fusion
  (143 shorter events, 10.7 us)
Async XLA Ops:
  0.0 57.5 %collective-permute-start.2 = (bf16[256,2048]{1,0:T(8,128)(2,1)}, bf16[256,2048]{1,0:T(8,128)(2,1)S(1)}, u32[]{:S(2)}, u32[]{:S(2)}) collective-permute-start(bf16[256,2048]{1,0:T(8,128)(2,1)} %param.6), channel_id=1, source_target_pairs={{0,2},{2,0},{4,6},{6,4},{8,10},{10,8},{12,14},{14,12},{16,18},{18,... | collective-permute-start | bytes 3145736 | tf_op jit(solution)/shard_map/ppermute | solution.py:29
  1.7 15.4 %collective-permute-start = (bf16[48,2048]{1,0:T(8,128)(2,1)}, bf16[48,2048]{1,0:T(8,128)(2,1)}, u32[]{:S(2)}, u32[]{:S(2)}) collective-permute-start(bf16[48,2048]{1,0:T(8,128)(2,1)} %slice.70), channel_id=1, source_target_pairs={{2,6},{6,10},{10,14},{14,18},{18,22},{22,26},{26,30},{3,7},{7,11},... | collective-permute-start | bytes 589832 | tf_op jit(solution)/shard_map/ppermute | solution.py:29
  4.4 10.2 %copy-start.30 = (f32[3,1024]{1,0:T(4,128)S(1)}, f32[3,1024]{1,0:T(4,128)}, u32[]{:S(2)}) copy-start(f32[3,1024]{1,0:T(4,128)} %param.9) | copy-start | bytes 36868
  5.4 17.4 %copy-start.15 = (bf16[64,2048]{1,0:T(8,128)(2,1)}, bf16[64,2048]{1,0:T(8,128)(2,1)S(1)}, u32[]{:S(2)}) copy-start(bf16[64,2048]{1,0:T(8,128)(2,1)S(1)} %get-tuple-element.39.refs_1_) | copy-start | bytes 786436
  5.4 17.5 %collective-permute-start.3 = (bf16[1,64,2048]{2,1,0:T(8,128)(2,1)}, bf16[1,64,2048]{2,1,0:T(8,128)(2,1)}, u32[]{:S(2)}, u32[]{:S(2)}) collective-permute-start(bf16[1,64,2048]{2,1,0:T(8,128)(2,1)} %get-tuple-element.41), channel_id=1, source_target_pairs={{0,8},{2,10},{4,12},{6,14},{8,0},{10,2},{12,4},{14,6},{16,24},{18,... | collective-permute-start | bytes 786440 | tf_op jit(solution)/shard_map/ppermute | solution.py:29
  6.9 17.6 %collective-permute-start.4 = (bf16[64,2048]{1,0:T(8,128)(2,1)S(1)}, bf16[64,2048]{1,0:T(8,128)(2,1)}, u32[]{:S(2)}, u32[]{:S(2)}) collective-permute-start(bf16[64,2048]{1,0:T(8,128)(2,1)S(1)} %get-tuple-element.39.refs_1_), channel_id=1, source_target_pairs={{8,16},{10,18},{12,20},{14,22},{16,8},{18,10},{20,12},{22,14},{9,1... | collective-permute-start | bytes 786440 | tf_op jit(solution)/shard_map/ppermute | solution.py:29
  9.3 11.2 %collective-permute-start.15 = (bf16[1,64,2048]{2,1,0:T(8,128)(2,1)}, bf16[1,64,2048]{2,1,0:T(8,128)(2,1)}, u32[]{:S(2)}, u32[]{:S(2)}) collective-permute-start(bf16[1,64,2048]{2,1,0:T(8,128)(2,1)} %get-tuple-element.36), channel_id=1, source_target_pairs={{0,8},{2,10},{4,12},{6,14},{8,0},{10,2},{12,4},{14,6},{16,24},{18,... | collective-permute-start | bytes 786440 | tf_op jit(solution)/shard_map/ppermute | solution.py:29
  16.2 42.6 %copy-start.14 = (bf16[256,2048]{1,0:T(8,128)(2,1)S(1)}, bf16[256,2048]{1,0:T(8,128)(2,1)}, u32[]{:S(2)}) copy-start(bf16[256,2048]{1,0:T(8,128)(2,1)} %param.6) | copy-start | bytes 3145732
  17.1 53.3 %collective-permute-start.8 = (bf16[3,64,2048]{2,1,0:T(8,128)(2,1)S(1)}, bf16[3,64,2048]{2,1,0:T(8,128)(2,1)S(1)}, u32[]{:S(2)}, u32[]{:S(2)}) collective-permute-start(bf16[3,64,2048]{2,1,0:T(8,128)(2,1)S(1)} %fusion), channel_id=1, source_target_pairs={{0,4},{2,6},{4,0},{6,2},{8,12},{10,14},{12,8},{14,10},{16,20},{18,... | collective-permute-start | bytes 2359304 | tf_op jit(solution)/shard_map/ppermute | solution.py:29
  20.4 4.7 %collective-permute-start.1 = (bf16[48,2048]{1,0:T(8,128)(2,1)}, bf16[48,2048]{1,0:T(8,128)(2,1)S(1)}, u32[]{:S(2)}, u32[]{:S(2)}) collective-permute-start(bf16[48,2048]{1,0:T(8,128)(2,1)} %collective-permute-done), channel_id=1, source_target_pairs={{2,0},{6,4},{10,8},{14,12},{18,16},{22,20},{26,24},{30,28},{3,1},{... | collective-permute-start | bytes 589832 | tf_op jit(solution)/shard_map/ppermute | solution.py:29
  22.8 36.2 %copy-start.4 = (bf16[128,2048]{1,0:T(8,128)(2,1)}, bf16[128,2048]{1,0:T(8,128)(2,1)S(1)}, u32[]{:S(2)}) copy-start(bf16[128,2048]{1,0:T(8,128)(2,1)S(1)} %pad_maximum_fusion.1.refs_7_) | copy-start | bytes 1572868
  22.8 56.0 %collective-permute-start.12 = (bf16[2,64,2048]{2,1,0:T(8,128)(2,1)}, bf16[2,64,2048]{2,1,0:T(8,128)(2,1)S(1)}, u32[]{:S(2)}, u32[]{:S(2)}) collective-permute-start(bf16[2,64,2048]{2,1,0:T(8,128)(2,1)} %slice.72), channel_id=1, source_target_pairs={{0,8},{2,10},{4,12},{6,14},{8,0},{10,2},{12,4},{14,6},{16,24},{18,... | collective-permute-start | bytes 1572872 | tf_op jit(solution)/shard_map/ppermute | solution.py:29
  24.5 19.5 %collective-permute-start.6 = (bf16[64,2048]{1,0:T(8,128)(2,1)}, bf16[64,2048]{1,0:T(8,128)(2,1)S(1)}, u32[]{:S(2)}, u32[]{:S(2)}) collective-permute-start(bf16[64,2048]{1,0:T(8,128)(2,1)} %bitcast.4), channel_id=1, source_target_pairs={{8,16},{10,18},{12,20},{14,22},{16,8},{18,10},{20,12},{22,14},{9,1... | collective-permute-start | bytes 786440 | tf_op jit(solution)/shard_map/ppermute | solution.py:29
  25.2 18.2 %collective-permute-start.5 = (bf16[64,2048]{1,0:T(8,128)(2,1)}, bf16[64,2048]{1,0:T(8,128)(2,1)S(1)}, u32[]{:S(2)}, u32[]{:S(2)}) collective-permute-start(bf16[64,2048]{1,0:T(8,128)(2,1)} %collective-permute-done.4), channel_id=1, source_target_pairs={{8,0},{10,2},{12,4},{14,6},{16,24},{18,26},{20,28},{22,30},{9,1},{... | collective-permute-start | bytes 786440 | tf_op jit(solution)/shard_map/ppermute | solution.py:29
  43.4 12.1 %collective-permute-start.16 = (bf16[128,2048]{1,0:T(8,128)(2,1)S(1)}, bf16[128,2048]{1,0:T(8,128)(2,1)S(1)}, u32[]{:S(2)}, u32[]{:S(2)}) collective-permute-start(bf16[128,2048]{1,0:T(8,128)(2,1)S(1)} %pad_maximum_fusion.1.refs_7_), channel_id=1, source_target_pairs={{8,16},{10,18},{12,20},{14,22},{16,8},{18,10},{20,12},{22,14},{9,1... | collective-permute-start | bytes 1572872 | tf_op jit(solution)/shard_map/ppermute | solution.py:29
  44.1 11.3 %collective-permute-start.7 = (bf16[64,2048]{1,0:T(8,128)(2,1)S(1)}, bf16[64,2048]{1,0:T(8,128)(2,1)S(1)}, u32[]{:S(2)}, u32[]{:S(2)}) collective-permute-start(bf16[64,2048]{1,0:T(8,128)(2,1)S(1)} %collective-permute-done.6), channel_id=1, source_target_pairs={{8,0},{10,2},{12,4},{14,6},{16,24},{18,26},{20,28},{22,30},{9,1},{... | collective-permute-start | bytes 786440 | tf_op jit(solution)/shard_map/ppermute | solution.py:29
  45.4 13.6 %copy-start.20 = (bf16[64,2048]{1,0:T(8,128)(2,1)}, bf16[64,2048]{1,0:T(8,128)(2,1)S(1)}, u32[]{:S(2)}) copy-start(bf16[64,2048]{1,0:T(8,128)(2,1)S(1)} %broadcast_select_fusion.8.refs_3_) | copy-start | bytes 786436
  55.4 9.4 %collective-permute-start.9 = (bf16[64,2048]{1,0:T(8,128)(2,1)}, bf16[64,2048]{1,0:T(8,128)(2,1)S(1)}, u32[]{:S(2)}, u32[]{:S(2)}) collective-permute-start(bf16[64,2048]{1,0:T(8,128)(2,1)} %bitcast.4), channel_id=1, source_target_pairs={{0,4},{2,6},{4,0},{6,2},{8,12},{10,14},{12,8},{14,10},{16,20},{18,... | collective-permute-start | bytes 786440 | tf_op jit(solution)/shard_map/ppermute | solution.py:29
  55.4 14.9 %collective-permute-start.10 = (bf16[64,2048]{1,0:T(8,128)(2,1)S(1)}, bf16[64,2048]{1,0:T(8,128)(2,1)S(1)}, u32[]{:S(2)}, u32[]{:S(2)}) collective-permute-start(bf16[64,2048]{1,0:T(8,128)(2,1)S(1)} %broadcast_select_fusion.8.refs_3_), channel_id=1, source_target_pairs={{0,4},{2,6},{4,0},{6,2},{8,12},{10,14},{12,8},{14,10},{16,20},{18,... | collective-permute-start | bytes 786440 | tf_op jit(solution)/shard_map/ppermute | solution.py:29
  57.5 22.9 %collective-permute-start.17 = (bf16[128,2048]{1,0:T(8,128)(2,1)S(1)}, bf16[128,2048]{1,0:T(8,128)(2,1)S(1)}, u32[]{:S(2)}, u32[]{:S(2)}) collective-permute-start(bf16[128,2048]{1,0:T(8,128)(2,1)S(1)} %collective-permute-done.16), channel_id=1, source_target_pairs={{8,0},{10,2},{12,4},{14,6},{16,24},{18,26},{20,28},{22,30},{9,1},{... | collective-permute-start | bytes 1572872 | tf_op jit(solution)/shard_map/ppermute | solution.py:29
  64.8 11.2 %collective-permute-start.11 = (bf16[64,2048]{1,0:T(8,128)(2,1)S(1)}, bf16[64,2048]{1,0:T(8,128)(2,1)S(1)}, u32[]{:S(2)}, u32[]{:S(2)}) collective-permute-start(bf16[64,2048]{1,0:T(8,128)(2,1)S(1)} %broadcast_select_fusion.7.refs_4_), channel_id=1, source_target_pairs={{0,4},{2,6},{4,0},{6,2},{8,12},{10,14},{12,8},{14,10},{16,20},{18,... | collective-permute-start | bytes 786440 | tf_op jit(solution)/shard_map/ppermute | solution.py:29
  70.4 15.6 %collective-permute-start.18 = (bf16[64,2048]{1,0:T(8,128)(2,1)S(1)}, bf16[64,2048]{1,0:T(8,128)(2,1)S(1)}, u32[]{:S(2)}, u32[]{:S(2)}) collective-permute-start(bf16[64,2048]{1,0:T(8,128)(2,1)S(1)} %copy-done.19), channel_id=1, source_target_pairs={{0,4},{2,6},{4,0},{6,2},{8,12},{10,14},{12,8},{14,10},{16,20},{18,... | collective-permute-start | bytes 786440 | tf_op jit(solution)/shard_map/ppermute | solution.py:29
  70.4 13.9 %collective-permute-start.22 = (bf16[2,64,2048]{2,1,0:T(8,128)(2,1)S(1)}, bf16[2,64,2048]{2,1,0:T(8,128)(2,1)S(1)}, u32[]{:S(2)}, u32[]{:S(2)}) collective-permute-start(bf16[2,64,2048]{2,1,0:T(8,128)(2,1)S(1)} %copy-done.22), channel_id=1, source_target_pairs={{0,8},{2,10},{4,12},{6,14},{8,0},{10,2},{12,4},{14,6},{16,24},{18,... | collective-permute-start | bytes 1572872 | tf_op jit(solution)/shard_map/ppermute | solution.py:29
  76.0 11.2 %collective-permute-start.19 = (bf16[64,2048]{1,0:T(8,128)(2,1)}, bf16[64,2048]{1,0:T(8,128)(2,1)S(1)}, u32[]{:S(2)}, u32[]{:S(2)}) collective-permute-start(bf16[64,2048]{1,0:T(8,128)(2,1)} %bitcast.10), channel_id=1, source_target_pairs={{0,4},{2,6},{4,0},{6,2},{8,12},{10,14},{12,8},{14,10},{16,20},{18,... | collective-permute-start | bytes 786440 | tf_op jit(solution)/shard_map/ppermute | solution.py:29
  78.8 12.7 %collective-permute-start.13 = (bf16[560,512]{1,0:T(8,128)(2,1)S(1)}, bf16[560,512]{1,0:T(8,128)(2,1)S(1)}, u32[]{:S(2)}, u32[]{:S(2)}) collective-permute-start(bf16[560,512]{1,0:T(8,128)(2,1)S(1)} %get-tuple-element.18.refs_1_), channel_id=1, source_target_pairs={{0,1},{1,0},{2,3},{3,2},{4,5},{5,4},{6,7},{7,6},{8,9},{9,8},{10,11... | collective-permute-start | bytes 1720328 | tf_op jit(solution)/shard_map/ppermute | solution.py:29
  80.5 16.5 %copy-start.8 = (bf16[128,2048]{1,0:T(8,128)(2,1)}, bf16[128,2048]{1,0:T(8,128)(2,1)S(1)}, u32[]{:S(2)}) copy-start(bf16[128,2048]{1,0:T(8,128)(2,1)S(1)} %broadcast_select_fusion.6.refs_8_) | copy-start | bytes 1572868
  80.5 16.5 %collective-permute-start.20 = (bf16[128,2048]{1,0:T(8,128)(2,1)S(1)}, bf16[128,2048]{1,0:T(8,128)(2,1)S(1)}, u32[]{:S(2)}, u32[]{:S(2)}) collective-permute-start(bf16[128,2048]{1,0:T(8,128)(2,1)S(1)} %broadcast_select_fusion.6.refs_8_), channel_id=1, source_target_pairs={{0,4},{2,6},{4,0},{6,2},{8,12},{10,14},{12,8},{14,10},{16,20},{18,... | collective-permute-start | bytes 1572872 | tf_op jit(solution)/shard_map/ppermute | solution.py:29
  84.3 7.2 %collective-permute-start.14 = (f32[8,640]{1,0:T(8,128)S(1)}, f32[8,640]{1,0:T(8,128)S(1)}, u32[]{:S(2)}, u32[]{:S(2)}) collective-permute-start(f32[8,640]{1,0:T(8,128)S(1)} %get-tuple-element.19.refs_3_), channel_id=1, source_target_pairs={{0,1},{1,0},{2,3},{3,2},{4,5},{5,4},{6,7},{7,6},{8,9},{9,8},{10,11... | collective-permute-start | bytes 61448 | tf_op jit(solution)/shard_map/ppermute | solution.py:29
  85.9 15.5 %copy-start.6 = (bf16[128,2048]{1,0:T(8,128)(2,1)}, bf16[128,2048]{1,0:T(8,128)(2,1)S(1)}, u32[]{:S(2)}) copy-start(bf16[128,2048]{1,0:T(8,128)(2,1)S(1)} %pad_maximum_fusion.2.refs_3_) | copy-start | bytes 1572868
  85.9 11.0 %copy-start.23 = (bf16[64,2048]{1,0:T(8,128)(2,1)}, bf16[64,2048]{1,0:T(8,128)(2,1)S(1)}, u32[]{:S(2)}) copy-start(bf16[64,2048]{1,0:T(8,128)(2,1)S(1)} %collective-permute-done.18.refs_9_) | copy-start | bytes 786436
  86.0 15.6 %collective-permute-start.23 = (bf16[128,2048]{1,0:T(8,128)(2,1)S(1)}, bf16[128,2048]{1,0:T(8,128)(2,1)S(1)}, u32[]{:S(2)}, u32[]{:S(2)}) collective-permute-start(bf16[128,2048]{1,0:T(8,128)(2,1)S(1)} %pad_maximum_fusion.2.refs_3_), channel_id=1, source_target_pairs={{8,16},{10,18},{12,20},{14,22},{16,8},{18,10},{20,12},{22,14},{9,1... | collective-permute-start | bytes 1572872 | tf_op jit(solution)/shard_map/ppermute | solution.py:29
  101.5 35.5 %collective-permute-start.21 = (bf16[544,2048]{1,0:T(8,128)(2,1)S(1)}, bf16[544,2048]{1,0:T(8,128)(2,1)S(1)}, u32[]{:S(2)}, u32[]{:S(2)}) collective-permute-start(bf16[544,2048]{1,0:T(8,128)(2,1)S(1)} %shard_map.65.refs_1_), channel_id=1, source_target_pairs={{0,2},{2,0},{4,6},{6,4},{8,10},{10,8},{12,14},{14,12},{16,18},{18,... | collective-permute-start | bytes 6684680 | tf_op jit(solution)/shard_map/ppermute | solution.py:29
  101.6 16.2 %collective-permute-start.24 = (bf16[128,2048]{1,0:T(8,128)(2,1)S(1)}, bf16[128,2048]{1,0:T(8,128)(2,1)S(1)}, u32[]{:S(2)}, u32[]{:S(2)}) collective-permute-start(bf16[128,2048]{1,0:T(8,128)(2,1)S(1)} %collective-permute-done.23), channel_id=1, source_target_pairs={{8,0},{10,2},{12,4},{14,6},{16,24},{18,26},{20,28},{22,30},{9,1},{... | collective-permute-start | bytes 1572872 | tf_op jit(solution)/shard_map/ppermute | solution.py:29
  104.6 36.1 %copy-start.12 = (bf16[128,2048]{1,0:T(8,128)(2,1)}, bf16[128,2048]{1,0:T(8,128)(2,1)S(1)}, u32[]{:S(2)}) copy-start(bf16[128,2048]{1,0:T(8,128)(2,1)S(1)} %pad_maximum_fusion.3.refs_7_) | copy-start | bytes 1572868
  104.6 13.5 %collective-permute-start.29 = (bf16[128,2048]{1,0:T(8,128)(2,1)S(1)}, bf16[128,2048]{1,0:T(8,128)(2,1)S(1)}, u32[]{:S(2)}, u32[]{:S(2)}) collective-permute-start(bf16[128,2048]{1,0:T(8,128)(2,1)S(1)} %pad_maximum_fusion.3.refs_7_), channel_id=1, source_target_pairs={{8,16},{10,18},{12,20},{14,22},{16,8},{18,10},{20,12},{22,14},{9,1... | collective-permute-start | bytes 1572872 | tf_op jit(solution)/shard_map/ppermute | solution.py:29
  117.8 19.2 %copy-start.11 = (bf16[128,2048]{1,0:T(8,128)(2,1)}, bf16[128,2048]{1,0:T(8,128)(2,1)S(1)}, u32[]{:S(2)}) copy-start(bf16[128,2048]{1,0:T(8,128)(2,1)S(1)} %broadcast_select_fusion.5.refs_4_) | copy-start | bytes 1572868
  117.8 19.1 %collective-permute-start.26 = (bf16[128,2048]{1,0:T(8,128)(2,1)S(1)}, bf16[128,2048]{1,0:T(8,128)(2,1)S(1)}, u32[]{:S(2)}, u32[]{:S(2)}) collective-permute-start(bf16[128,2048]{1,0:T(8,128)(2,1)S(1)} %broadcast_select_fusion.5.refs_4_), channel_id=1, source_target_pairs={{0,4},{2,6},{4,0},{6,2},{8,12},{10,14},{12,8},{14,10},{16,20},{18,... | collective-permute-start | bytes 1572872 | tf_op jit(solution)/shard_map/ppermute | solution.py:29
  118.2 24.2 %collective-permute-start.30 = (bf16[128,2048]{1,0:T(8,128)(2,1)S(1)}, bf16[128,2048]{1,0:T(8,128)(2,1)S(1)}, u32[]{:S(2)}, u32[]{:S(2)}) collective-permute-start(bf16[128,2048]{1,0:T(8,128)(2,1)S(1)} %collective-permute-done.29), channel_id=1, source_target_pairs={{8,0},{10,2},{12,4},{14,6},{16,24},{18,26},{20,28},{22,30},{9,1},{... | collective-permute-start | bytes 1572872 | tf_op jit(solution)/shard_map/ppermute | solution.py:29
  119.5 17.5 %collective-permute-start.25 = (bf16[64,2048]{1,0:T(8,128)(2,1)S(1)}, bf16[64,2048]{1,0:T(8,128)(2,1)S(1)}, u32[]{:S(2)}, u32[]{:S(2)}) collective-permute-start(bf16[64,2048]{1,0:T(8,128)(2,1)S(1)} %get-tuple-element.45), channel_id=1, source_target_pairs={{0,4},{2,6},{4,0},{6,2},{8,12},{10,14},{12,8},{14,10},{16,20},{18,... | collective-permute-start | bytes 786440 | tf_op jit(solution)/shard_map/ppermute | solution.py:29
  140.8 25.4 %collective-permute-start.27 = (bf16[544,512]{1,0:T(8,128)(2,1)S(1)}, bf16[544,512]{1,0:T(8,128)(2,1)S(1)}, u32[]{:S(2)}, u32[]{:S(2)}) collective-permute-start(bf16[544,512]{1,0:T(8,128)(2,1)S(1)} %get-tuple-element.21.refs_1_), channel_id=1, source_target_pairs={{0,1},{1,0},{2,3},{3,2},{4,5},{5,4},{6,7},{7,6},{8,9},{9,8},{10,11... | collective-permute-start | bytes 1671176 | tf_op jit(solution)/shard_map/ppermute | solution.py:29
  142.4 23.8 %copy-start.13 = (bf16[128,2048]{1,0:T(8,128)(2,1)}, bf16[128,2048]{1,0:T(8,128)(2,1)S(1)}, u32[]{:S(2)}) copy-start(bf16[128,2048]{1,0:T(8,128)(2,1)S(1)} %broadcast_select_fusion.4.refs_8_) | copy-start | bytes 1572868
  142.4 23.7 %collective-permute-start.33 = (bf16[128,2048]{1,0:T(8,128)(2,1)S(1)}, bf16[128,2048]{1,0:T(8,128)(2,1)S(1)}, u32[]{:S(2)}, u32[]{:S(2)}) collective-permute-start(bf16[128,2048]{1,0:T(8,128)(2,1)S(1)} %broadcast_select_fusion.4.refs_8_), channel_id=1, source_target_pairs={{0,4},{2,6},{4,0},{6,2},{8,12},{10,14},{12,8},{14,10},{16,20},{18,... | collective-permute-start | bytes 1572872 | tf_op jit(solution)/shard_map/ppermute | solution.py:29
  142.8 20.2 %collective-permute-start.31 = (bf16[64,2048]{1,0:T(8,128)(2,1)S(1)}, bf16[64,2048]{1,0:T(8,128)(2,1)}, u32[]{:S(2)}, u32[]{:S(2)}) collective-permute-start(bf16[64,2048]{1,0:T(8,128)(2,1)S(1)} %copy-done.17), channel_id=1, source_target_pairs={{0,4},{2,6},{4,0},{6,2},{8,12},{10,14},{12,8},{14,10},{16,20},{18,... | collective-permute-start | bytes 786440 | tf_op jit(solution)/shard_map/ppermute | solution.py:29
  144.5 21.6 %collective-permute-start.32 = (bf16[64,2048]{1,0:T(8,128)(2,1)}, bf16[64,2048]{1,0:T(8,128)(2,1)}, u32[]{:S(2)}, u32[]{:S(2)}) collective-permute-start(bf16[64,2048]{1,0:T(8,128)(2,1)} %get-tuple-element.43), channel_id=1, source_target_pairs={{0,4},{2,6},{4,0},{6,2},{8,12},{10,14},{12,8},{14,10},{16,20},{18,... | collective-permute-start | bytes 786440 | tf_op jit(solution)/shard_map/ppermute | solution.py:29
  144.8 21.3 %collective-permute-start.28 = (f32[8,640]{1,0:T(8,128)S(1)}, f32[8,640]{1,0:T(8,128)S(1)}, u32[]{:S(2)}, u32[]{:S(2)}) collective-permute-start(f32[8,640]{1,0:T(8,128)S(1)} %get-tuple-element.22.refs_3_), channel_id=1, source_target_pairs={{0,1},{1,0},{2,3},{3,2},{4,5},{5,4},{6,7},{7,6},{8,9},{9,8},{10,11... | collective-permute-start | bytes 61448 | tf_op jit(solution)/shard_map/ppermute | solution.py:29
  170.6 50.8 %copy-start.1 = (bf16[544,2048]{1,0:T(8,128)(2,1)S(1)}, bf16[544,2048]{1,0:T(8,128)(2,1)}, u32[]{:S(2)}) copy-start(bf16[544,2048]{1,0:T(8,128)(2,1)} %get-tuple-element.20.refs_0_) | copy-start | bytes 6684676
  170.7 50.1 %collective-permute-start.34 = (bf16[528,2048]{1,0:T(8,128)(2,1)S(1)}, bf16[528,2048]{1,0:T(8,128)(2,1)S(1)}, u32[]{:S(2)}, u32[]{:S(2)}) collective-permute-start(bf16[528,2048]{1,0:T(8,128)(2,1)S(1)} %shard_map.67.refs_1_), channel_id=1, source_target_pairs={{0,2},{2,0},{4,6},{6,4},{8,10},{10,8},{12,14},{14,12},{16,18},{18,... | collective-permute-start | bytes 6488072 | tf_op jit(solution)/shard_map/ppermute | solution.py:29
  170.8 50.0 %copy-start.7 = (bf16[128,2048]{1,0:T(8,128)(2,1)}, bf16[128,2048]{1,0:T(8,128)(2,1)S(1)}, u32[]{:S(2)}) copy-start(bf16[128,2048]{1,0:T(8,128)(2,1)S(1)} %pad_maximum_fusion.4.refs_3_) | copy-start | bytes 1572868
  170.8 0.8 collective-permute-start.35
  171.6 27.8 %collective-permute-start.36 = (bf16[128,2048]{1,0:T(8,128)(2,1)S(1)}, bf16[128,2048]{1,0:T(8,128)(2,1)S(1)}, u32[]{:S(2)}, u32[]{:S(2)}) collective-permute-start(bf16[128,2048]{1,0:T(8,128)(2,1)S(1)} %collective-permute-done.35), channel_id=1, source_target_pairs={{8,0},{10,2},{12,4},{14,6},{16,24},{18,26},{20,28},{22,30},{9,1},{... | collective-permute-start | bytes 1572872 | tf_op jit(solution)/shard_map/ppermute | solution.py:29
  173.0 51.5 %copy-start.5 = (bf16[128,2048]{1,0:T(8,128)(2,1)}, bf16[128,2048]{1,0:T(8,128)(2,1)S(1)}, u32[]{:S(2)}) copy-start(bf16[128,2048]{1,0:T(8,128)(2,1)S(1)} %pad_maximum_fusion.5.refs_3_) | copy-start | bytes 1572868
  173.0 26.8 %collective-permute-start.41 = (bf16[128,2048]{1,0:T(8,128)(2,1)S(1)}, bf16[128,2048]{1,0:T(8,128)(2,1)S(1)}, u32[]{:S(2)}, u32[]{:S(2)}) collective-permute-start(bf16[128,2048]{1,0:T(8,128)(2,1)S(1)} %pad_maximum_fusion.5.refs_3_), channel_id=1, source_target_pairs={{8,16},{10,18},{12,20},{14,22},{16,8},{18,10},{20,12},{22,14},{9,1... | collective-permute-start | bytes 1572872 | tf_op jit(solution)/shard_map/ppermute | solution.py:29
  199.5 21.3 %copy-start.10 = (bf16[128,2048]{1,0:T(8,128)(2,1)}, bf16[128,2048]{1,0:T(8,128)(2,1)S(1)}, u32[]{:S(2)}) copy-start(bf16[128,2048]{1,0:T(8,128)(2,1)S(1)} %broadcast_select_fusion.3.refs_4_) | copy-start | bytes 1572868
  199.5 21.3 %collective-permute-start.38 = (bf16[128,2048]{1,0:T(8,128)(2,1)S(1)}, bf16[128,2048]{1,0:T(8,128)(2,1)S(1)}, u32[]{:S(2)}, u32[]{:S(2)}) collective-permute-start(bf16[128,2048]{1,0:T(8,128)(2,1)S(1)} %broadcast_select_fusion.3.refs_4_), channel_id=1, source_target_pairs={{0,4},{2,6},{4,0},{6,2},{8,12},{10,14},{12,8},{14,10},{16,20},{18,... | collective-permute-start | bytes 1572872 | tf_op jit(solution)/shard_map/ppermute | solution.py:29
  199.8 25.3 %collective-permute-start.42 = (bf16[128,2048]{1,0:T(8,128)(2,1)S(1)}, bf16[128,2048]{1,0:T(8,128)(2,1)S(1)}, u32[]{:S(2)}, u32[]{:S(2)}) collective-permute-start(bf16[128,2048]{1,0:T(8,128)(2,1)S(1)} %collective-permute-done.41), channel_id=1, source_target_pairs={{8,0},{10,2},{12,4},{14,6},{16,24},{18,26},{20,28},{22,30},{9,1},{... | collective-permute-start | bytes 1572872 | tf_op jit(solution)/shard_map/ppermute | solution.py:29
  202.3 18.5 %collective-permute-start.37 = (bf16[1,64,2048]{2,1,0:T(8,128)(2,1)S(1)}, bf16[1,64,2048]{2,1,0:T(8,128)(2,1)S(1)}, u32[]{:S(2)}, u32[]{:S(2)}) collective-permute-start(bf16[1,64,2048]{2,1,0:T(8,128)(2,1)S(1)} %slice.97), channel_id=1, source_target_pairs={{0,8},{2,10},{4,12},{6,14},{8,0},{10,2},{12,4},{14,6},{16,24},{18,... | collective-permute-start | bytes 786440 | tf_op jit(solution)/shard_map/ppermute | solution.py:29
  205.7 20.3 %collective-permute-start.43 = (bf16[64,2048]{1,0:T(8,128)(2,1)S(1)}, bf16[64,2048]{1,0:T(8,128)(2,1)S(1)}, u32[]{:S(2)}, u32[]{:S(2)}) collective-permute-start(bf16[64,2048]{1,0:T(8,128)(2,1)S(1)} %get-tuple-element.34), channel_id=1, source_target_pairs={{0,4},{2,6},{4,0},{6,2},{8,12},{10,14},{12,8},{14,10},{16,20},{18,... | collective-permute-start | bytes 786440 | tf_op jit(solution)/shard_map/ppermute | solution.py:29
  224.5 12.8 %collective-permute-start.39 = (bf16[528,512]{1,0:T(8,128)(2,1)S(1)}, bf16[528,512]{1,0:T(8,128)(2,1)S(1)}, u32[]{:S(2)}, u32[]{:S(2)}) collective-permute-start(bf16[528,512]{1,0:T(8,128)(2,1)S(1)} %get-tuple-element.24.refs_1_), channel_id=1, source_target_pairs={{0,1},{1,0},{2,3},{3,2},{4,5},{5,4},{6,7},{7,6},{8,9},{9,8},{10,11... | collective-permute-start | bytes 1622024 | tf_op jit(solution)/shard_map/ppermute | solution.py:29
  225.2 13.9 %copy-start.9 = (bf16[128,2048]{1,0:T(8,128)(2,1)}, bf16[128,2048]{1,0:T(8,128)(2,1)S(1)}, u32[]{:S(2)}) copy-start(bf16[128,2048]{1,0:T(8,128)(2,1)S(1)} %broadcast_select_fusion.2.refs_4_) | copy-start | bytes 1572868
  225.2 13.8 %collective-permute-start.45 = (bf16[128,2048]{1,0:T(8,128)(2,1)S(1)}, bf16[128,2048]{1,0:T(8,128)(2,1)S(1)}, u32[]{:S(2)}, u32[]{:S(2)}) collective-permute-start(bf16[128,2048]{1,0:T(8,128)(2,1)S(1)} %broadcast_select_fusion.2.refs_4_), channel_id=1, source_target_pairs={{0,4},{2,6},{4,0},{6,2},{8,12},{10,14},{12,8},{14,10},{16,20},{18,... | collective-permute-start | bytes 1572872 | tf_op jit(solution)/shard_map/ppermute | solution.py:29
  226.0 13.0 %copy-start.24 = (bf16[64,2048]{1,0:T(8,128)(2,1)}, bf16[64,2048]{1,0:T(8,128)(2,1)S(1)}, u32[]{:S(2)}) copy-start(bf16[64,2048]{1,0:T(8,128)(2,1)S(1)} %collective-permute-done.43.refs_5_) | copy-start | bytes 786436
  226.0 13.0 %collective-permute-start.44 = (bf16[1,64,2048]{2,1,0:T(8,128)(2,1)S(1)}, bf16[1,64,2048]{2,1,0:T(8,128)(2,1)S(1)}, u32[]{:S(2)}, u32[]{:S(2)}) collective-permute-start(bf16[1,64,2048]{2,1,0:T(8,128)(2,1)S(1)} %bitcast.36), channel_id=1, source_target_pairs={{0,8},{2,10},{4,12},{6,14},{8,0},{10,2},{12,4},{14,6},{16,24},{18,... | collective-permute-start | bytes 786440 | tf_op jit(solution)/shard_map/ppermute | solution.py:29
  226.1 11.2 %collective-permute-start.40 = (f32[8,640]{1,0:T(8,128)S(1)}, f32[8,640]{1,0:T(8,128)S(1)}, u32[]{:S(2)}, u32[]{:S(2)}) collective-permute-start(f32[8,640]{1,0:T(8,128)S(1)} %get-tuple-element.25.refs_3_), channel_id=1, source_target_pairs={{0,1},{1,0},{2,3},{3,2},{4,5},{5,4},{6,7},{7,6},{8,9},{9,8},{10,11... | collective-permute-start | bytes 61448 | tf_op jit(solution)/shard_map/ppermute | solution.py:29
  244.5 2.7 %collective-permute-start.46 = (bf16[256,2048]{1,0:T(8,128)(2,1)S(1)}, bf16[256,2048]{1,0:T(8,128)(2,1)S(1)}, u32[]{:S(2)}, u32[]{:S(2)}) collective-permute-start(bf16[256,2048]{1,0:T(8,128)(2,1)S(1)} %get-tuple-element.28), channel_id=1, source_target_pairs={{0,2},{2,0},{4,6},{6,4},{8,10},{10,8},{12,14},{14,12},{16,18},{18,... | collective-permute-start | bytes 3145736 | tf_op jit(solution)/shard_map/ppermute | solution.py:29
  (14 other events, 68.7 us)
